TPU v7x, 256 devices: a whole 4x4x8 slice. The times are simulated.
256 devices in a mesh: ep: 16 (over y, x), tp: 16 (over z, core).
Axes of the slice: x: 4, y: 4, z: 8, core: 2. Of those that a mesh axis runs over, the one named last changes fastest.
Arguments:
- mixer_input_rows: bfloat16 [32768, 2048], P(('ep', 'tp')), may hold values from -6 to 6
- mixer_norm_gain: float32 [2048], replicated, may hold values from 0.1 to 1.9
- query_weight: bfloat16 [2048, 2048], P(None, 'tp'), may hold values from -0.125 to 0.125
- key_weight: bfloat16 [2048, 2048], P(None, 'tp'), may hold values from -0.125 to 0.125
- value_weight: bfloat16 [2048, 2048], P(None, 'tp'), may hold values from -0.125 to 0.125
- write_strength_projection: bfloat16 [2048, 16], replicated, may hold values from -0.125 to 0.125
- decay_projection: bfloat16 [2048, 16], replicated, may hold values from -0.125 to 0.125
- head_decay_speed: float32 [16], P('tp'), may hold values from 0 to 1
- largest_write_strength: float32 [16], P('tp'), may hold values from 0 to 1
- extra_log_decay: float32 [32768, 16], P('ep', 'tp'), may hold values from -1 to 0
- head_norm_gain: float32 [128], replicated, may hold values from 0.1 to 1.9
- mixer_output_weight: bfloat16 [2048, 2048], P('tp'), may hold values from -0.125 to 0.125
- expert_input_rows: bfloat16 [2048, 2048], P(('ep', 'tp')), may hold values from -6 to 6
- expert_norm_gain: float32 [2048], replicated, may hold values from 0.1 to 1.9
- routes: int32 [2048, 2], P(('ep', 'tp')), may hold values from 0 to 15, all different within a row; in each aligned block of 8 rows (0 to 7, 8 to 15, ...) at most 2 rows name the same one
- expert_route_weight: float32 [2048, 2], P(('ep', 'tp')), may hold values from 0.2 to 1
- gate_weight: bfloat16 [16, 2048, 7168], P('ep', None, 'tp'), may hold values from -0.125 to 0.125
- up_weight: bfloat16 [16, 2048, 7168], P('ep', None, 'tp'), may hold values from -0.125 to 0.125
- down_weight: bfloat16 [16, 7168, 2048], P('ep', 'tp'), may hold values from -0.0625 to 0.0625
Outputs:
- mix_out: bfloat16 [32768, 2048], P(('ep', 'tp'))
- exp_out: bfloat16 [2048, 2048], P(('ep', 'tp'))
Inputs may be any that keep to these rules, and one draw needn't show every extreme that they name: `routes`: within the rows of one device (aligned blocks of 8 rows) no expert is named more than 2 times, some device names some expert exactly 2 times, and the 2 experts of a row differ.
All inputs are finite; a program needn't handle non-finite values.
Results may differ from a plain program's by a relative error of at most 0.019.
Values may be sent and summed in bfloat16 or wider, within the bound.
No kernel may reach another device: no remote copies, remote signals or barrier semaphores. Data moves between devices by JAX's collectives and lax.ppermute only.
A program may use at most 128 MiB of HBM per device.

v0:
```python
import functools

import jax
import jax.numpy as jnp
from jax import lax
from jax.experimental import pallas as pl
from jax.experimental.pallas import tpu as pltpu
from jax.sharding import Mesh
from jax.sharding import PartitionSpec as P


HEAD = 128
BLOCK = 128
TOKENS = 8
SLOTS = 2
EP = ("ep_0", "ep_1")
TP = ("tp_0", "tp_1")
EP_TP = ("ep_0", "ep_1", "tp_0", "tp_1")
F32 = jnp.float32
BF16 = jnp.bfloat16


norm_eps = 1e-06
NN = (((1,), (0,)), ((), ()))
NT = (((1,), (1,)), ((), ()))
TN = (((0,), (0,)), ((), ()))


def mm(a, b, dims=NN):
    return lax.dot_general(a.astype(BF16), b.astype(BF16), dims, preferred_element_type=F32)


def silu(x):
    return x / (1.0 + jnp.exp(-x))


def rms_scale(rows_in, gain_vec):
    widened = rows_in.astype(F32)
    scaled = widened * lax.rsqrt(jnp.mean(widened * widened, axis=-1, keepdims=True) + norm_eps)
    return (scaled * gain_vec).astype(BF16)


def invert_unit_lower(mats, row, col):
    apart = row ^ col
    eye = (row == col).astype(F32)
    size = 1
    invs = None
    while size < BLOCK:
        pick = (apart >= size) & (apart < 2 * size)
        parts = [jnp.where(pick, m, 0.0) for m in mats]
        if invs is None:
            invs = [eye - p for p in parts]
        else:
            invs_low = [x.astype(BF16) for x in invs]
            half = [mm(p, x) for p, x in zip(parts, invs_low)]
            invs = [x - mm(xl, h) for x, xl, h in zip(invs, invs_low, half)]
        size *= 2
    return invs


def weights_kernel(head_ref, q_ref, k_ref, v_ref, strength_ref, decay_ref, out_ref):
    out_ref[:, 0:HEAD] = q_ref[...]
    out_ref[:, HEAD : 2 * HEAD] = k_ref[...]
    out_ref[:, 2 * HEAD : 3 * HEAD] = v_ref[...]
    heads = strength_ref.shape[1]
    row = lax.broadcasted_iota(jnp.int32, (heads, HEAD), 0)
    col = lax.broadcasted_iota(jnp.int32, (heads, HEAD), 1)
    here = row == head_ref[0]
    first = (here & (col == 0)).astype(BF16)
    second = (here & (col == 1)).astype(BF16)
    out_ref[:, 3 * HEAD :] = (mm(strength_ref[...], first) + mm(decay_ref[...], second)).astype(BF16)


def join_weights(head, query, key, value, strength, decay):
    depth = query.shape[0]
    step = depth // 4
    tall = lambda x: pl.BlockSpec((step, x.shape[1]), lambda i: (i, 0))
    return pl.pallas_call(
        weights_kernel,
        grid=(4,),
        out_shape=jax.ShapeDtypeStruct((depth, 4 * HEAD), BF16),
        in_specs=[pl.BlockSpec(memory_space=pltpu.SMEM)] + [tall(x) for x in (query, key, value, strength, decay)],
        out_specs=pl.BlockSpec((step, 4 * HEAD), lambda i: (i, 0)),
        cost_estimate=pl.CostEstimate(flops=10**8, bytes_accessed=depth * HEAD * 16, transcendentals=0),
    )(head, query, key, value, strength, decay)


def span_kernel(count, scal_ref, rows_ref, w_ref, extra_ref, g_ref, h_ref, ab_ref, proj, low, high, lasts):
    proj[...] = lax.dot_general(rows_ref[...], w_ref[...], NN, preferred_element_type=F32)
    row = lax.broadcasted_iota(jnp.int32, (BLOCK, BLOCK), 0)
    col = lax.broadcasted_iota(jnp.int32, (BLOCK, BLOCK), 1)
    upper = (row <= col).astype(F32)
    speed, largest = scal_ref[0], scal_ref[1]
    start = pl.program_id(0) * count
    mats, keep = [], []
    for b in range(count):
        at = slice(b * BLOCK, (b + 1) * BLOCK)
        q = silu(proj[at, 0:HEAD])
        k = silu(proj[at, HEAD : 2 * HEAD])
        v = silu(proj[at, 2 * HEAD : 3 * HEAD])
        k = k * lax.rsqrt(jnp.sum(k * k, axis=1, keepdims=True) + 1e-06)
        small = proj[at, 3 * HEAD : 4 * HEAD]
        strength = largest * (1.0 / (1.0 + jnp.exp(-small[:, 0:1])))
        flipped = small.T
        x = flipped[0:8, :]
        soft = jnp.maximum(x, 0.0) + jnp.log1p(jnp.exp(-jnp.abs(x)))
        steps = extra_ref[pl.ds(start + b, 1), :] - speed * soft[1:2, :]
        cum_row = lax.dot_general(
            jnp.broadcast_to(steps, (8, BLOCK)), upper, NN, preferred_element_type=F32, precision=lax.Precision.HIGHEST
        )[0:1, :]
        across = jnp.broadcast_to(cum_row, (BLOCK, BLOCK))
        down = across.T
        total = jnp.broadcast_to(cum_row[:, BLOCK - 1 : BLOCK], (BLOCK, BLOCK))
        decay = jnp.exp(jnp.where(row >= col, down - across, -1e30))
        grow = jnp.exp(down)
        both = mm(jnp.concatenate([k, q], axis=0), k, NT)
        mats.append(jnp.where(row > col, both[:BLOCK] * decay * strength, 0.0))
        right = jnp.concatenate([v * strength, k * (grow * strength)], axis=1)
        keep.append((q * grow, both[BLOCK:] * decay, right, k * jnp.exp(total - down)))
        lasts[start + b] = jnp.exp(total[0:8, :])
    invs = invert_unit_lower(mats, row, col)
    for b in range(count):
        query_dec, scores, right, keys_dec = keep[b]
        solved = mm(invs[b], right)
        seen = mm(scores, solved)
        kept = mm(keys_dec, solved, TN)
        high[start + b, :, :HEAD] = kept[:, :HEAD]
        high[start + b, :, HEAD:] = seen[:, :HEAD]
        low[start + b, :HEAD, :] = (query_dec - seen[:, HEAD:]).astype(BF16)
        low[start + b, HEAD:, :] = kept[:, HEAD:].astype(BF16)

    @pl.when(pl.program_id(0) == pl.num_programs(0) - 1)
    def _():
        maps = (row == col).astype(F32)
        memory = jnp.zeros((HEAD, HEAD), F32)
        for j in range(low.shape[0]):
            both = jnp.concatenate([maps, memory], axis=1).astype(BF16)
            out = mm(low[j], both)
            g_ref[j * BLOCK : (j + 1) * BLOCK, :] = out[:HEAD, :HEAD].astype(BF16)
            h_ref[j * BLOCK : (j + 1) * BLOCK, :] = out[:HEAD, HEAD:] + high[j, :, HEAD:]
            last = lasts[j, 0:1, :]
            maps = maps * last - out[HEAD:, :HEAD]
            memory = memory * last - out[HEAD:, HEAD:] + high[j, :, :HEAD]
        ab_ref[:, :HEAD] = maps.astype(BF16)
        ab_ref[:, HEAD:] = memory.astype(BF16)


def span_terms(scal, rows, weights, extra, count):
    length, depth = rows.shape
    blocks = length // BLOCK
    width = weights.shape[1]
    whole = lambda i: (0, 0)
    return pl.pallas_call(
        functools.partial(span_kernel, count),
        grid=(blocks // count,),
        out_shape=(
            jax.ShapeDtypeStruct((length, HEAD), BF16),
            jax.ShapeDtypeStruct((length, HEAD), F32),
            jax.ShapeDtypeStruct((HEAD, 2 * HEAD), BF16),
        ),
        in_specs=[
            pl.BlockSpec(memory_space=pltpu.SMEM),
            pl.BlockSpec((count * BLOCK, depth), lambda i: (i, 0)),
            pl.BlockSpec(weights.shape, whole),
            pl.BlockSpec(extra.shape, whole),
        ],
        out_specs=(
            pl.BlockSpec((length, HEAD), whole),
            pl.BlockSpec((length, HEAD), whole),
            pl.BlockSpec((HEAD, 2 * HEAD), whole),
        ),
        scratch_shapes=[
            pltpu.VMEM((count * BLOCK, width), F32),
            pltpu.VMEM((blocks, 2 * HEAD, HEAD), BF16),
            pltpu.VMEM((blocks, HEAD, 2 * HEAD), F32),
            pltpu.VMEM((blocks, 8, HEAD), F32),
        ],
        cost_estimate=pl.CostEstimate(
            flops=length * 2 * (depth * width + 40 * HEAD * HEAD * 4),
            bytes_accessed=2 * (rows.size + weights.size) + length * HEAD * 6,
            transcendentals=0,
        ),
    )(scal, rows, weights, extra)


def row_kernel(here_ref, own_ref, one_ref, two_ref, three_ref, before_ref, total_ref, slots):
    here = here_ref[0]
    slots[here] = own_ref[...]
    slots[(here + 3) % 4] = one_ref[...]
    slots[(here + 2) % 4] = two_ref[...]
    slots[(here + 1) % 4] = three_ref[...]
    row = lax.broadcasted_iota(jnp.int32, (HEAD, 2 * HEAD), 0)
    col = lax.broadcasted_iota(jnp.int32, (HEAD, 2 * HEAD), 1)
    eye = (row == col).astype(F32)
    so_far = slots[0].astype(F32)
    before = jnp.where(here == 0, eye, so_far)
    for k in range(1, 4):
        piece = slots[k]
        own = jnp.where(col >= HEAD, piece.astype(F32), 0.0)
        so_far = mm(piece[:, :HEAD], so_far) + own
        if k < 3:
            before = jnp.where(here > k, so_far, before)
    before_ref[...] = before
    total_ref[...] = so_far.astype(BF16)


def compose_row(here, own, one, two, three):
    vmem = pl.BlockSpec(memory_space=pltpu.VMEM)
    return pl.pallas_call(
        row_kernel,
        out_shape=(jax.ShapeDtypeStruct((HEAD, 2 * HEAD), F32), jax.ShapeDtypeStruct((HEAD, 2 * HEAD), BF16)),
        in_specs=[pl.BlockSpec(memory_space=pltpu.SMEM)] + [vmem] * 4,
        out_specs=(vmem, vmem),
        scratch_shapes=[pltpu.VMEM((4, HEAD, 2 * HEAD), BF16)],
        compiler_params=pltpu.CompilerParams(vmem_limit_bytes=8 * 1024 * 1024),
        cost_estimate=pl.CostEstimate(flops=12 * HEAD**3, bytes_accessed=8 * HEAD * HEAD, transcendentals=0),
    )(here, own, one, two, three)


def apply_kernel(here_ref, one_ref, two_ref, three_ref, before_ref, g_ref, h_ref, gain_ref, out_ref, slots):
    here = here_ref[0]
    slots[(here + 3) % 4] = one_ref[...]
    slots[(here + 2) % 4] = two_ref[...]
    slots[(here + 1) % 4] = three_ref[...]
    memory = jnp.where(here > 0, slots[0][:, HEAD:].astype(F32), 0.0)
    for k in range(1, 3):
        piece = slots[k]
        moved = mm(piece[:, :HEAD], memory) + piece[:, HEAD:].astype(F32)
        memory = jnp.where(here > k, moved, memory)
    memory = mm(before_ref[:, :HEAD], memory) + before_ref[:, HEAD:]
    heads_out = mm(g_ref[...], memory) + h_ref[...]
    scale = lax.rsqrt(jnp.mean(heads_out * heads_out, axis=1, keepdims=True) + norm_eps)
    out_ref[...] = (heads_out * scale * gain_ref[...]).astype(BF16)


def apply_memory(here, one, two, three, before, g, h, gain):
    vmem = pl.BlockSpec(memory_space=pltpu.VMEM)
    return pl.pallas_call(
        apply_kernel,
        out_shape=jax.ShapeDtypeStruct(h.shape, BF16),
        in_specs=[pl.BlockSpec(memory_space=pltpu.SMEM)] + [vmem] * 7,
        out_specs=vmem,
        scratch_shapes=[pltpu.VMEM((4, HEAD, 2 * HEAD), BF16)],
        compiler_params=pltpu.CompilerParams(vmem_limit_bytes=8 * 1024 * 1024),
        cost_estimate=pl.CostEstimate(flops=h.size * 2 * HEAD, bytes_accessed=h.size * 8, transcendentals=0),
    )(here, one, two, three, before, g, h, gain.reshape(1, HEAD))


def output_kernel(core_ref, x_ref, w_ref, mine_ref, theirs_ref, total):
    step = pl.program_id(0)

    @pl.when(step == 0)
    def _():
        total[...] = jnp.zeros_like(total)

    rows = jnp.concatenate([x_ref[0], x_ref[1]], axis=1)
    total[...] += mm(rows, w_ref[...])

    @pl.when(step == pl.num_programs(0) - 1)
    def _():
        first = core_ref[0] == 0
        mine_ref[...] = jnp.where(first, total[:BLOCK], total[BLOCK:])
        theirs_ref[...] = jnp.where(first, total[BLOCK:], total[:BLOCK]).astype(BF16)


def output_product(core, by_head, weights):
    depth, width = weights.shape
    whole = lambda i: (0, 0)
    return pl.pallas_call(
        output_kernel,
        grid=(depth // (2 * HEAD),),
        out_shape=(jax.ShapeDtypeStruct((BLOCK, width), F32), jax.ShapeDtypeStruct((BLOCK, width), BF16)),
        in_specs=[
            pl.BlockSpec(memory_space=pltpu.SMEM),
            pl.BlockSpec((2, 2 * BLOCK, HEAD), lambda i: (i, 0, 0)),
            pl.BlockSpec((2 * HEAD, width), lambda i: (i, 0)),
        ],
        out_specs=(pl.BlockSpec((BLOCK, width), whole), pl.BlockSpec((BLOCK, width), whole)),
        scratch_shapes=[pltpu.VMEM((2 * BLOCK, width), F32)],
        cost_estimate=pl.CostEstimate(
            flops=4 * BLOCK * depth * width, bytes_accessed=2 * depth * width, transcendentals=0
        ),
    )(core, by_head.reshape(-1, 2 * BLOCK, HEAD), weights)


def route_columns(side, experts):
    tokens = side.shape[1]
    expert = lax.broadcasted_iota(jnp.int32, (experts, tokens), 0).astype(F32)
    first, second = side[0:1] == expert, side[1:2] == expert
    named = (first | second).astype(F32)
    row = lax.broadcasted_iota(jnp.int32, (tokens, tokens), 0)
    col = lax.broadcasted_iota(jnp.int32, (tokens, tokens), 1)
    earlier = ((row < col) & (row // TOKENS == col // TOKENS)).astype(F32)
    return first, named, mm(named, earlier)


def slot_rows(named, slots, e):
    tokens = named.shape[1]
    rows = tokens // TOKENS * SLOTS
    row = lax.broadcasted_iota(jnp.int32, (rows, tokens), 0)
    col = lax.broadcasted_iota(jnp.int32, (rows, tokens), 1)
    taken = jnp.where(named[e : e + 1] > 0.5, slots[e : e + 1], -1.0)
    return (taken == (row % SLOTS).astype(F32)) & (row // SLOTS == col // TOKENS)


def pack_kernel(experts, tok_ref, out_ref):
    width = out_ref.shape[1]
    side = tok_ref[:, width:].astype(F32).T
    _, named, slots = route_columns(side, experts)
    rows = out_ref.shape[0] // experts
    group = 4
    for e in range(0, experts, group):
        pick = jnp.concatenate([slot_rows(named, slots, e + i).astype(F32) for i in range(group)], axis=0)
        out_ref[e * rows : (e + group) * rows, :] = mm(pick, tok_ref[:, :width]).astype(BF16)


def pack_tokens(tokens, experts):
    count, width = tokens.shape
    vmem = pl.BlockSpec(memory_space=pltpu.VMEM)
    rows = count // TOKENS * SLOTS * experts
    return pl.pallas_call(
        functools.partial(pack_kernel, experts),
        out_shape=jax.ShapeDtypeStruct((rows, width - HEAD), BF16),
        in_specs=[vmem],
        out_specs=vmem,
        cost_estimate=pl.CostEstimate(flops=2 * rows * count * width, bytes_accessed=2 * rows * width, transcendentals=0),
    )(tokens)


def combine_kernel(experts, core_ref, side_ref, back_ref, mine_ref, theirs_ref, total):
    side = side_ref[...].astype(F32).T
    first, named, slots = route_columns(side, experts)
    share = [side[2 + k : 3 + k] + side[4 + k : 5 + k] + side[6 + k : 7 + k] for k in range(2)]
    picks = []
    for e in range(experts):
        share_row = jnp.where(first[e : e + 1], share[0], share[1])
        picks.append(jnp.where(slot_rows(named, slots, e), share_row, 0.0))
    pick = jnp.concatenate(picks, axis=0)
    high = pick.astype(BF16)
    low = (pick - high.astype(F32)).astype(BF16)
    back = back_ref[...]
    out = mm(high, back, TN) + mm(low, back, TN)
    total[...] = out.reshape(total.shape)
    core = core_ref[0]
    for z in range(mine_ref.shape[0]):
        mine_ref[z] = total[2 * z + core].astype(BF16)
        theirs_ref[z] = total[2 * z + 1 - core].astype(BF16)


def combine_tokens(core, tokens, back, experts):
    count, _ = tokens.shape
    width = back.shape[1]
    devices = count // TOKENS
    whole = lambda i: (0, 0)
    cube = lambda i: (0, 0, 0)
    half = (devices // 2, TOKENS, width)
    out = jax.ShapeDtypeStruct(half, BF16)
    return pl.pallas_call(
        functools.partial(combine_kernel, experts),
        grid=(1,),
        out_shape=(out, out),
        in_specs=[
            pl.BlockSpec(memory_space=pltpu.SMEM),
            pl.BlockSpec((count, HEAD), lambda i: (0, width // HEAD)),
            pl.BlockSpec(back.shape, whole),
        ],
        out_specs=(pl.BlockSpec(half, cube), pl.BlockSpec(half, cube)),
        scratch_shapes=[pltpu.VMEM((devices, TOKENS, width), F32)],
        cost_estimate=pl.CostEstimate(
            flops=4 * count * back.size, bytes_accessed=2 * back.size + 4 * count * width, transcendentals=0
        ),
    )(core, tokens, back)


def expert_kernel(rows_ref, gate_ref, up_ref, down_ref, out_ref, rows, gate, up, down, sems):
    copies = [
        pltpu.make_async_copy(src, dst, sems.at[i])
        for i, (src, dst) in enumerate(((rows_ref, rows), (gate_ref, gate), (up_ref, up), (down_ref, down)))
    ]
    for copy in copies:
        copy.start()
    copies[0].wait()
    copies[1].wait()
    gated = silu(mm(rows[...], gate[...], NT))
    copies[2].wait()
    hidden = (gated * mm(rows[...], up[...], NT)).astype(BF16)
    copies[3].wait()
    out_ref[...] = mm(hidden, down[...]).astype(BF16)


def expert_sums(rows, gate, up, down):
    count, width = rows.shape
    units = gate.shape[0]
    return pl.pallas_call(
        expert_kernel,
        out_shape=jax.ShapeDtypeStruct((count, width), BF16),
        in_specs=[pl.BlockSpec(memory_space=pl.ANY)] * 4,
        out_specs=pl.BlockSpec(memory_space=pltpu.VMEM),
        scratch_shapes=[
            pltpu.VMEM((count, width), BF16),
            pltpu.VMEM((units, width), BF16),
            pltpu.VMEM((units, width), BF16),
            pltpu.VMEM((units, width), BF16),
            pltpu.SemaphoreType.DMA((4,)),
        ],
        cost_estimate=pl.CostEstimate(
            flops=6 * count * width * units, bytes_accessed=6 * units * width + 4 * count * width, transcendentals=0
        ),
    )(rows, gate, up, down)


def around(x, axis):
    size = lax.axis_size(axis)
    out = []
    for k in range(1, size):
        out.append(lax.ppermute(x, axis, [(i, (i + k) % size) for i in range(size)]))
    return out


def mixed_step(
    mixer_input_rows,
    mixer_norm_gain,
    query_weight,
    key_weight,
    value_weight,
    write_strength_projection,
    decay_projection,
    head_decay_speed,
    largest_write_strength,
    extra_log_decay,
    head_norm_gain,
    mixer_output_weight,
    expert_input_rows,
    expert_norm_gain,
    routes,
    expert_route_weight,
    gate_weight,
    up_weight,
    down_weight,
):
    head = lax.axis_index(TP)
    core = lax.axis_index("tp_1")
    experts = gate_weight.shape[0] * lax.axis_size(EP)
    cross = lambda x: lax.ppermute(x, "tp_1", [(0, 1), (1, 0)])

    mix_normed = rms_scale(mixer_input_rows, mixer_norm_gain)
    mix_rows = lax.all_gather(mix_normed, TP, axis=0, tiled=True)

    exp_normed = rms_scale(expert_input_rows, expert_norm_gain)
    parts, rest = [], expert_route_weight
    for _ in range(3):
        part = lax.reduce_precision(rest, 8, 7)
        parts.append(part.astype(BF16))
        rest = rest - part
    side = jnp.concatenate([routes.astype(BF16)] + parts, axis=1)
    side = jnp.pad(side, ((0, 0), (0, HEAD - side.shape[1])))
    tokens = lax.all_gather(jnp.concatenate([exp_normed, side], axis=1), TP, axis=0, tiled=True)
    packed = pack_tokens(tokens, experts)
    exp_rows = lax.all_to_all(packed, EP, split_axis=0, concat_axis=0, tiled=True)
    partial = expert_sums(exp_rows, gate_weight[0].T, up_weight[0].T, down_weight[0])
    back = lax.all_to_all(partial, EP, split_axis=0, concat_axis=0, tiled=True)
    mine, theirs = combine_tokens(core[None], tokens, back, experts)
    crossed = cross(theirs)
    pair = (mine.astype(F32) + crossed.astype(F32)).astype(BF16)

    weights = join_weights(
        head[None], query_weight, key_weight, value_weight, write_strength_projection, decay_projection
    )
    scal = jnp.concatenate([head_decay_speed, largest_write_strength])
    extra = extra_log_decay.reshape(-1, BLOCK)
    gains, local, span = span_terms(scal, mix_rows, weights, extra, 8)
    before, total = compose_row(lax.axis_index("ep_1")[None], span, *around(span, "ep_1"))
    mixed = apply_memory(lax.axis_index("ep_0")[None], *around(total, "ep_0"), before, gains, local, head_norm_gain)

    by_head = lax.all_to_all(mixed, "tp_0", split_axis=0, concat_axis=0, tiled=True)
    w_own = lax.all_gather(mixer_output_weight, "tp_0", axis=0, tiled=True)
    mix_mine, mix_theirs = output_product(core[None], by_head, w_own)
    mix_out = (mix_mine + cross(mix_theirs).astype(F32)).astype(BF16)

    pieces = lax.all_to_all(pair, "tp_0", split_axis=0, concat_axis=0, tiled=True)
    exp_out = jnp.sum(pieces.astype(F32), axis=0).astype(BF16)
    return (mix_out, exp_out)


def solution(mesh):
    torus = Mesh(mesh.devices.reshape(4, 4, 8, 2), ("ep_0", "ep_1", "tp_0", "tp_1"))
    placed = (
        P(EP_TP, None),
        P(),
        P(None, TP),
        P(None, TP),
        P(None, TP),
        P(),
        P(),
        P(TP),
        P(TP),
        P(EP, TP),
        P(),
        P(TP, None),
        P(EP_TP, None),
        P(),
        P(EP_TP, None),
        P(EP_TP, None),
        P(EP, None, TP),
        P(EP, None, TP),
        P(EP, TP, None),
    )
    return jax.shard_map(
        mixed_step,
        mesh=torus,
        in_specs=placed,
        out_specs=(P(EP_TP, None), P(EP_TP, None)),
        check_vma=False,
    )
```

profile of v0, /device:TPU:1, one launch (start us, length us, event | category | flops | bytes accessed | tf_op | source)
XLA Modules:
  0.0 186.6 jit_solution(2817432545691001765)
XLA Ops:
  7.2 0.0 copy-start.12
  7.2 0.0 copy-start.13
  7.2 0.0 copy-start.8
  7.2 0.0 copy-start.11
  7.2 0.0 all-gather.3.cloned.1.call-start
  7.3 1.2 fusion
  8.5 2.0 %fusion.2 = bf16[128,2048]{1,0:T(8,128)(2,1)} fusion(bf16[128,2048]{1,0:T(8,128)(2,1)} %param.19, f32[2048]{0:T(1024)} %param.20, f32[128]{0:T(128)S(1)} %add_rsqrt_fusion.1), kind=kLoop, calls=%fused_computation.4 | loop fusion | flops 1048576 | bytes 1057280 | tf_op jit(solution)/shard_map/convert_element_type | solution.py:40
  10.5 0.0 all-gather.3.cloned.1.call-update
  10.5 0.0 all-gather.5.cloned.1.call-start
  10.6 0.7 all-gather.5.cloned.1.call-update
  11.3 0.0 copy-done.12
  11.3 0.1 copy.28
  11.4 0.0 copy-done.13
  11.4 0.1 copy.30
  11.5 0.1 fusion.14
  11.6 0.0 copy-done.8
  11.6 0.1 fusion.3
  11.7 0.0 copy-done.11
  11.7 0.1 fusion.5
  11.8 26.0 %all_gather.11.tok_ref.side_ref = bf16[128,2176]{1,0:T(8,128)(2,1)} all-gather(bf16[8,2176]{1,0:T(8,128)(2,1)S(1)} %pad_maximum_fusion), channel_id=1, replica_groups=mesh['ep_0'=4,'ep_1'=4,'tp_0'=8,'tp_1'=2] {'tp_0','tp_1'}, dimensions={0}, use_global_device_ids=true | all-gather | bytes 591872 | tf_op jit(solution)/shard_map/all_gather | solution.py:457
  37.8 3.2 %shard_map.199 = bf16[512,2048]{1,0:T(8,128)(2,1)} custom-call(bf16[128,2176]{1,0:T(8,128)(2,1)} %all_gather.11.tok_ref.side_ref), custom_call_target="tpu_custom_call" | custom-call | flops 285212672 | bytes 2228224 | tf_op jit(solution)/shard_map/pallas_call | solution.py:321
  41.0 34.6 %all_to_all.36 = bf16[16,32,2048]{2,1,0:T(8,128)(2,1)} all-to-all(bf16[16,32,2048]{2,1,0:T(8,128)(2,1)} %bitcast.20), channel_id=1, replica_groups=mesh['ep_0'=4,'ep_1'=4,'tp_0'=8,'tp_1'=2] {'ep_0','ep_1'}, dimensions={0} | all-to-all | bytes 4194304 | tf_op jit(solution)/shard_map/all_to_all | solution.py:459
  75.6 7.4 %shard_map.200 = bf16[512,2048]{1,0:T(8,128)(2,1)} custom-call(bf16[512,2048]{1,0:T(8,128)(2,1)} %bitcast.22, bf16[448,2048]{1,0:T(8,128)(2,1)} %bitcast.23, bf16[448,2048]{1,0:T(8,128)(2,1)} %bitcast.24, bf16[448,2048]{1,0:T(8,128)(2,1)} %bitcast.25), custom_call_target="tpu_custom_call" | custom-call | flops 2818572288 | bytes 9699328 | tf_op jit(solution)/shard_map/pallas_call | solution.py:394
  83.1 0.0 copy-start.9
  83.1 0.0 copy-start.10
  83.1 3.9 %all-to-all-start.2 = ((bf16[16,32,2048]{2,1,0:T(8,128)(2,1)}), bf16[16,32,2048]{2,1,0:T(8,128)(2,1)S(1)}, u32[]{:S(2)}, u32[]{:S(2)}) async-start(bf16[16,32,2048]{2,1,0:T(8,128)(2,1)} %bitcast.21), calls=%async_computation.2 | async-start | bytes 4194304 | tf_op jit(solution)/shard_map/all_to_all | solution.py:461
  87.0 0.0 copy-done.9
  87.0 1.0 copy.26.strength_ref
  88.0 1.0 copy.27.decay_ref
  90.3 4.3 %shard_map.194.w_ref = bf16[2048,512]{1,0:T(8,128)(2,1)} custom-call(s32[1]{0:T(128)} %bitcast.3.head_ref, bf16[2048,128]{1,0:T(8,128)(2,1)} %q_ref.1, bf16[2048,128]{1,0:T(8,128)(2,1)} %k_ref.1, bf16[2048,128]{1,0:T(8,128)(2,1)} %v_ref.1, bf16[2048,16]{1,0:T(8,128)(2,1)} %copy.26.strength_ref, bf16[2048,16]{1,0:T(8,128)(2,1)} %copy.27.decay_ref), custom_call_target="tpu_custom_call" | custom-call | flops 100000000 | bytes 4194304 | tf_op jit(solution)/shard_map/pallas_call | solution.py:78
  94.7 0.6 pad_maximum_fusion.1.scal_ref
  95.3 20.3 %shard_map.195 = (bf16[2048,128]{1,0:T(8,128)(2,1)}, f32[2048,128]{1,0:T(8,128)}, bf16[128,256]{1,0:T(8,128)(2,1)}) custom-call(f32[2]{0:T(128)} %pad_maximum_fusion.1.scal_ref, bf16[2048,2048]{1,0:T(8,128)(2,1)} %all-gather.3.cloned.1.call-done.rows_ref, bf16[2048,512]{1,0:T(8,128)(2,1)} %shard_map.194.w_ref, f32[16,128]{1,0:T(8,128)} %bitcast.26), custom_call_target="tpu_custom_call" | custom-call | flops 15032385536 | bytes 12058624 | tf_op jit(solution)/shard_map/pallas_call | solution.py:153
  115.6 1.2 collective-permute-start
  116.8 2.4 %collective-permute-start.1 = (bf16[128,256]{1,0:T(8,128)(2,1)}, bf16[128,256]{1,0:T(8,128)(2,1)S(1)}, u32[]{:S(2)}, u32[]{:S(2)}) collective-permute-start(bf16[128,256]{1,0:T(8,128)(2,1)} %get-tuple-element.11.own_ref), channel_id=1, source_target_pairs={{0,32},{16,48},{32,0},{48,16},{1,33},{17,49},{33,1},{49,17},{2,34}... | collective-permute-start | bytes 196616 | tf_op jit(solution)/shard_map/ppermute | solution.py:416
  119.2 1.2 collective-permute-start.2
  120.4 0.1 collective-permute-done.one_ref
  120.5 1.3 collective-permute-done.1.two_ref
  121.9 1.3 collective-permute-done.2.three_ref
  123.2 0.8 copy-done.2
  124.0 0.5 shard_map.196
  124.5 1.1 collective-permute-start.3
  125.6 2.4 %collective-permute-start.4 = (bf16[128,256]{1,0:T(8,128)(2,1)S(1)}, bf16[128,256]{1,0:T(8,128)(2,1)S(1)}, u32[]{:S(2)}, u32[]{:S(2)}) collective-permute-start(bf16[128,256]{1,0:T(8,128)(2,1)S(1)} %get-tuple-element.12), channel_id=1, source_target_pairs={{0,128},{64,192},{128,0},{192,64},{1,129},{65,193},{129,1},{193,65... | collective-permute-start | bytes 196616 | tf_op jit(solution)/shard_map/ppermute | solution.py:416
  128.0 1.2 collective-permute-start.5
  129.2 0.0 collective-permute-done.3.one_ref
  129.2 1.2 collective-permute-done.4.two_ref
  130.4 0.8 collective-permute-done.5.three_ref
  131.1 1.2 copy-done
  132.4 1.0 copy-done.1
  133.4 1.7 shard_map.197
  135.1 0.0 all-to-all-done.2
  135.1 3.5 %all-to-all-start = ((bf16[8,256,128]{2,1,0:T(8,128)(2,1)}), bf16[8,256,128]{2,1,0:T(8,128)(2,1)S(1)}, u32[]{:S(2)}, u32[]{:S(2)}) async-start(bf16[8,256,128]{2,1,0:T(8,128)(2,1)} %bitcast.6), calls=%async_computation | async-start | bytes 1048576 | tf_op jit(solution)/shard_map/all_to_all | solution.py:475
  138.6 3.5 %shard_map.201 = (bf16[8,8,2048]{2,1,0:T(8,128)(2,1)}, bf16[8,8,2048]{2,1,0:T(8,128)(2,1)}) custom-call(s32[1]{0:T(128)} %bitcast.core_ref, bf16[128,2176]{1,0:T(8,128)(2,1)} %all_gather.11.tok_ref.side_ref, bf16[512,2048]{1,0:T(8,128)(2,1)} %bitcast.19), custom_call_target="tpu_custom_call" | custom-call | flops 536870912 | bytes 3145728 | tf_op jit(solution)/shard_map/pallas_call | solution.py:358
  142.1 4.9 %collective-permute-start.7 = (bf16[8,8,2048]{2,1,0:T(8,128)(2,1)}, bf16[8,8,2048]{2,1,0:T(8,128)(2,1)S(1)}, u32[]{:S(2)}, u32[]{:S(2)}) collective-permute-start(bf16[8,8,2048]{2,1,0:T(8,128)(2,1)} %get-tuple-element.19), channel_id=1, source_target_pairs={{0,1},{1,0},{2,3},{3,2},{4,5},{5,4},{6,7},{7,6},{8,9},{9,8},{10,11... | collective-permute-start | bytes 786440 | tf_op jit(solution)/shard_map/ppermute | solution.py:444
  147.0 3.5 %all-to-all-done.x_ref = bf16[8,256,128]{2,1,0:T(8,128)(2,1)S(1)} async-done(((bf16[8,256,128]{2,1,0:T(8,128)(2,1)}), bf16[8,256,128]{2,1,0:T(8,128)(2,1)S(1)}, u32[]{:S(2)}, u32[]{:S(2)}) %all-to-all-start) | async-done | bytes 524320 | tf_op jit(solution)/shard_map/all_to_all | solution.py:475
  150.5 0.8 copy-done.5
  151.3 5.5 %shard_map.198 = (f32[128,2048]{1,0:T(8,128)}, bf16[128,2048]{1,0:T(8,128)(2,1)}) custom-call(s32[1]{0:T(128)} %bitcast.core_ref, bf16[8,256,128]{2,1,0:T(8,128)(2,1)} %copy-done.5, bf16[1024,2048]{1,0:T(8,128)(2,1)} %all-gather.5.cloned.1.call-done.w_ref), custom_call_target="tpu_custom_call" | custom-call | flops 1073741824 | bytes 4194304 | tf_op jit(solution)/shard_map/pallas_call | solution.py:269
  156.8 6.5 %collective-permute-start.6 = (bf16[128,2048]{1,0:T(8,128)(2,1)}, bf16[128,2048]{1,0:T(8,128)(2,1)S(1)}, u32[]{:S(2)}, u32[]{:S(2)}) collective-permute-start(bf16[128,2048]{1,0:T(8,128)(2,1)} %get-tuple-element.17), channel_id=1, source_target_pairs={{0,1},{1,0},{2,3},{3,2},{4,5},{5,4},{6,7},{7,6},{8,9},{9,8},{10,11... | collective-permute-start | bytes 1572872 | tf_op jit(solution)/shard_map/ppermute | solution.py:444
  163.3 0.0 collective-permute-done.7
  163.3 0.0 copy-done.7
  163.3 0.1 add_convert_fusion.1
  163.4 14.8 %all_to_all.37 = bf16[8,8,2048]{2,1,0:T(8,128)(2,1)S(1)} all-to-all(bf16[8,8,2048]{2,1,0:T(8,128)(2,1)S(1)} %add_convert_fusion.1), channel_id=1, replica_groups=mesh['ep_0'=4,'ep_1'=4,'tp_0'=8,'tp_1'=2] {'tp_0'}, dimensions={0} | all-to-all | bytes 524288 | tf_op jit(solution)/shard_map/all_to_all | solution.py:480
  178.2 0.7 reduce_sum.32
  178.8 0.0 collective-permute-done.6
  178.8 0.9 add_convert_fusion
  (19 shorter events, 0.1 us)
Async XLA Ops:
  7.2 4.1 %copy-start.12 = (f32[8,2]{0,1:T(2,128)S(1)}, f32[8,2]{0,1:T(2,128)}, u32[]{:S(2)}) copy-start(f32[8,2]{0,1:T(2,128)} %param.34) | copy-start | bytes 196
  7.2 4.2 %copy-start.13 = (s32[8,2]{0,1:T(2,128)S(1)}, s32[8,2]{0,1:T(2,128)}, u32[]{:S(2)}) copy-start(s32[8,2]{0,1:T(2,128)} %param.33) | copy-start | bytes 196
  7.2 4.4 %copy-start.8 = (bf16[8,2048]{1,0:T(8,128)(2,1)S(1)}, bf16[8,2048]{1,0:T(8,128)(2,1)}, u32[]{:S(2)}) copy-start(bf16[8,2048]{1,0:T(8,128)(2,1)} %param.31) | copy-start | bytes 98308
  7.2 4.5 %copy-start.11 = (f32[2048]{0:T(1024)S(1)}, f32[2048]{0:T(1024)}, u32[]{:S(2)}) copy-start(f32[2048]{0:T(1024)} %param.32) | copy-start | bytes 24580
  7.2 88.1 %all-gather.3.cloned.1.call-start = ((), (), s32[]{:S(2)}) async-start(), calls=%async_computation.4 | async-start | bytes 8912896 | tf_op jit(solution)/shard_map/all_gather | solution.py:447
  10.5 136.4 %all-gather.5.cloned.1.call-start = ((), (), s32[]{:S(2)}) async-start(), calls=%async_computation.5 | async-start | bytes 4718592 | tf_op jit(solution)/shard_map/all_gather | solution.py:476
  83.1 3.9 %copy-start.9 = (bf16[2048,16]{0,1:T(8,128)(2,1)S(1)}, bf16[2048,16]{0,1:T(8,128)(2,1)}, u32[]{:S(2)}) copy-start(bf16[2048,16]{0,1:T(8,128)(2,1)} %param.24) | copy-start | bytes 196612
  83.1 4.9 %copy-start.10 = (bf16[2048,16]{0,1:T(8,128)(2,1)S(1)}, bf16[2048,16]{0,1:T(8,128)(2,1)}, u32[]{:S(2)}) copy-start(bf16[2048,16]{0,1:T(8,128)(2,1)} %param.25) | copy-start | bytes 196612
  83.1 52.0 %all-to-all-start.2 = ((bf16[16,32,2048]{2,1,0:T(8,128)(2,1)}), bf16[16,32,2048]{2,1,0:T(8,128)(2,1)S(1)}, u32[]{:S(2)}, u32[]{:S(2)}) async-start(bf16[16,32,2048]{2,1,0:T(8,128)(2,1)} %bitcast.21), calls=%async_computation.2 | async-start | bytes 4194304 | tf_op jit(solution)/shard_map/all_to_all | solution.py:461
  95.3 35.9 %copy-start.3 = (f32[128]{0:T(128)S(1)}, f32[128]{0:T(128)}, u32[]{:S(2)}) copy-start(f32[128]{0:T(128)} %param.29) | copy-start | bytes 1540
  115.6 4.9 %collective-permute-start = (bf16[128,256]{1,0:T(8,128)(2,1)}, bf16[128,256]{1,0:T(8,128)(2,1)S(1)}, u32[]{:S(2)}, u32[]{:S(2)}) collective-permute-start(bf16[128,256]{1,0:T(8,128)(2,1)} %get-tuple-element.11.own_ref), channel_id=1, source_target_pairs={{0,16},{16,32},{32,48},{48,0},{1,17},{17,33},{33,49},{49,1},{2,18}... | collective-permute-start | bytes 196616 | tf_op jit(solution)/shard_map/ppermute | solution.py:416
  116.8 5.0 %collective-permute-start.1 = (bf16[128,256]{1,0:T(8,128)(2,1)}, bf16[128,256]{1,0:T(8,128)(2,1)S(1)}, u32[]{:S(2)}, u32[]{:S(2)}) collective-permute-start(bf16[128,256]{1,0:T(8,128)(2,1)} %get-tuple-element.11.own_ref), channel_id=1, source_target_pairs={{0,32},{16,48},{32,0},{48,16},{1,33},{17,49},{33,1},{49,17},{2,34}... | collective-permute-start | bytes 196616 | tf_op jit(solution)/shard_map/ppermute | solution.py:416
  119.2 3.9 %collective-permute-start.2 = (bf16[128,256]{1,0:T(8,128)(2,1)}, bf16[128,256]{1,0:T(8,128)(2,1)S(1)}, u32[]{:S(2)}, u32[]{:S(2)}) collective-permute-start(bf16[128,256]{1,0:T(8,128)(2,1)} %get-tuple-element.11.own_ref), channel_id=1, source_target_pairs={{0,48},{16,0},{32,16},{48,32},{1,49},{17,1},{33,17},{49,33},{2,50}... | collective-permute-start | bytes 196616 | tf_op jit(solution)/shard_map/ppermute | solution.py:416
  123.2 0.8 copy-start.2
  124.5 4.7 %collective-permute-start.3 = (bf16[128,256]{1,0:T(8,128)(2,1)S(1)}, bf16[128,256]{1,0:T(8,128)(2,1)S(1)}, u32[]{:S(2)}, u32[]{:S(2)}) collective-permute-start(bf16[128,256]{1,0:T(8,128)(2,1)S(1)} %get-tuple-element.12), channel_id=1, source_target_pairs={{0,64},{64,128},{128,192},{192,0},{1,65},{65,129},{129,193},{193,1... | collective-permute-start | bytes 196616 | tf_op jit(solution)/shard_map/ppermute | solution.py:416
  125.6 4.8 %collective-permute-start.4 = (bf16[128,256]{1,0:T(8,128)(2,1)S(1)}, bf16[128,256]{1,0:T(8,128)(2,1)S(1)}, u32[]{:S(2)}, u32[]{:S(2)}) collective-permute-start(bf16[128,256]{1,0:T(8,128)(2,1)S(1)} %get-tuple-element.12), channel_id=1, source_target_pairs={{0,128},{64,192},{128,0},{192,64},{1,129},{65,193},{129,1},{193,65... | collective-permute-start | bytes 196616 | tf_op jit(solution)/shard_map/ppermute | solution.py:416
  128.0 3.1 %collective-permute-start.5 = (bf16[128,256]{1,0:T(8,128)(2,1)S(1)}, bf16[128,256]{1,0:T(8,128)(2,1)S(1)}, u32[]{:S(2)}, u32[]{:S(2)}) collective-permute-start(bf16[128,256]{1,0:T(8,128)(2,1)S(1)} %get-tuple-element.12), channel_id=1, source_target_pairs={{0,192},{64,0},{128,64},{192,128},{1,193},{65,1},{129,65},{193,129... | collective-permute-start | bytes 196616 | tf_op jit(solution)/shard_map/ppermute | solution.py:416
  131.1 1.2 copy-start
  132.4 1.0 copy-start.1
  135.1 3.5 %copy-start.4 = (bf16[16,32,2048]{2,1,0:T(8,128)(2,1)}, bf16[16,32,2048]{2,1,0:T(8,128)(2,1)S(1)}, u32[]{:S(2)}) copy-start(bf16[16,32,2048]{2,1,0:T(8,128)(2,1)S(1)} %all-to-all-done.2) | copy-start | bytes 6291460
  135.1 15.3 %all-to-all-start = ((bf16[8,256,128]{2,1,0:T(8,128)(2,1)}), bf16[8,256,128]{2,1,0:T(8,128)(2,1)S(1)}, u32[]{:S(2)}, u32[]{:S(2)}) async-start(bf16[8,256,128]{2,1,0:T(8,128)(2,1)} %bitcast.6), calls=%async_computation | async-start | bytes 1048576 | tf_op jit(solution)/shard_map/all_to_all | solution.py:475
  142.1 21.2 %copy-start.7 = (bf16[8,8,2048]{2,1,0:T(8,128)(2,1)S(1)}, bf16[8,8,2048]{2,1,0:T(8,128)(2,1)}, u32[]{:S(2)}) copy-start(bf16[8,8,2048]{2,1,0:T(8,128)(2,1)} %get-tuple-element.18) | copy-start | bytes 786436
  142.1 21.2 %collective-permute-start.7 = (bf16[8,8,2048]{2,1,0:T(8,128)(2,1)}, bf16[8,8,2048]{2,1,0:T(8,128)(2,1)S(1)}, u32[]{:S(2)}, u32[]{:S(2)}) collective-permute-start(bf16[8,8,2048]{2,1,0:T(8,128)(2,1)} %get-tuple-element.19), channel_id=1, source_target_pairs={{0,1},{1,0},{2,3},{3,2},{4,5},{5,4},{6,7},{7,6},{8,9},{9,8},{10,11... | collective-permute-start | bytes 786440 | tf_op jit(solution)/shard_map/ppermute | solution.py:444
  150.5 0.8 copy-start.5
  156.8 22.1 %copy-start.6 = (f32[128,2048]{1,0:T(8,128)S(1)}, f32[128,2048]{1,0:T(8,128)}, u32[]{:S(2)}) copy-start(f32[128,2048]{1,0:T(8,128)} %get-tuple-element.16) | copy-start | bytes 3145732
  156.8 22.1 %collective-permute-start.6 = (bf16[128,2048]{1,0:T(8,128)(2,1)}, bf16[128,2048]{1,0:T(8,128)(2,1)S(1)}, u32[]{:S(2)}, u32[]{:S(2)}) collective-permute-start(bf16[128,2048]{1,0:T(8,128)(2,1)} %get-tuple-element.17), channel_id=1, source_target_pairs={{0,1},{1,0},{2,3},{3,2},{4,5},{5,4},{6,7},{7,6},{8,9},{9,8},{10,11... | collective-permute-start | bytes 1572872 | tf_op jit(solution)/shard_map/ppermute | solution.py:444
Sparse Core Ops, SparseCore 0:
  10.7 61.1 all-gather.2
  73.6 52.6 all-gather.4
where the time goes:
time: 187 us
  blocking collectives  75.4 us (40%)
  Pallas kernels  46.5 us (25%)
  starting transfers between devices  28.3 us (15%)
  between operations  15.5 us (8%)
  waiting for transfers between devices  8.94 us (5%)
  local copies, waits for them, and re-layouts  6.17 us (3%)
  other arithmetic  5.79 us (3%)
    all_to_all x1, blocking collectives, mixed_step(): lax.all_to_all(packed, EP, split_axis=0, concat_axis=0, tiled=True)  34.6 us
    all_gather x1, blocking collectives, mixed_step(): lax.all_gather(jnp.concatenate([exp_normed, side], axis=1), TP, axis=0, t...  26 us
    pallas_call x1, Pallas kernels, span_terms(): pl.pallas_call(functools.partial(span_kernel, count), grid=(blocks // cou...  20.3 us
    all_to_all x1, blocking collectives, mixed_step(): lax.all_to_all(pair, 'tp_0', split_axis=0, concat_axis=0, tiled=True)  14.8 us
    ppermute x2, starting transfers between devices, mixed_step(): cross = lambda x: lax.ppermute(x, 'tp_1', [(0, 1), (1, 0)])  11.4 us
    ppermute x6, starting transfers between devices, around(): lax.ppermute(x, axis, [(i, (i + k) % size) for i in range(size)])  9.51 us
    pallas_call x1, Pallas kernels, expert_sums(): pl.pallas_call(expert_kernel, out_shape=jax.ShapeDtypeStruct((count, widt...  7.41 us
    unnamed x31, local copies, waits for them, and re-layouts  6.07 us
  transfers between devices with their start and end apart: 12, of which 6 were waited for; matrix products, arithmetic and copies ran while one was open for 2% of the time, Pallas kernels for 25%

commit v1 on v0

--- a/solution.py
+++ b/solution.py
@@ -217,70 +217,78 @@
     )(here, own, one, two, three)
 
 
-def apply_kernel(here_ref, one_ref, two_ref, three_ref, before_ref, g_ref, h_ref, gain_ref, out_ref, slots):
-    here = here_ref[0]
-    slots[(here + 3) % 4] = one_ref[...]
-    slots[(here + 2) % 4] = two_ref[...]
-    slots[(here + 1) % 4] = three_ref[...]
-    memory = jnp.where(here > 0, slots[0][:, HEAD:].astype(F32), 0.0)
-    for k in range(1, 3):
-        piece = slots[k]
-        moved = mm(piece[:, :HEAD], memory) + piece[:, HEAD:].astype(F32)
-        memory = jnp.where(here > k, moved, memory)
-    memory = mm(before_ref[:, :HEAD], memory) + before_ref[:, HEAD:]
-    heads_out = mm(g_ref[...], memory) + h_ref[...]
+def apply_kernel(here_ref, one_ref, two_ref, three_ref, before_ref, g_ref, h_ref, gain_ref, out_ref, slots, entering):
+    @pl.when(pl.program_id(0) == 0)
+    def _():
+        here = here_ref[0]
+        slots[(here + 3) % 4] = one_ref[...]
+        slots[(here + 2) % 4] = two_ref[...]
+        slots[(here + 1) % 4] = three_ref[...]
+        memory = jnp.where(here > 0, slots[0][:, HEAD:].astype(F32), 0.0)
+        for k in range(1, 3):
+            piece = slots[k]
+            moved = mm(piece[:, :HEAD], memory) + piece[:, HEAD:].astype(F32)
+            memory = jnp.where(here > k, moved, memory)
+        entering[...] = mm(before_ref[:, :HEAD], memory) + before_ref[:, HEAD:]
+
+    heads_out = mm(g_ref[...], entering[...]) + h_ref[...]
     scale = lax.rsqrt(jnp.mean(heads_out * heads_out, axis=1, keepdims=True) + norm_eps)
     out_ref[...] = (heads_out * scale * gain_ref[...]).astype(BF16)
 
 
 def apply_memory(here, one, two, three, before, g, h, gain):
-    vmem = pl.BlockSpec(memory_space=pltpu.VMEM)
+    rows = h.shape[0]
+    step = rows // 4
+    whole = lambda i: (0, 0)
+    tall = lambda i: (i, 0)
+    piece = pl.BlockSpec((HEAD, 2 * HEAD), whole)
     return pl.pallas_call(
         apply_kernel,
+        grid=(4,),
         out_shape=jax.ShapeDtypeStruct(h.shape, BF16),
-        in_specs=[pl.BlockSpec(memory_space=pltpu.SMEM)] + [vmem] * 7,
-        out_specs=vmem,
-        scratch_shapes=[pltpu.VMEM((4, HEAD, 2 * HEAD), BF16)],
-        compiler_params=pltpu.CompilerParams(vmem_limit_bytes=8 * 1024 * 1024),
+        in_specs=[pl.BlockSpec(memory_space=pltpu.SMEM)]
+        + [piece] * 4
+        + [pl.BlockSpec((step, HEAD), tall), pl.BlockSpec((step, HEAD), tall), pl.BlockSpec((1, HEAD), whole)],
+        out_specs=pl.BlockSpec((step, HEAD), tall),
+        scratch_shapes=[pltpu.VMEM((4, HEAD, 2 * HEAD), BF16), pltpu.VMEM((HEAD, HEAD), F32)],
         cost_estimate=pl.CostEstimate(flops=h.size * 2 * HEAD, bytes_accessed=h.size * 8, transcendentals=0),
     )(here, one, two, three, before, g, h, gain.reshape(1, HEAD))
 
 
-def output_kernel(core_ref, x_ref, w_ref, mine_ref, theirs_ref, total):
-    step = pl.program_id(0)
-
-    @pl.when(step == 0)
+def output_kernel(core_ref, x_ref, w_ref, mine_ref, theirs_ref, rows):
+    @pl.when(pl.program_id(0) == 0)
     def _():
-        total[...] = jnp.zeros_like(total)
-
-    rows = jnp.concatenate([x_ref[0], x_ref[1]], axis=1)
-    total[...] += mm(rows, w_ref[...])
-
-    @pl.when(step == pl.num_programs(0) - 1)
-    def _():
-        first = core_ref[0] == 0
-        mine_ref[...] = jnp.where(first, total[:BLOCK], total[BLOCK:])
-        theirs_ref[...] = jnp.where(first, total[BLOCK:], total[:BLOCK]).astype(BF16)
+        for part in range(2):
+            owner = core_ref[0] if part == 0 else 1 - core_ref[0]
+            at = pl.ds(pl.multiple_of(owner * BLOCK, BLOCK), BLOCK)
+            for h in range(x_ref.shape[0]):
+                rows[part * BLOCK : (part + 1) * BLOCK, h * HEAD : (h + 1) * HEAD] = x_ref[h, at, :]
+
+    out = mm(rows[...], w_ref[...])
+    mine_ref[...] = out[:BLOCK]
+    theirs_ref[...] = out[BLOCK:].astype(BF16)
 
 
 def output_product(core, by_head, weights):
     depth, width = weights.shape
-    whole = lambda i: (0, 0)
+    heads = depth // HEAD
+    step = width // 4
+    column = lambda i: (0, i)
     return pl.pallas_call(
         output_kernel,
-        grid=(depth // (2 * HEAD),),
+        grid=(4,),
         out_shape=(jax.ShapeDtypeStruct((BLOCK, width), F32), jax.ShapeDtypeStruct((BLOCK, width), BF16)),
         in_specs=[
             pl.BlockSpec(memory_space=pltpu.SMEM),
-            pl.BlockSpec((2, 2 * BLOCK, HEAD), lambda i: (i, 0, 0)),
-            pl.BlockSpec((2 * HEAD, width), lambda i: (i, 0)),
+            pl.BlockSpec((heads, 2 * BLOCK, HEAD), lambda i: (0, 0, 0)),
+            pl.BlockSpec((depth, step), column),
         ],
-        out_specs=(pl.BlockSpec((BLOCK, width), whole), pl.BlockSpec((BLOCK, width), whole)),
-        scratch_shapes=[pltpu.VMEM((2 * BLOCK, width), F32)],
+        out_specs=(pl.BlockSpec((BLOCK, step), column), pl.BlockSpec((BLOCK, step), column)),
+        scratch_shapes=[pltpu.VMEM((2 * BLOCK, depth), BF16)],
         cost_estimate=pl.CostEstimate(
             flops=4 * BLOCK * depth * width, bytes_accessed=2 * depth * width, transcendentals=0
         ),
-    )(core, by_head.reshape(-1, 2 * BLOCK, HEAD), weights)
+    )(core, by_head.reshape(heads, 2 * BLOCK, HEAD), weights)
 
 
 def route_columns(side, experts):
@@ -327,7 +335,7 @@
     )(tokens)
 
 
-def combine_kernel(experts, core_ref, side_ref, back_ref, mine_ref, theirs_ref, total):
+def combine_kernel(experts, side_ref, back_ref, out_ref):
     side = side_ref[...].astype(F32).T
     first, named, slots = route_columns(side, experts)
     share = [side[2 + k : 3 + k] + side[4 + k : 5 + k] + side[6 + k : 7 + k] for k in range(2)]
@@ -340,73 +348,71 @@
     low = (pick - high.astype(F32)).astype(BF16)
     back = back_ref[...]
     out = mm(high, back, TN) + mm(low, back, TN)
-    total[...] = out.reshape(total.shape)
-    core = core_ref[0]
-    for z in range(mine_ref.shape[0]):
-        mine_ref[z] = total[2 * z + core].astype(BF16)
-        theirs_ref[z] = total[2 * z + 1 - core].astype(BF16)
-
-
-def combine_tokens(core, tokens, back, experts):
+    out_ref[...] = out.reshape(out_ref.shape).astype(BF16)
+
+
+def combine_tokens(tokens, back, experts):
     count, _ = tokens.shape
     width = back.shape[1]
-    devices = count // TOKENS
-    whole = lambda i: (0, 0)
-    cube = lambda i: (0, 0, 0)
-    half = (devices // 2, TOKENS, width)
-    out = jax.ShapeDtypeStruct(half, BF16)
+    shape = (count // TOKENS, TOKENS, width)
     return pl.pallas_call(
         functools.partial(combine_kernel, experts),
         grid=(1,),
-        out_shape=(out, out),
+        out_shape=jax.ShapeDtypeStruct(shape, BF16),
         in_specs=[
-            pl.BlockSpec(memory_space=pltpu.SMEM),
             pl.BlockSpec((count, HEAD), lambda i: (0, width // HEAD)),
-            pl.BlockSpec(back.shape, whole),
+            pl.BlockSpec(back.shape, lambda i: (0, 0)),
         ],
-        out_specs=(pl.BlockSpec(half, cube), pl.BlockSpec(half, cube)),
-        scratch_shapes=[pltpu.VMEM((devices, TOKENS, width), F32)],
+        out_specs=pl.BlockSpec(shape, lambda i: (0, 0, 0)),
         cost_estimate=pl.CostEstimate(
-            flops=4 * count * back.size, bytes_accessed=2 * back.size + 4 * count * width, transcendentals=0
+            flops=4 * count * back.size, bytes_accessed=2 * back.size + 2 * count * width, transcendentals=0
         ),
-    )(core, tokens, back)
-
-
-def expert_kernel(rows_ref, gate_ref, up_ref, down_ref, out_ref, rows, gate, up, down, sems):
-    copies = [
-        pltpu.make_async_copy(src, dst, sems.at[i])
-        for i, (src, dst) in enumerate(((rows_ref, rows), (gate_ref, gate), (up_ref, up), (down_ref, down)))
-    ]
+    )(tokens, back)
+
+
+def expert_kernel(own_ref, other_ref, gate_ref, up_ref, down_ref, mine_ref, theirs_ref, rows, gate, up, down, sems):
+    half = own_ref.shape[0]
+    pairs = (
+        (own_ref, rows.at[pl.ds(0, half)]),
+        (other_ref, rows.at[pl.ds(half, half)]),
+        (gate_ref, gate),
+        (up_ref, up),
+        (down_ref, down),
+    )
+    copies = [pltpu.make_async_copy(src, dst, sems.at[i]) for i, (src, dst) in enumerate(pairs)]
     for copy in copies:
         copy.start()
-    copies[0].wait()
-    copies[1].wait()
+    for copy in copies[:3]:
+        copy.wait()
     gated = silu(mm(rows[...], gate[...], NT))
-    copies[2].wait()
+    copies[3].wait()
     hidden = (gated * mm(rows[...], up[...], NT)).astype(BF16)
-    copies[3].wait()
-    out_ref[...] = mm(hidden, down[...]).astype(BF16)
-
-
-def expert_sums(rows, gate, up, down):
-    count, width = rows.shape
+    copies[4].wait()
+    theirs_ref[...] = mm(hidden[half:], down[...]).astype(BF16)
+    mine_ref[...] = mm(hidden[:half], down[...]).astype(BF16)
+
+
+def expert_sums(own, other, gate, up, down):
+    half, width = own.shape
     units = gate.shape[0]
+    out = jax.ShapeDtypeStruct((half, width), BF16)
+    vmem = pl.BlockSpec(memory_space=pltpu.VMEM)
     return pl.pallas_call(
         expert_kernel,
-        out_shape=jax.ShapeDtypeStruct((count, width), BF16),
-        in_specs=[pl.BlockSpec(memory_space=pl.ANY)] * 4,
-        out_specs=pl.BlockSpec(memory_space=pltpu.VMEM),
+        out_shape=(out, out),
+        in_specs=[pl.BlockSpec(memory_space=pl.ANY)] * 5,
+        out_specs=(vmem, vmem),
         scratch_shapes=[
-            pltpu.VMEM((count, width), BF16),
+            pltpu.VMEM((2 * half, width), BF16),
             pltpu.VMEM((units, width), BF16),
             pltpu.VMEM((units, width), BF16),
             pltpu.VMEM((units, width), BF16),
-            pltpu.SemaphoreType.DMA((4,)),
+            pltpu.SemaphoreType.DMA((5,)),
         ],
         cost_estimate=pl.CostEstimate(
-            flops=6 * count * width * units, bytes_accessed=6 * units * width + 4 * count * width, transcendentals=0
+            flops=12 * half * width * units, bytes_accessed=6 * units * width + 8 * half * width, transcendentals=0
         ),
-    )(rows, gate, up, down)
+    )(own, other, gate, up, down)
 
 
 def around(x, axis):
@@ -454,14 +460,14 @@
         rest = rest - part
     side = jnp.concatenate([routes.astype(BF16)] + parts, axis=1)
     side = jnp.pad(side, ((0, 0), (0, HEAD - side.shape[1])))
-    tokens = lax.all_gather(jnp.concatenate([exp_normed, side], axis=1), TP, axis=0, tiled=True)
+    tokens = lax.all_gather(jnp.concatenate([exp_normed, side], axis=1), "tp_0", axis=0, tiled=True)
     packed = pack_tokens(tokens, experts)
     exp_rows = lax.all_to_all(packed, EP, split_axis=0, concat_axis=0, tiled=True)
-    partial = expert_sums(exp_rows, gate_weight[0].T, up_weight[0].T, down_weight[0])
-    back = lax.all_to_all(partial, EP, split_axis=0, concat_axis=0, tiled=True)
-    mine, theirs = combine_tokens(core[None], tokens, back, experts)
-    crossed = cross(theirs)
-    pair = (mine.astype(F32) + crossed.astype(F32)).astype(BF16)
+    other_rows = cross(exp_rows)
+    mine, theirs = expert_sums(exp_rows, other_rows, gate_weight[0].T, up_weight[0].T, down_weight[0])
+    pair = (mine.astype(F32) + cross(theirs).astype(F32)).astype(BF16)
+    back = lax.all_to_all(pair, EP, split_axis=0, concat_axis=0, tiled=True)
+    combined = combine_tokens(tokens, back, experts)
 
     weights = join_weights(
         head[None], query_weight, key_weight, value_weight, write_strength_projection, decay_projection
@@ -469,7 +475,8 @@
     scal = jnp.concatenate([head_decay_speed, largest_write_strength])
     extra = extra_log_decay.reshape(-1, BLOCK)
     gains, local, span = span_terms(scal, mix_rows, weights, extra, 8)
-    before, total = compose_row(lax.axis_index("ep_1")[None], span, *around(span, "ep_1"))
+    row_pieces = around(span, "ep_1")
+    before, total = compose_row(lax.axis_index("ep_1")[None], span, *row_pieces)
     mixed = apply_memory(lax.axis_index("ep_0")[None], *around(total, "ep_0"), before, gains, local, head_norm_gain)
 
     by_head = lax.all_to_all(mixed, "tp_0", split_axis=0, concat_axis=0, tiled=True)
@@ -477,7 +484,7 @@
     mix_mine, mix_theirs = output_product(core[None], by_head, w_own)
     mix_out = (mix_mine + cross(mix_theirs).astype(F32)).astype(BF16)
 
-    pieces = lax.all_to_all(pair, "tp_0", split_axis=0, concat_axis=0, tiled=True)
+    pieces = lax.all_to_all(combined, "tp_0", split_axis=0, concat_axis=0, tiled=True)
     exp_out = jnp.sum(pieces.astype(F32), axis=0).astype(BF16)
     return (mix_out, exp_out)
 

time: 187 us -> 193 us (1.032); the launches traced: 187 us -> 190 us
  waiting for transfers between devices: 8.94 us -> 25.6 us
  blocking collectives: 75.4 us -> 60.3 us
    all_to_all x1, blocking collectives: 34.6 us -> 18.7 us  [mixed_step(): lax.all_to_all(packed, EP, split_axis=0, concat_axis=0, tiled=True)]
    all_to_all x1, waiting for transfers between devices: 3.5 us -> 13.5 us  [mixed_step(): lax.all_to_all(mixed, 'tp_0', split_axis=0, concat_axis=0, tiled=True)]
    all_to_all x1, waiting for transfers between devices: 0.01 us -> 4.77 us  [mixed_step(): back = lax.all_to_all(pair, EP, split_axis=0, concat_axis=0, tiled=True)]
    ppermute x6, starting transfers between devices: 9.51 us -> 5.84 us  [around(): lax.ppermute(x, axis, [(i, (i + k) % size) for i in range(size)])]
    pallas_call x3, Pallas kernels: 14.6 us -> 16.9 us  [the longest x1 7.14 us: expert_sums(): pl.pallas_call(expert_kernel, out_shape=(out, out), in_specs=[pl.BlockSpe...]
    all_to_all x1, starting transfers between devices: 3.86 us -> 6.01 us  [mixed_step(): back = lax.all_to_all(pair, EP, split_axis=0, concat_axis=0, tiled=True)]
    ppermute x2 -> x3, starting transfers between devices: 11.4 us -> 10.7 us  [mixed_step(): cross = lambda x: lax.ppermute(x, 'tp_1', [(0, 1), (1, 0)])]
    unnamed x31 -> x37, local copies, waits for them, and re-layouts: 6.07 us -> 6.22 us
  transfers between devices with their start and end apart: 12 -> 13, of which waited for: 6 -> 7; matrix products, arithmetic and copies ran while one was open for 2% -> 3% of each run, Pallas kernels for 25% -> 25%
where the time goes in v1:
time: 193 us; the launch traced here: 190 us
  blocking collectives  60.3 us (31%)
  Pallas kernels  47.3 us (25%)
  starting transfers between devices  27.8 us (14%)
  waiting for transfers between devices  25.6 us (13%)
  between operations  15.5 us (8%)
  other arithmetic  7.11 us (4%)
  local copies, waits for them, and re-layouts  6.32 us (3%)
    all_gather x1, blocking collectives, mixed_step(): lax.all_gather(jnp.concatenate([exp_normed, side], axis=1), 'tp_0', axis=...  27.3 us
    pallas_call x1, Pallas kernels, span_terms(): pl.pallas_call(functools.partial(span_kernel, count), grid=(blocks // cou...  20.3 us
    all_to_all x1, blocking collectives, mixed_step(): lax.all_to_all(packed, EP, split_axis=0, concat_axis=0, tiled=True)  18.7 us
    all_to_all x1, blocking collectives, mixed_step(): lax.all_to_all(combined, 'tp_0', split_axis=0, concat_axis=0, tiled=True)  14.3 us
    all_to_all x1, waiting for transfers between devices, mixed_step(): lax.all_to_all(mixed, 'tp_0', split_axis=0, concat_axis=0, tiled=True)  13.5 us
    ppermute x3, starting transfers between devices, mixed_step(): cross = lambda x: lax.ppermute(x, 'tp_1', [(0, 1), (1, 0)])  10.7 us
    pallas_call x1, Pallas kernels, expert_sums(): pl.pallas_call(expert_kernel, out_shape=(out, out), in_specs=[pl.BlockSpe...  7.14 us
    ppermute x6, waiting for transfers between devices, around(): lax.ppermute(x, axis, [(i, (i + k) % size) for i in range(size)])  6.63 us
  transfers between devices with their start and end apart: 13, of which 7 were waited for; matrix products, arithmetic and copies ran while one was open for 3% of the time, Pallas kernels for 25%

profile of v1, /device:TPU:1, one launch (start us, length us, event | category | flops | bytes accessed | tf_op | source)
XLA Modules:
  0.0 190.0 jit_solution(8870960557372389582)
XLA Ops:
  7.2 0.0 copy-start.14
  7.2 0.0 all-gather.3.cloned.1.call-start
  7.3 1.2 fusion
  8.5 2.0 %fusion.2 = bf16[128,2048]{1,0:T(8,128)(2,1)} fusion(bf16[128,2048]{1,0:T(8,128)(2,1)} %param.19, f32[2048]{0:T(1024)} %param.20, f32[128]{0:T(128)S(1)} %add_rsqrt_fusion.1), kind=kLoop, calls=%fused_computation.5 | loop fusion | flops 1048576 | bytes 1057280 | tf_op jit(solution)/shard_map/convert_element_type | solution.py:40
  10.5 0.0 all-gather.3.cloned.1.call-update
  10.5 0.0 all-gather.5.cloned.1.call-start
  10.6 0.7 all-gather.5.cloned.1.call-update
  11.3 0.0 copy-start.8
  11.3 0.1 copy.28
  11.4 0.0 copy-done.16
  11.4 0.1 copy.30
  11.5 0.1 fusion.14
  11.6 0.0 copy-done.7
  11.6 0.1 fusion.3
  11.7 0.1 fusion.5
  11.8 0.0 copy-start.9
  11.8 27.3 %all_gather.11.tok_ref.side_ref = bf16[64,2176]{1,0:T(8,128)(2,1)} all-gather(bf16[8,2176]{1,0:T(8,128)(2,1)S(1)} %pad_maximum_fusion), channel_id=1, replica_groups=mesh['ep_0'=4,'ep_1'=4,'tp_0'=8,'tp_1'=2] {'tp_0'}, dimensions={0}, use_global_device_ids=true | all-gather | bytes 313344 | tf_op jit(solution)/shard_map/all_gather | solution.py:463
  39.2 2.6 %shard_map.199 = bf16[256,2048]{1,0:T(8,128)(2,1)} custom-call(bf16[64,2176]{1,0:T(8,128)(2,1)} %all_gather.11.tok_ref.side_ref), custom_call_target="tpu_custom_call" | custom-call | flops 71303168 | bytes 1114112 | tf_op jit(solution)/shard_map/pallas_call | solution.py:329
  41.8 18.7 %all_to_all.36 = bf16[16,16,2048]{2,1,0:T(8,128)(2,1)S(1)} all-to-all(bf16[16,16,2048]{2,1,0:T(8,128)(2,1)} %bitcast.19), channel_id=1, replica_groups=mesh['ep_0'=4,'ep_1'=4,'tp_0'=8,'tp_1'=2] {'ep_0','ep_1'}, dimensions={0} | all-to-all | bytes 2097152 | tf_op jit(solution)/shard_map/all_to_all | solution.py:465
  60.5 6.9 %collective-permute-start.7 = (bf16[256,2048]{1,0:T(8,128)(2,1)S(1)}, bf16[256,2048]{1,0:T(8,128)(2,1)S(1)}, u32[]{:S(2)}, u32[]{:S(2)}) collective-permute-start(bf16[256,2048]{1,0:T(8,128)(2,1)S(1)} %bitcast.21), channel_id=1, source_target_pairs={{0,1},{1,0},{2,3},{3,2},{4,5},{5,4},{6,7},{7,6},{8,9},{9,8},{10,11... | collective-permute-start | bytes 3145736 | tf_op jit(solution)/shard_map/ppermute | solution.py:450
  67.4 1.0 copy.26.strength_ref
  68.4 0.0 copy-done.9
  68.4 1.0 copy.27.decay_ref
  70.7 4.4 %shard_map.194.w_ref = bf16[2048,512]{1,0:T(8,128)(2,1)} custom-call(s32[1]{0:T(128)} %bitcast.3.head_ref, bf16[2048,128]{1,0:T(8,128)(2,1)} %q_ref.1, bf16[2048,128]{1,0:T(8,128)(2,1)} %k_ref.1, bf16[2048,128]{1,0:T(8,128)(2,1)} %v_ref.1, bf16[2048,16]{1,0:T(8,128)(2,1)} %copy.26.strength_ref, bf16[2048,16]{1,0:T(8,128)(2,1)} %copy.27.decay_ref), custom_call_target="tpu_custom_call" | custom-call | flops 100000000 | bytes 4194304 | tf_op jit(solution)/shard_map/pallas_call | solution.py:78
  75.1 0.6 pad_maximum_fusion.1.scal_ref
  75.7 0.0 collective-permute-done.7.other_ref
  75.7 1.0 copy-done.15
  76.7 7.1 %shard_map.200 = (bf16[256,2048]{1,0:T(8,128)(2,1)}, bf16[256,2048]{1,0:T(8,128)(2,1)}) custom-call(bf16[256,2048]{1,0:T(8,128)(2,1)} %bitcast.22, bf16[256,2048]{1,0:T(8,128)(2,1)} %copy-done.15, bf16[448,2048]{1,0:T(8,128)(2,1)} %bitcast.24, bf16[448,2048]{1,0:T(8,128)(2,1)} %bitcast.25, bf16[448,2048]{1,0:T(8,128)(2,1)} %bitcast.26), custom_call_target="tpu_custom_call" | custom-call | flops 2818572288 | bytes 9699328 | tf_op jit(solution)/shard_map/pallas_call | solution.py:400
  83.9 0.2 collective-permute-start.8
  84.1 20.3 %shard_map.195 = (bf16[2048,128]{1,0:T(8,128)(2,1)}, f32[2048,128]{1,0:T(8,128)}, bf16[128,256]{1,0:T(8,128)(2,1)}) custom-call(f32[2]{0:T(128)} %pad_maximum_fusion.1.scal_ref, bf16[2048,2048]{1,0:T(8,128)(2,1)} %all-gather.3.cloned.1.call-done.rows_ref, bf16[2048,512]{1,0:T(8,128)(2,1)} %shard_map.194.w_ref, f32[16,128]{1,0:T(8,128)} %bitcast.27), custom_call_target="tpu_custom_call" | custom-call | flops 15032385536 | bytes 12058624 | tf_op jit(solution)/shard_map/pallas_call | solution.py:153
  104.4 0.5 collective-permute-start
  104.9 1.1 collective-permute-start.1
  106.0 1.3 collective-permute-start.2
  107.4 2.0 %collective-permute-done.one_ref = bf16[128,256]{1,0:T(8,128)(2,1)S(1)} collective-permute-done((bf16[128,256]{1,0:T(8,128)(2,1)}, bf16[128,256]{1,0:T(8,128)(2,1)S(1)}, u32[]{:S(2)}, u32[]{:S(2)}) %collective-permute-start) | collective-permute-done | bytes 65568 | tf_op jit(solution)/shard_map/ppermute | solution.py:422
  109.3 0.5 collective-permute-done.1.two_ref
  109.8 1.1 collective-permute-done.2.three_ref
  110.9 0.8 copy-done.1
  111.7 0.5 shard_map.196
  112.2 0.6 copy-done
  112.9 0.0 collective-permute-start.3
  112.9 2.0 %collective-permute-start.4 = (bf16[128,256]{1,0:T(8,128)(2,1)S(1)}, bf16[128,256]{1,0:T(8,128)(2,1)S(1)}, u32[]{:S(2)}, u32[]{:S(2)}) collective-permute-start(bf16[128,256]{1,0:T(8,128)(2,1)S(1)} %get-tuple-element.12), channel_id=1, source_target_pairs={{0,128},{64,192},{128,0},{192,64},{1,129},{65,193},{129,1},{193,65... | collective-permute-start | bytes 196616 | tf_op jit(solution)/shard_map/ppermute | solution.py:422
  114.9 0.8 collective-permute-start.5
  115.7 2.6 %collective-permute-done.3.one_ref = bf16[128,256]{1,0:T(8,128)(2,1)S(1)} collective-permute-done((bf16[128,256]{1,0:T(8,128)(2,1)S(1)}, bf16[128,256]{1,0:T(8,128)(2,1)S(1)}, u32[]{:S(2)}, u32[]{:S(2)}) %collective-permute-start.3) | collective-permute-done | bytes 65568 | tf_op jit(solution)/shard_map/ppermute | solution.py:422
  118.3 0.0 collective-permute-done.4.two_ref
  118.3 0.6 collective-permute-done.5.three_ref
  118.9 0.0 copy-done.10
  118.9 0.0 copy-done.11
  118.9 0.5 copy-done.12
  119.5 4.5 %shard_map.197 = bf16[2048,128]{1,0:T(8,128)(2,1)} custom-call(s32[1]{0:T(128)} %bitcast.1.here_ref, bf16[128,256]{1,0:T(8,128)(2,1)} %copy-done.10, bf16[128,256]{1,0:T(8,128)(2,1)} %copy-done.11, bf16[128,256]{1,0:T(8,128)(2,1)} %copy-done.12, f32[128,256]{1,0:T(8,128)} %copy-done, bf16[2048,128]{1,0:T(8,128)(2,1)} %get-tuple-element.14.g_ref, ...), custom_call_target="tpu_custom_call" | custom-call | flops 67108864 | bytes 2097152 | tf_op jit(solution)/shard_map/pallas_call | solution.py:245
  124.0 5.1 %all-to-all-start = ((bf16[8,256,128]{2,1,0:T(8,128)(2,1)}), bf16[8,256,128]{2,1,0:T(8,128)(2,1)S(1)}, u32[]{:S(2)}, u32[]{:S(2)}) async-start(bf16[8,256,128]{2,1,0:T(8,128)(2,1)} %bitcast.20), calls=%async_computation | async-start | bytes 1048576 | tf_op jit(solution)/shard_map/all_to_all | solution.py:482
  129.1 0.0 collective-permute-done.8
  129.1 1.4 add_convert_fusion
  130.5 13.5 %all-to-all-done.x_ref = bf16[8,256,128]{2,1,0:T(8,128)(2,1)S(1)} async-done(((bf16[8,256,128]{2,1,0:T(8,128)(2,1)}), bf16[8,256,128]{2,1,0:T(8,128)(2,1)S(1)}, u32[]{:S(2)}, u32[]{:S(2)}) %all-to-all-start) | async-done | bytes 524320 | tf_op jit(solution)/shard_map/all_to_all | solution.py:482
  144.0 6.0 %all-to-all-start.2 = ((bf16[16,16,2048]{2,1,0:T(8,128)(2,1)}), bf16[16,16,2048]{2,1,0:T(8,128)(2,1)S(1)}, u32[]{:S(2)}, u32[]{:S(2)}) async-start(bf16[16,16,2048]{2,1,0:T(8,128)(2,1)} %bitcast.14), calls=%async_computation.2 | async-start | bytes 2097152 | tf_op jit(solution)/shard_map/all_to_all | solution.py:469
  150.0 0.0 all-gather.5.cloned.1.call-done.w_ref
  150.0 5.3 %shard_map.198 = (f32[128,2048]{1,0:T(8,128)}, bf16[128,2048]{1,0:T(8,128)(2,1)}) custom-call(s32[1]{0:T(128)} %bitcast.core_ref, bf16[8,256,128]{2,1,0:T(8,128)(2,1)} %copy-done.3, bf16[1024,2048]{1,0:T(8,128)(2,1)} %all-gather.5.cloned.1.call-done.w_ref), custom_call_target="tpu_custom_call" | custom-call | flops 1073741824 | bytes 4194304 | tf_op jit(solution)/shard_map/pallas_call | solution.py:277
  155.3 3.6 %collective-permute-start.6 = (bf16[128,2048]{1,0:T(8,128)(2,1)}, bf16[128,2048]{1,0:T(8,128)(2,1)S(1)}, u32[]{:S(2)}, u32[]{:S(2)}) collective-permute-start(bf16[128,2048]{1,0:T(8,128)(2,1)} %get-tuple-element.17), channel_id=1, source_target_pairs={{0,1},{1,0},{2,3},{3,2},{4,5},{5,4},{6,7},{7,6},{8,9},{9,8},{10,11... | collective-permute-start | bytes 1572872 | tf_op jit(solution)/shard_map/ppermute | solution.py:450
  158.9 4.8 %all-to-all-done.2 = bf16[16,16,2048]{2,1,0:T(8,128)(2,1)S(1)} async-done(((bf16[16,16,2048]{2,1,0:T(8,128)(2,1)}), bf16[16,16,2048]{2,1,0:T(8,128)(2,1)S(1)}, u32[]{:S(2)}, u32[]{:S(2)}) %all-to-all-start.2) | async-done | bytes 1048608 | tf_op jit(solution)/shard_map/all_to_all | solution.py:469
  163.7 1.0 copy-done.2
  164.7 2.6 %shard_map.201 = bf16[8,8,2048]{2,1,0:T(8,128)(2,1)} custom-call(bf16[64,2176]{1,0:T(8,128)(2,1)} %all_gather.11.tok_ref.side_ref, bf16[256,2048]{1,0:T(8,128)(2,1)} %bitcast.18), custom_call_target="tpu_custom_call" | custom-call | flops 134217728 | bytes 1310720 | tf_op jit(solution)/shard_map/pallas_call | solution.py:358
  167.3 14.3 %all_to_all.37 = bf16[8,8,2048]{2,1,0:T(8,128)(2,1)S(1)} all-to-all(bf16[8,8,2048]{2,1,0:T(8,128)(2,1)} %shard_map.201), channel_id=1, replica_groups=mesh['ep_0'=4,'ep_1'=4,'tp_0'=8,'tp_1'=2] {'tp_0'}, dimensions={0} | all-to-all | bytes 524288 | tf_op jit(solution)/shard_map/all_to_all | solution.py:487
  181.6 0.7 reduce_sum.32
  182.2 0.0 collective-permute-done.6
  182.2 0.9 add_convert_fusion.1
  (27 shorter events, 0.1 us)
Async XLA Ops:
  7.2 4.1 %copy-start.14 = (f32[8,2]{0,1:T(2,128)S(1)}, f32[8,2]{0,1:T(2,128)}, u32[]{:S(2)}) copy-start(f32[8,2]{0,1:T(2,128)} %param.34) | copy-start | bytes 196
  7.2 4.2 %copy-start.16 = (s32[8,2]{0,1:T(2,128)S(1)}, s32[8,2]{0,1:T(2,128)}, u32[]{:S(2)}) copy-start(s32[8,2]{0,1:T(2,128)} %param.33) | copy-start | bytes 196
  7.2 4.4 %copy-start.7 = (bf16[8,2048]{1,0:T(8,128)(2,1)S(1)}, bf16[8,2048]{1,0:T(8,128)(2,1)}, u32[]{:S(2)}) copy-start(bf16[8,2048]{1,0:T(8,128)(2,1)} %param.31) | copy-start | bytes 98308
  7.2 4.5 %copy-start.13 = (f32[2048]{0:T(1024)S(1)}, f32[2048]{0:T(1024)}, u32[]{:S(2)}) copy-start(f32[2048]{0:T(1024)} %param.32) | copy-start | bytes 24580
  7.2 76.9 %all-gather.3.cloned.1.call-start = ((), (), s32[]{:S(2)}) async-start(), calls=%async_computation.4 | async-start | bytes 8912896 | tf_op jit(solution)/shard_map/all_gather | solution.py:453
  10.5 139.5 %all-gather.5.cloned.1.call-start = ((), (), s32[]{:S(2)}) async-start(), calls=%async_computation.5 | async-start | bytes 4718592 | tf_op jit(solution)/shard_map/all_gather | solution.py:483
  11.3 56.1 %copy-start.8 = (bf16[2048,16]{0,1:T(8,128)(2,1)S(1)}, bf16[2048,16]{0,1:T(8,128)(2,1)}, u32[]{:S(2)}) copy-start(bf16[2048,16]{0,1:T(8,128)(2,1)} %param.24) | copy-start | bytes 196612
  11.8 56.6 %copy-start.9 = (bf16[2048,16]{0,1:T(8,128)(2,1)S(1)}, bf16[2048,16]{0,1:T(8,128)(2,1)}, u32[]{:S(2)}) copy-start(bf16[2048,16]{0,1:T(8,128)(2,1)} %param.25) | copy-start | bytes 196612
  60.5 14.6 %copy-start.5 = (bf16[16,16,2048]{2,1,0:T(8,128)(2,1)}, bf16[16,16,2048]{2,1,0:T(8,128)(2,1)S(1)}, u32[]{:S(2)}) copy-start(bf16[16,16,2048]{2,1,0:T(8,128)(2,1)S(1)} %all_to_all.36) | copy-start | bytes 3145732
  60.5 15.2 %collective-permute-start.7 = (bf16[256,2048]{1,0:T(8,128)(2,1)S(1)}, bf16[256,2048]{1,0:T(8,128)(2,1)S(1)}, u32[]{:S(2)}, u32[]{:S(2)}) collective-permute-start(bf16[256,2048]{1,0:T(8,128)(2,1)S(1)} %bitcast.21), channel_id=1, source_target_pairs={{0,1},{1,0},{2,3},{3,2},{4,5},{5,4},{6,7},{7,6},{8,9},{9,8},{10,11... | collective-permute-start | bytes 3145736 | tf_op jit(solution)/shard_map/ppermute | solution.py:450
  75.7 1.0 copy-start.15
  83.9 45.3 %collective-permute-start.8 = (bf16[256,2048]{1,0:T(8,128)(2,1)}, bf16[256,2048]{1,0:T(8,128)(2,1)S(1)}, u32[]{:S(2)}, u32[]{:S(2)}) collective-permute-start(bf16[256,2048]{1,0:T(8,128)(2,1)} %get-tuple-element.19), channel_id=1, source_target_pairs={{0,1},{1,0},{2,3},{3,2},{4,5},{5,4},{6,7},{7,6},{8,9},{9,8},{10,11... | collective-permute-start | bytes 3145736 | tf_op jit(solution)/shard_map/ppermute | solution.py:450
  84.1 45.1 %copy-start.4 = (bf16[256,2048]{1,0:T(8,128)(2,1)S(1)}, bf16[256,2048]{1,0:T(8,128)(2,1)}, u32[]{:S(2)}) copy-start(bf16[256,2048]{1,0:T(8,128)(2,1)} %get-tuple-element.18) | copy-start | bytes 3145732
  104.4 4.9 %collective-permute-start = (bf16[128,256]{1,0:T(8,128)(2,1)}, bf16[128,256]{1,0:T(8,128)(2,1)S(1)}, u32[]{:S(2)}, u32[]{:S(2)}) collective-permute-start(bf16[128,256]{1,0:T(8,128)(2,1)} %get-tuple-element.11.own_ref), channel_id=1, source_target_pairs={{0,16},{16,32},{32,48},{48,0},{1,17},{17,33},{33,49},{49,1},{2,18}... | collective-permute-start | bytes 196616 | tf_op jit(solution)/shard_map/ppermute | solution.py:422
  104.9 4.9 %collective-permute-start.1 = (bf16[128,256]{1,0:T(8,128)(2,1)}, bf16[128,256]{1,0:T(8,128)(2,1)S(1)}, u32[]{:S(2)}, u32[]{:S(2)}) collective-permute-start(bf16[128,256]{1,0:T(8,128)(2,1)} %get-tuple-element.11.own_ref), channel_id=1, source_target_pairs={{0,32},{16,48},{32,0},{48,16},{1,33},{17,49},{33,1},{49,17},{2,34}... | collective-permute-start | bytes 196616 | tf_op jit(solution)/shard_map/ppermute | solution.py:422
  106.0 4.8 %collective-permute-start.2 = (bf16[128,256]{1,0:T(8,128)(2,1)}, bf16[128,256]{1,0:T(8,128)(2,1)S(1)}, u32[]{:S(2)}, u32[]{:S(2)}) collective-permute-start(bf16[128,256]{1,0:T(8,128)(2,1)} %get-tuple-element.11.own_ref), channel_id=1, source_target_pairs={{0,48},{16,0},{32,16},{48,32},{1,49},{17,1},{33,17},{49,33},{2,50}... | collective-permute-start | bytes 196616 | tf_op jit(solution)/shard_map/ppermute | solution.py:422
  110.9 0.8 copy-start.1
  112.2 0.6 copy-start
  112.9 5.4 %collective-permute-start.3 = (bf16[128,256]{1,0:T(8,128)(2,1)S(1)}, bf16[128,256]{1,0:T(8,128)(2,1)S(1)}, u32[]{:S(2)}, u32[]{:S(2)}) collective-permute-start(bf16[128,256]{1,0:T(8,128)(2,1)S(1)} %get-tuple-element.12), channel_id=1, source_target_pairs={{0,64},{64,128},{128,192},{192,0},{1,65},{65,129},{129,193},{193,1... | collective-permute-start | bytes 196616 | tf_op jit(solution)/shard_map/ppermute | solution.py:422
  112.9 5.4 %collective-permute-start.4 = (bf16[128,256]{1,0:T(8,128)(2,1)S(1)}, bf16[128,256]{1,0:T(8,128)(2,1)S(1)}, u32[]{:S(2)}, u32[]{:S(2)}) collective-permute-start(bf16[128,256]{1,0:T(8,128)(2,1)S(1)} %get-tuple-element.12), channel_id=1, source_target_pairs={{0,128},{64,192},{128,0},{192,64},{1,129},{65,193},{129,1},{193,65... | collective-permute-start | bytes 196616 | tf_op jit(solution)/shard_map/ppermute | solution.py:422
  114.9 4.0 %collective-permute-start.5 = (bf16[128,256]{1,0:T(8,128)(2,1)S(1)}, bf16[128,256]{1,0:T(8,128)(2,1)S(1)}, u32[]{:S(2)}, u32[]{:S(2)}) collective-permute-start(bf16[128,256]{1,0:T(8,128)(2,1)S(1)} %get-tuple-element.12), channel_id=1, source_target_pairs={{0,192},{64,0},{128,64},{192,128},{1,193},{65,1},{129,65},{193,129... | collective-permute-start | bytes 196616 | tf_op jit(solution)/shard_map/ppermute | solution.py:422
  118.3 0.6 copy-start.10
  118.3 0.7 copy-start.11
  118.9 0.6 copy-start.12
  124.0 20.0 %all-to-all-start = ((bf16[8,256,128]{2,1,0:T(8,128)(2,1)}), bf16[8,256,128]{2,1,0:T(8,128)(2,1)S(1)}, u32[]{:S(2)}, u32[]{:S(2)}) async-start(bf16[8,256,128]{2,1,0:T(8,128)(2,1)} %bitcast.20), calls=%async_computation | async-start | bytes 1048576 | tf_op jit(solution)/shard_map/all_to_all | solution.py:482
  144.0 6.1 %copy-start.3 = (bf16[8,256,128]{2,1,0:T(8,128)(2,1)}, bf16[8,256,128]{2,1,0:T(8,128)(2,1)S(1)}, u32[]{:S(2)}) copy-start(bf16[8,256,128]{2,1,0:T(8,128)(2,1)S(1)} %all-to-all-done.x_ref) | copy-start | bytes 1572868
  144.0 19.7 %all-to-all-start.2 = ((bf16[16,16,2048]{2,1,0:T(8,128)(2,1)}), bf16[16,16,2048]{2,1,0:T(8,128)(2,1)S(1)}, u32[]{:S(2)}, u32[]{:S(2)}) async-start(bf16[16,16,2048]{2,1,0:T(8,128)(2,1)} %bitcast.14), calls=%async_computation.2 | async-start | bytes 2097152 | tf_op jit(solution)/shard_map/all_to_all | solution.py:469
  155.3 27.0 %copy-start.6 = (f32[128,2048]{1,0:T(8,128)S(1)}, f32[128,2048]{1,0:T(8,128)}, u32[]{:S(2)}) copy-start(f32[128,2048]{1,0:T(8,128)} %get-tuple-element.16) | copy-start | bytes 3145732
  155.3 27.0 %collective-permute-start.6 = (bf16[128,2048]{1,0:T(8,128)(2,1)}, bf16[128,2048]{1,0:T(8,128)(2,1)S(1)}, u32[]{:S(2)}, u32[]{:S(2)}) collective-permute-start(bf16[128,2048]{1,0:T(8,128)(2,1)} %get-tuple-element.17), channel_id=1, source_target_pairs={{0,1},{1,0},{2,3},{3,2},{4,5},{5,4},{6,7},{7,6},{8,9},{9,8},{10,11... | collective-permute-start | bytes 1572872 | tf_op jit(solution)/shard_map/ppermute | solution.py:450
  163.7 1.0 copy-start.2
Sparse Core Ops, SparseCore 0:
  10.7 61.5 all-gather.2
  74.0 52.8 all-gather.4

commit v2 on v1

v2 whole, which is shorter than its diff:
```python
import functools

import jax
import jax.numpy as jnp
from jax import lax
from jax.experimental import pallas as pl
from jax.experimental.pallas import tpu as pltpu
from jax.sharding import Mesh
from jax.sharding import PartitionSpec as P


HEAD = 128
BLOCK = 128
TOKENS = 8
SLOTS = 2
SPAN_LIMIT = 44
EP = ("ep_0", "ep_1")
TP = ("tp_0", "tp_1")
EP_TP = ("ep_0", "ep_1", "tp_0", "tp_1")
F32 = jnp.float32
BF16 = jnp.bfloat16


norm_eps = 1e-06
NN = (((1,), (0,)), ((), ()))
NT = (((1,), (1,)), ((), ()))
TN = (((0,), (0,)), ((), ()))


def mm(a, b, dims=NN):
    return lax.dot_general(a.astype(BF16), b.astype(BF16), dims, preferred_element_type=F32)


def silu(x):
    return x / (1.0 + jnp.exp(-x))


def rms_scale(rows_in, gain_vec):
    widened = rows_in.astype(F32)
    scaled = widened * lax.rsqrt(jnp.mean(widened * widened, axis=-1, keepdims=True) + norm_eps)
    return (scaled * gain_vec).astype(BF16)


def invert_unit_lower(mats, row, col):
    apart = row ^ col
    eye = (row == col).astype(F32)
    size = 1
    invs = None
    while size < BLOCK:
        pick = (apart >= size) & (apart < 2 * size)
        parts = [jnp.where(pick, m, 0.0) for m in mats]
        if invs is None:
            invs = [eye - p for p in parts]
        else:
            invs_low = [x.astype(BF16) for x in invs]
            half = [mm(p, x) for p, x in zip(parts, invs_low)]
            invs = [x - mm(xl, h) for x, xl, h in zip(invs, invs_low, half)]
        size *= 2
    return invs


def span_kernel(
    chunks, scal_ref, head_ref, rows_ref, q_ref, k_ref, v_ref, strength_ref, decay_ref, extra_ref,
    g_ref, h_ref, ab_ref, rows, weights, proj, low, high, lasts, sems
):
    tall = rows_ref.shape[0] // chunks
    blocks = rows_ref.shape[0] // BLOCK
    count = blocks // 2
    copies = [
        pltpu.make_async_copy(ref, weights.at[:, pl.ds(i * HEAD, HEAD)], sems.at[i])
        for i, ref in enumerate((q_ref, k_ref, v_ref))
    ]
    row_copies = [
        pltpu.make_async_copy(rows_ref.at[pl.ds(i * tall, tall)], rows.at[pl.ds(i * tall, tall)], sems.at[3 + i])
        for i in range(chunks)
    ]
    for copy in copies + row_copies:
        copy.start()
    heads = strength_ref.shape[0]
    pick_row = lax.broadcasted_iota(jnp.int32, (heads, HEAD), 0) == head_ref[0]
    pick_col = lax.broadcasted_iota(jnp.int32, (heads, HEAD), 1)
    weights[:, 3 * HEAD :] = (
        mm(strength_ref[...], (pick_row & (pick_col == 0)).astype(BF16), TN)
        + mm(decay_ref[...], (pick_row & (pick_col == 1)).astype(BF16), TN)
    ).astype(BF16)
    row = lax.broadcasted_iota(jnp.int32, (BLOCK, BLOCK), 0)
    col = lax.broadcasted_iota(jnp.int32, (BLOCK, BLOCK), 1)
    upper = (row <= col).astype(F32)
    speed, largest = scal_ref[0], scal_ref[1]
    for copy in copies:
        copy.wait()

    def half(i, carry):
        start = i * count
        for c in range(chunks // 2):
            chunk = i * (chunks // 2) + c
            at = pl.ds(pl.multiple_of(chunk * tall, tall), tall)
            pltpu.make_async_copy(rows_ref.at[at], rows.at[at], sems.at[3 + chunk]).wait()
            proj[c * tall : (c + 1) * tall, :] = lax.dot_general(
                rows[at, :], weights[...], NN, preferred_element_type=F32
            )
        mats, keep = [], []
        for b in range(count):
            at = slice(b * BLOCK, (b + 1) * BLOCK)
            q = silu(proj[at, 0:HEAD])
            k = silu(proj[at, HEAD : 2 * HEAD])
            v = silu(proj[at, 2 * HEAD : 3 * HEAD])
            k = k * lax.rsqrt(jnp.sum(k * k, axis=1, keepdims=True) + 1e-06)
            small = proj[at, 3 * HEAD : 4 * HEAD]
            strength = largest * (1.0 / (1.0 + jnp.exp(-small[:, 0:1])))
            flipped = small.T
            x = flipped[0:8, :]
            soft = jnp.maximum(x, 0.0) + jnp.log1p(jnp.exp(-jnp.abs(x)))
            steps = extra_ref[pl.ds(start + b, 1), :] - speed * soft[1:2, :]
            cum_row = lax.dot_general(
                jnp.broadcast_to(steps, (8, BLOCK)), upper, NN, preferred_element_type=F32, precision=lax.Precision.HIGHEST
            )[0:1, :]
            across = jnp.broadcast_to(cum_row, (BLOCK, BLOCK))
            down = across.T
            total = jnp.broadcast_to(cum_row[:, BLOCK - 1 : BLOCK], (BLOCK, BLOCK))
            decay = jnp.exp(jnp.where(row >= col, down - across, -1e30))
            grow = jnp.exp(down)
            both = mm(jnp.concatenate([k, q], axis=0), k, NT)
            mats.append(jnp.where(row > col, both[:BLOCK] * decay * strength, 0.0))
            right = jnp.concatenate([v * strength, k * (grow * strength)], axis=1)
            keep.append((q * grow, both[BLOCK:] * decay, right, k * jnp.exp(total - down)))
            lasts[start + b] = jnp.exp(total[0:8, :])
        invs = invert_unit_lower(mats, row, col)
        for b in range(count):
            query_dec, scores, right, keys_dec = keep[b]
            solved = mm(invs[b], right)
            seen = mm(scores, solved)
            kept = mm(keys_dec, solved, TN)
            high[start + b, :, :HEAD] = kept[:, :HEAD]
            high[start + b, :, HEAD:] = seen[:, :HEAD]
            low[start + b, :HEAD, :] = (query_dec - seen[:, HEAD:]).astype(BF16)
            low[start + b, HEAD:, :] = kept[:, HEAD:].astype(BF16)
        return carry

    lax.fori_loop(0, 2, half, 0)
    maps = (row == col).astype(F32)
    memory = jnp.zeros((HEAD, HEAD), F32)
    for j in range(blocks):
        both = jnp.concatenate([maps, memory], axis=1).astype(BF16)
        out = mm(low[j], both)
        g_ref[j * BLOCK : (j + 1) * BLOCK, :] = out[:HEAD, :HEAD].astype(BF16)
        h_ref[j * BLOCK : (j + 1) * BLOCK, :] = out[:HEAD, HEAD:] + high[j, :, HEAD:]
        last = lasts[j, 0:1, :]
        maps = maps * last - out[HEAD:, :HEAD]
        memory = memory * last - out[HEAD:, HEAD:] + high[j, :, :HEAD]
    ab_ref[:, :HEAD] = maps.astype(BF16)
    ab_ref[:, HEAD:] = memory.astype(BF16)


def span_terms(scal, head, rows, query, key, value, strength, decay, extra):
    length, depth = rows.shape
    blocks = length // BLOCK
    width = 4 * HEAD
    chunks = 4
    smem = pl.BlockSpec(memory_space=pltpu.SMEM)
    vmem = pl.BlockSpec(memory_space=pltpu.VMEM)
    hbm = pl.BlockSpec(memory_space=pltpu.HBM)
    return pl.pallas_call(
        functools.partial(span_kernel, chunks),
        out_shape=(
            jax.ShapeDtypeStruct((length, HEAD), BF16),
            jax.ShapeDtypeStruct((length, HEAD), F32),
            jax.ShapeDtypeStruct((HEAD, 2 * HEAD), BF16),
        ),
        in_specs=[smem, smem, hbm, hbm, hbm, hbm, vmem, vmem, vmem],
        out_specs=(vmem, vmem, vmem),
        scratch_shapes=[
            pltpu.VMEM((length, depth), BF16),
            pltpu.VMEM((depth, width), BF16),
            pltpu.VMEM((length // 2, width), F32),
            pltpu.VMEM((blocks, 2 * HEAD, HEAD), BF16),
            pltpu.VMEM((blocks, HEAD, 2 * HEAD), F32),
            pltpu.VMEM((blocks, 8, HEAD), F32),
            pltpu.SemaphoreType.DMA((3 + chunks,)),
        ],
        compiler_params=pltpu.CompilerParams(vmem_limit_bytes=SPAN_LIMIT * 1024 * 1024),
        cost_estimate=pl.CostEstimate(
            flops=length * 2 * (depth * width + 40 * HEAD * HEAD * 4),
            bytes_accessed=2 * (rows.size + depth * width) + length * HEAD * 6,
            transcendentals=0,
        ),
    )(scal, head, *[pltpu.with_memory_space_constraint(x, pltpu.HBM) for x in (rows, query, key, value)], strength, decay, extra)


def row_kernel(here_ref, own_ref, one_ref, two_ref, three_ref, before_ref, total_ref, slots):
    here = here_ref[0]
    slots[here] = own_ref[...]
    slots[(here + 3) % 4] = one_ref[...]
    slots[(here + 2) % 4] = two_ref[...]
    slots[(here + 1) % 4] = three_ref[...]
    row = lax.broadcasted_iota(jnp.int32, (HEAD, 2 * HEAD), 0)
    col = lax.broadcasted_iota(jnp.int32, (HEAD, 2 * HEAD), 1)
    eye = (row == col).astype(F32)
    so_far = slots[0].astype(F32)
    before = jnp.where(here == 0, eye, so_far)
    for k in range(1, 4):
        piece = slots[k]
        own = jnp.where(col >= HEAD, piece.astype(F32), 0.0)
        so_far = mm(piece[:, :HEAD], so_far) + own
        if k < 3:
            before = jnp.where(here > k, so_far, before)
    before_ref[...] = before
    total_ref[...] = so_far.astype(BF16)


def compose_row(here, own, one, two, three):
    vmem = pl.BlockSpec(memory_space=pltpu.VMEM)
    return pl.pallas_call(
        row_kernel,
        out_shape=(jax.ShapeDtypeStruct((HEAD, 2 * HEAD), F32), jax.ShapeDtypeStruct((HEAD, 2 * HEAD), BF16)),
        in_specs=[pl.BlockSpec(memory_space=pltpu.SMEM)] + [vmem] * 4,
        out_specs=(vmem, vmem),
        scratch_shapes=[pltpu.VMEM((4, HEAD, 2 * HEAD), BF16)],
        compiler_params=pltpu.CompilerParams(vmem_limit_bytes=8 * 1024 * 1024),
        cost_estimate=pl.CostEstimate(flops=12 * HEAD**3, bytes_accessed=8 * HEAD * HEAD, transcendentals=0),
    )(here, own, one, two, three)


def apply_kernel(here_ref, one_ref, two_ref, three_ref, before_ref, g_ref, h_ref, gain_ref, out_ref, slots):
    here = here_ref[0]
    slots[(here + 3) % 4] = one_ref[...]
    slots[(here + 2) % 4] = two_ref[...]
    slots[(here + 1) % 4] = three_ref[...]
    memory = jnp.where(here > 0, slots[0][:, HEAD:].astype(F32), 0.0)
    for k in range(1, 3):
        piece = slots[k]
        moved = mm(piece[:, :HEAD], memory) + piece[:, HEAD:].astype(F32)
        memory = jnp.where(here > k, moved, memory)
    memory = mm(before_ref[:, :HEAD], memory) + before_ref[:, HEAD:]
    heads_out = mm(g_ref[...], memory) + h_ref[...]
    scale = lax.rsqrt(jnp.mean(heads_out * heads_out, axis=1, keepdims=True) + norm_eps)
    out_ref[...] = (heads_out * scale * gain_ref[...]).astype(BF16)


def apply_memory(here, one, two, three, before, g, h, gain):
    vmem = pl.BlockSpec(memory_space=pltpu.VMEM)
    return pl.pallas_call(
        apply_kernel,
        out_shape=jax.ShapeDtypeStruct(h.shape, BF16),
        in_specs=[pl.BlockSpec(memory_space=pltpu.SMEM)] + [vmem] * 7,
        out_specs=vmem,
        scratch_shapes=[pltpu.VMEM((4, HEAD, 2 * HEAD), BF16)],
        compiler_params=pltpu.CompilerParams(vmem_limit_bytes=8 * 1024 * 1024),
        cost_estimate=pl.CostEstimate(flops=h.size * 2 * HEAD, bytes_accessed=h.size * 8, transcendentals=0),
    )(here, one, two, three, before, g, h, gain.reshape(1, HEAD))


def output_kernel(x_ref, w_ref, out_ref, rows):
    @pl.when(pl.program_id(0) == 0)
    def _():
        for h in range(x_ref.shape[0]):
            rows[:, h * HEAD : (h + 1) * HEAD] = x_ref[h]

    out_ref[...] = mm(rows[...], w_ref[...]).astype(BF16)


def output_product(by_head, weights):
    depth, width = weights.shape
    count = by_head.shape[1]
    step = width // 8
    column = lambda i: (0, i)
    return pl.pallas_call(
        output_kernel,
        grid=(8,),
        out_shape=jax.ShapeDtypeStruct((count, width), BF16),
        in_specs=[pl.BlockSpec(by_head.shape, lambda i: (0, 0, 0)), pl.BlockSpec((depth, step), column)],
        out_specs=pl.BlockSpec((count, step), column),
        scratch_shapes=[pltpu.VMEM((count, depth), BF16)],
        cost_estimate=pl.CostEstimate(
            flops=2 * count * depth * width, bytes_accessed=2 * depth * width, transcendentals=0
        ),
        compiler_params=pltpu.CompilerParams(vmem_limit_bytes=32 * 1024 * 1024),
    )(by_head, pltpu.with_memory_space_constraint(weights, pltpu.HBM))


def route_columns(side, experts):
    tokens = side.shape[1]
    expert = lax.broadcasted_iota(jnp.int32, (experts, tokens), 0).astype(F32)
    first, second = side[0:1] == expert, side[1:2] == expert
    named = (first | second).astype(F32)
    row = lax.broadcasted_iota(jnp.int32, (tokens, tokens), 0)
    col = lax.broadcasted_iota(jnp.int32, (tokens, tokens), 1)
    earlier = ((row < col) & (row // TOKENS == col // TOKENS)).astype(F32)
    return first, named, mm(named, earlier)


def slot_rows(named, slots, e):
    tokens = named.shape[1]
    rows = tokens // TOKENS * SLOTS
    row = lax.broadcasted_iota(jnp.int32, (rows, tokens), 0)
    col = lax.broadcasted_iota(jnp.int32, (rows, tokens), 1)
    taken = jnp.where(named[e : e + 1] > 0.5, slots[e : e + 1], -1.0)
    return (taken == (row % SLOTS).astype(F32)) & (row // SLOTS == col // TOKENS)


def pack_kernel(experts, tok_ref, out_ref):
    width = out_ref.shape[1]
    side = tok_ref[:, width:].astype(F32).T
    _, named, slots = route_columns(side, experts)
    rows = out_ref.shape[0] // experts
    group = 4
    for e in range(0, experts, group):
        pick = jnp.concatenate([slot_rows(named, slots, e + i).astype(F32) for i in range(group)], axis=0)
        out_ref[e * rows : (e + group) * rows, :] = mm(pick, tok_ref[:, :width]).astype(BF16)


def pack_tokens(tokens, experts):
    count, width = tokens.shape
    vmem = pl.BlockSpec(memory_space=pltpu.VMEM)
    rows = count // TOKENS * SLOTS * experts
    return pl.pallas_call(
        functools.partial(pack_kernel, experts),
        out_shape=jax.ShapeDtypeStruct((rows, width - HEAD), BF16),
        in_specs=[vmem],
        out_specs=vmem,
        cost_estimate=pl.CostEstimate(flops=2 * rows * count * width, bytes_accessed=2 * rows * width, transcendentals=0),
    )(tokens)


def combine_kernel(experts, side_ref, back_ref, out_ref):
    side = side_ref[...].astype(F32).T
    first, named, slots = route_columns(side, experts)
    share = [side[2 + k : 3 + k] + side[4 + k : 5 + k] + side[6 + k : 7 + k] for k in range(2)]
    picks = []
    for e in range(experts):
        share_row = jnp.where(first[e : e + 1], share[0], share[1])
        picks.append(jnp.where(slot_rows(named, slots, e), share_row, 0.0))
    pick = jnp.concatenate(picks, axis=0)
    high = pick.astype(BF16)
    low = (pick - high.astype(F32)).astype(BF16)
    back = back_ref[...]
    out = mm(high, back, TN) + mm(low, back, TN)
    out_ref[...] = out.reshape(out_ref.shape).astype(BF16)


def combine_tokens(tokens, back, experts):
    count, _ = tokens.shape
    width = back.shape[1]
    shape = (count // TOKENS, TOKENS, width)
    return pl.pallas_call(
        functools.partial(combine_kernel, experts),
        grid=(1,),
        out_shape=jax.ShapeDtypeStruct(shape, BF16),
        in_specs=[
            pl.BlockSpec((count, HEAD), lambda i: (0, width // HEAD)),
            pl.BlockSpec(back.shape, lambda i: (0, 0)),
        ],
        out_specs=pl.BlockSpec(shape, lambda i: (0, 0, 0)),
        compiler_params=pltpu.CompilerParams(vmem_limit_bytes=24 * 1024 * 1024),
        cost_estimate=pl.CostEstimate(
            flops=4 * count * back.size, bytes_accessed=2 * back.size + 2 * count * width, transcendentals=0
        ),
    )(tokens, back)


def expert_kernel(own_ref, other_ref, gate_ref, up_ref, down_ref, mine_ref, theirs_ref, rows, gate, up, down, sems):
    half = own_ref.shape[0]
    pairs = (
        (own_ref, rows.at[pl.ds(0, half)]),
        (other_ref, rows.at[pl.ds(half, half)]),
        (gate_ref, gate),
        (up_ref, up),
        (down_ref, down),
    )
    copies = [pltpu.make_async_copy(src, dst, sems.at[i]) for i, (src, dst) in enumerate(pairs)]
    for copy in copies:
        copy.start()
    for copy in copies[:3]:
        copy.wait()
    gated = silu(mm(rows[...], gate[...], NT))
    copies[3].wait()
    hidden = (gated * mm(rows[...], up[...], NT)).astype(BF16)
    copies[4].wait()
    theirs_ref[...] = mm(hidden[half:], down[...]).astype(BF16)
    mine_ref[...] = mm(hidden[:half], down[...]).astype(BF16)


def expert_sums(own, other, gate, up, down):
    half, width = own.shape
    units = gate.shape[0]
    out = jax.ShapeDtypeStruct((half, width), BF16)
    vmem = pl.BlockSpec(memory_space=pltpu.VMEM)
    return pl.pallas_call(
        expert_kernel,
        out_shape=(out, out),
        in_specs=[pl.BlockSpec(memory_space=pl.ANY)] * 5,
        out_specs=(vmem, vmem),
        scratch_shapes=[
            pltpu.VMEM((2 * half, width), BF16),
            pltpu.VMEM((units, width), BF16),
            pltpu.VMEM((units, width), BF16),
            pltpu.VMEM((units, width), BF16),
            pltpu.SemaphoreType.DMA((5,)),
        ],
        cost_estimate=pl.CostEstimate(
            flops=12 * half * width * units, bytes_accessed=6 * units * width + 8 * half * width, transcendentals=0
        ),
        compiler_params=pltpu.CompilerParams(vmem_limit_bytes=36 * 1024 * 1024),
    )(own, other, *[pltpu.with_memory_space_constraint(x, pltpu.HBM) for x in (gate, up, down)])


def around(x, axis):
    size = lax.axis_size(axis)
    out = []
    for k in range(1, size):
        out.append(lax.ppermute(x, axis, [(i, (i + k) % size) for i in range(size)]))
    return out


def mixed_step(
    mixer_input_rows,
    mixer_norm_gain,
    query_weight,
    key_weight,
    value_weight,
    write_strength_projection,
    decay_projection,
    head_decay_speed,
    largest_write_strength,
    extra_log_decay,
    head_norm_gain,
    mixer_output_weight,
    expert_input_rows,
    expert_norm_gain,
    routes,
    expert_route_weight,
    gate_weight,
    up_weight,
    down_weight,
):
    head = lax.axis_index(TP)
    experts = gate_weight.shape[0] * lax.axis_size(EP)
    cross = lambda x: lax.ppermute(x, "tp_1", [(0, 1), (1, 0)])

    mix_normed = rms_scale(mixer_input_rows, mixer_norm_gain)
    exp_normed = rms_scale(expert_input_rows, expert_norm_gain)
    parts, rest = [], expert_route_weight
    for _ in range(3):
        part = lax.reduce_precision(rest, 8, 7)
        parts.append(part.astype(BF16))
        rest = rest - part
    side = jnp.concatenate([routes.astype(BF16)] + parts, axis=1)
    side = jnp.pad(side, ((0, 0), (0, HEAD - side.shape[1])))
    tokens = lax.all_gather(jnp.concatenate([exp_normed, side], axis=1), "tp_0", axis=0, tiled=True)
    tokens, mix_normed = lax.optimization_barrier((tokens, mix_normed))
    mix_rows = lax.all_gather(mix_normed, TP, axis=0, tiled=True)
    packed = pack_tokens(tokens, experts)
    exp_rows = lax.all_to_all(packed, EP, split_axis=0, concat_axis=0, tiled=True)
    other_rows = cross(exp_rows)
    mine, theirs = expert_sums(exp_rows, other_rows, gate_weight[0].T, up_weight[0].T, down_weight[0])
    pair = (mine.astype(F32) + cross(theirs).astype(F32)).astype(BF16)
    back = lax.all_to_all(pair, EP, split_axis=0, concat_axis=0, tiled=True)
    combined = combine_tokens(tokens, back, experts)

    scal = jnp.concatenate([head_decay_speed, largest_write_strength])
    extra = extra_log_decay.reshape(-1, BLOCK)
    gains, local, span = span_terms(
        scal,
        head[None],
        mix_rows,
        query_weight,
        key_weight,
        value_weight,
        write_strength_projection.T,
        decay_projection.T,
        extra,
    )
    row_pieces = around(span, "ep_1")
    before, total = compose_row(lax.axis_index("ep_1")[None], span, *row_pieces)
    mixed = apply_memory(lax.axis_index("ep_0")[None], *around(total, "ep_0"), before, gains, local, head_norm_gain)

    by_head = lax.all_to_all(mixed.reshape(-1, BLOCK, HEAD), TP, split_axis=0, concat_axis=0, tiled=True)
    w_whole = lax.all_gather(mixer_output_weight, TP, axis=0, tiled=True)
    mix_out = output_product(by_head, w_whole)

    pieces = lax.all_to_all(combined, "tp_0", split_axis=0, concat_axis=0, tiled=True)
    exp_out = jnp.sum(pieces.astype(F32), axis=0).astype(BF16)
    return (mix_out, exp_out)


def solution(mesh):
    torus = Mesh(mesh.devices.reshape(4, 4, 8, 2), ("ep_0", "ep_1", "tp_0", "tp_1"))
    placed = (
        P(EP_TP, None),
        P(),
        P(None, TP),
        P(None, TP),
        P(None, TP),
        P(),
        P(),
        P(TP),
        P(TP),
        P(EP, TP),
        P(),
        P(TP, None),
        P(EP_TP, None),
        P(),
        P(EP_TP, None),
        P(EP_TP, None),
        P(EP, None, TP),
        P(EP, None, TP),
        P(EP, TP, None),
    )
    return jax.shard_map(
        mixed_step,
        mesh=torus,
        in_specs=placed,
        out_specs=(P(EP_TP, None), P(EP_TP, None)),
        check_vma=False,
    )
```

time: 193 us -> 187 us (0.969)
  waiting for transfers between devices: 25.6 us -> 45 us
  blocking collectives: 60.3 us -> 44 us
  Pallas kernels: 47.3 us -> 38.6 us
  starting transfers between devices: 27.8 us -> 33.8 us
  local copies, waits for them, and re-layouts: 6.32 us -> 0.87 us
    all_to_all x1 -> x0, blocking collectives: 14.3 us -> none  [mixed_step(): lax.all_to_all(combined, 'tp_0', split_axis=0, concat_axis=0, tiled=True)]
    all_to_all x1, waiting for transfers between devices: 4.77 us -> 16.2 us  [mixed_step(): back = lax.all_to_all(pair, EP, split_axis=0, concat_axis=0, tiled=True)]
    all_to_all x1 -> x2, starting transfers between devices: 5.15 us -> 15.7 us  [the longest x1 11.4 us: mixed_step(): lax.all_to_all(mixed.reshape(-1, BLOCK, HEAD), TP, split_axis=0, concat_a...]
    pallas_call x4 -> x3, Pallas kernels: 34.5 us -> 28.6 us  [the longest x1 19 us: span_terms(): pl.pallas_call(functools.partial(span_kernel, chunks), out_shape=(jax.Sha...]
    all_gather x1, waiting for transfers between devices: 0.02 us -> 5.69 us  [mixed_step(): w_whole = lax.all_gather(mixer_output_weight, TP, axis=0, tiled=True)]
    unnamed x37 -> x11, local copies, waits for them, and re-layouts: 6.22 us -> 0.78 us
    ppermute x3 -> x2, waiting for transfers between devices: 0.01 us -> 5.06 us  [mixed_step(): cross = lambda x: lax.ppermute(x, 'tp_1', [(0, 1), (1, 0)])]
    all_to_all x1 -> x2, waiting for transfers between devices: 13.5 us -> 11 us  [the longest x1 11 us: mixed_step(): lax.all_to_all(mixed.reshape(-1, BLOCK, HEAD), TP, split_axis=0, concat_a...]
  transfers between devices with their start and end apart: 13 -> 13, of which waited for: 7 -> 10; matrix products, arithmetic and copies ran while one was open for 3% -> 1% of each run, Pallas kernels for 25% -> 17%
where the time goes in v2:
time: 187 us; the launch traced here: 186 us
  waiting for transfers between devices  45 us (24%)
  blocking collectives  44 us (24%)
  Pallas kernels  38.6 us (21%)
  starting transfers between devices  33.8 us (18%)
  between operations  15.4 us (8%)
  other arithmetic  7.89 us (4%)
    all_gather x1, blocking collectives, mixed_step(): lax.all_gather(jnp.concatenate([exp_normed, side], axis=1), 'tp_0', axis=...  25.3 us
    pallas_call x1, Pallas kernels, span_terms(): pl.pallas_call(functools.partial(span_kernel, chunks), out_shape=(jax.Sha...  19 us
    all_to_all x1, blocking collectives, mixed_step(): lax.all_to_all(packed, EP, split_axis=0, concat_axis=0, tiled=True)  18.7 us
    all_to_all x1, waiting for transfers between devices, mixed_step(): back = lax.all_to_all(pair, EP, split_axis=0, concat_axis=0, tiled=True)  16.2 us
    all_to_all x1, starting transfers between devices, mixed_step(): lax.all_to_all(mixed.reshape(-1, BLOCK, HEAD), TP, split_axis=0, concat_a...  11.4 us
    all_to_all x1, waiting for transfers between devices, mixed_step(): lax.all_to_all(mixed.reshape(-1, BLOCK, HEAD), TP, split_axis=0, concat_a...  11 us
    ppermute x2, starting transfers between devices, mixed_step(): cross = lambda x: lax.ppermute(x, 'tp_1', [(0, 1), (1, 0)])  8.45 us
    pallas_call x1, Pallas kernels, output_product(): pl.pallas_call(output_kernel, grid=(8,), out_shape=jax.ShapeDtypeStruct((...  7.84 us
  transfers between devices with their start and end apart: 13, of which 10 were waited for; matrix products, arithmetic and copies ran while one was open for 1% of the time, Pallas kernels for 17%

profile of v2, /device:TPU:1, one launch (start us, length us, event | category | flops | bytes accessed | tf_op | source)
XLA Modules:
  0.0 185.7 jit_solution(3013816382626263876)
XLA Ops:
  7.2 0.0 all-gather.3.cloned.1.call-start
  7.2 0.8 copy.24
  8.0 0.7 convert_element_type.39
  8.7 0.1 copy.26
  8.8 0.9 fusion.3
  9.7 0.8 fusion.5
  10.5 0.1 fusion.14
  10.6 25.3 %all_gather.9.tok_ref.side_ref = bf16[64,2176]{1,0:T(8,128)(2,1)} all-gather(bf16[8,2176]{1,0:T(8,128)(2,1)S(1)} %pad_maximum_fusion), channel_id=1, replica_groups=mesh['ep_0'=4,'ep_1'=4,'tp_0'=8,'tp_1'=2] {'tp_0'}, dimensions={0}, use_global_device_ids=true | all-gather | bytes 313344 | tf_op jit(solution)/shard_map/all_gather | solution.py:449
  35.9 1.2 fusion
  37.2 2.0 %fusion.2 = bf16[128,2048]{1,0:T(8,128)(2,1)} fusion(bf16[128,2048]{1,0:T(8,128)(2,1)} %param.19, f32[2048]{0:T(1024)} %param.20, f32[128]{0:T(128)S(1)} %add_rsqrt_fusion), kind=kLoop, calls=%fused_computation.5 | loop fusion | flops 1048576 | bytes 1057280 | tf_op jit(solution)/shard_map/convert_element_type | solution.py:41
  39.2 0.0 all-gather.3.cloned.1.call-update
  39.2 0.0 all-gather.5.cloned.1.call-start
  39.3 0.7 all-gather.5.cloned.1.call-update
  40.0 2.5 %shard_map.198 = bf16[256,2048]{1,0:T(8,128)(2,1)} custom-call(bf16[64,2176]{1,0:T(8,128)(2,1)} %all_gather.9.tok_ref.side_ref), custom_call_target="tpu_custom_call" | custom-call | flops 71303168 | bytes 1114112 | tf_op jit(solution)/shard_map/pallas_call | solution.py:316
  42.5 18.7 %all_to_all.32 = bf16[16,16,2048]{2,1,0:T(8,128)(2,1)S(1)} all-to-all(bf16[16,16,2048]{2,1,0:T(8,128)(2,1)} %bitcast.26), channel_id=1, replica_groups=mesh['ep_0'=4,'ep_1'=4,'tp_0'=8,'tp_1'=2] {'ep_0','ep_1'}, dimensions={0} | all-to-all | bytes 2097152 | tf_op jit(solution)/shard_map/all_to_all | solution.py:453
  61.2 7.9 %collective-permute-start.6 = (bf16[256,2048]{1,0:T(8,128)(2,1)S(1)}, bf16[256,2048]{1,0:T(8,128)(2,1)S(1)}, u32[]{:S(2)}, u32[]{:S(2)}) collective-permute-start(bf16[256,2048]{1,0:T(8,128)(2,1)S(1)} %bitcast.20), channel_id=1, source_target_pairs={{0,1},{1,0},{2,3},{3,2},{4,5},{5,4},{6,7},{7,6},{8,9},{9,8},{10,11... | collective-permute-start | bytes 3145736 | tf_op jit(solution)/shard_map/ppermute | solution.py:438
  69.1 2.5 %collective-permute-done.6.other_ref = bf16[256,2048]{1,0:T(8,128)(2,1)S(1)} collective-permute-done((bf16[256,2048]{1,0:T(8,128)(2,1)S(1)}, bf16[256,2048]{1,0:T(8,128)(2,1)S(1)}, u32[]{:S(2)}, u32[]{:S(2)}) %collective-permute-start.6) | collective-permute-done | bytes 1048608 | tf_op jit(solution)/shard_map/ppermute | solution.py:438
  71.6 5.6 %shard_map.199 = (bf16[256,2048]{1,0:T(8,128)(2,1)S(1)}, bf16[256,2048]{1,0:T(8,128)(2,1)S(1)}) custom-call(bf16[256,2048]{1,0:T(8,128)(2,1)S(1)} %bitcast.21, bf16[256,2048]{1,0:T(8,128)(2,1)S(1)} %collective-permute-done.6.other_ref, bf16[448,2048]{1,0:T(8,128)(2,1)} %bitcast.27, bf16[448,2048]{1,0:T(8,128)(2,1)} %bitcast.28, bf16[448,2048]{1,0:T(8,128)(2,1)} %bitcast.29), custom_call_target="tpu_custom_call" | custom-call | flops 2818572288 | bytes 9699328 | tf_op jit(solution)/shard_map/pallas_call | solution.py:388
  77.3 0.5 collective-permute-start.7
  77.8 2.6 %collective-permute-done.7 = bf16[256,2048]{1,0:T(8,128)(2,1)S(1)} collective-permute-done((bf16[256,2048]{1,0:T(8,128)(2,1)S(1)}, bf16[256,2048]{1,0:T(8,128)(2,1)S(1)}, u32[]{:S(2)}, u32[]{:S(2)}) %collective-permute-start.7) | collective-permute-done | bytes 1048608 | tf_op jit(solution)/shard_map/ppermute | solution.py:438
  80.4 0.0 copy-start
  80.4 1.4 add_convert_fusion
  81.8 0.0 copy-start.2
  81.8 0.0 copy-start.3
  81.8 0.0 copy-start.4
  81.8 3.8 %all-to-all-start.2 = ((bf16[16,16,2048]{2,1,0:T(8,128)(2,1)}), bf16[16,16,2048]{2,1,0:T(8,128)(2,1)S(1)}, u32[]{:S(2)}, u32[]{:S(2)}) async-start(bf16[16,16,2048]{2,1,0:T(8,128)(2,1)} %bitcast.15), calls=%async_computation.2 | async-start | bytes 2097152 | tf_op jit(solution)/shard_map/all_to_all | solution.py:457
  86.9 0.1 pad_maximum_fusion.1.scal_ref
  87.0 16.2 %all-to-all-done.2 = bf16[16,16,2048]{2,1,0:T(8,128)(2,1)S(1)} async-done(((bf16[16,16,2048]{2,1,0:T(8,128)(2,1)}), bf16[16,16,2048]{2,1,0:T(8,128)(2,1)S(1)}, u32[]{:S(2)}, u32[]{:S(2)}) %all-to-all-start.2) | async-done | bytes 1048608 | tf_op jit(solution)/shard_map/all_to_all | solution.py:457
  103.1 0.0 copy-done
  103.1 1.4 shard_map.200
  104.5 4.2 %all-to-all-start.3 = ((bf16[8,8,2048]{2,1,0:T(8,128)(2,1)}), bf16[8,8,2048]{2,1,0:T(8,128)(2,1)S(1)}, u32[]{:S(2)}, u32[]{:S(2)}) async-start(bf16[8,8,2048]{2,1,0:T(8,128)(2,1)} %shard_map.200), calls=%async_computation.3 | async-start | bytes 524288 | tf_op jit(solution)/shard_map/all_to_all | solution.py:481
  108.7 0.0 all-gather.3.cloned.1.call-done.rows_ref
  108.8 0.0 copy-done.2
  108.8 0.0 copy-done.3
  108.8 0.0 copy-done.4
  108.8 0.0 copy-start.1
  108.8 19.0 %shard_map.194 = (bf16[2048,128]{1,0:T(8,128)(2,1)S(1)}, f32[2048,128]{1,0:T(8,128)S(1)}, bf16[128,256]{1,0:T(8,128)(2,1)S(1)}) custom-call(f32[2]{0:T(128)S(1)} %pad_maximum_fusion.1.scal_ref, s32[1]{0:T(128)} %bitcast.2.head_ref, bf16[2048,2048]{1,0:T(8,128)(2,1)} %all-gather.3.cloned.1.call-done.rows_ref, bf16[2048,128]{1,0:T(8,128)(2,1)} %q_ref.1, ...), custom_call_target="tpu_custom_call" | custom-call | flops 15032385536 | bytes 12058624 | tf_op jit(solution)/shard_map/pallas_call | solution.py:163
  127.8 0.1 collective-permute-start
  127.9 1.0 collective-permute-start.1
  128.9 2.0 %collective-permute-start.2 = (bf16[128,256]{1,0:T(8,128)(2,1)S(1)}, bf16[128,256]{1,0:T(8,128)(2,1)S(1)}, u32[]{:S(2)}, u32[]{:S(2)}) collective-permute-start(bf16[128,256]{1,0:T(8,128)(2,1)S(1)} %get-tuple-element.12.own_ref), channel_id=1, source_target_pairs={{0,48},{16,0},{32,16},{48,32},{1,49},{17,1},{33,17},{49,33},{2,50}... | collective-permute-start | bytes 196616 | tf_op jit(solution)/shard_map/ppermute | solution.py:411
  130.9 2.1 %collective-permute-done.one_ref = bf16[128,256]{1,0:T(8,128)(2,1)S(1)} collective-permute-done((bf16[128,256]{1,0:T(8,128)(2,1)S(1)}, bf16[128,256]{1,0:T(8,128)(2,1)S(1)}, u32[]{:S(2)}, u32[]{:S(2)}) %collective-permute-start) | collective-permute-done | bytes 65568 | tf_op jit(solution)/shard_map/ppermute | solution.py:411
  133.0 0.4 collective-permute-done.1.two_ref
  133.4 0.6 collective-permute-done.2.three_ref
  133.9 0.5 shard_map.195
  134.4 0.1 collective-permute-start.3
  134.5 1.6 collective-permute-start.4
  136.1 1.1 collective-permute-start.5
  137.2 2.7 %collective-permute-done.3.one_ref = bf16[128,256]{1,0:T(8,128)(2,1)S(1)} collective-permute-done((bf16[128,256]{1,0:T(8,128)(2,1)S(1)}, bf16[128,256]{1,0:T(8,128)(2,1)S(1)}, u32[]{:S(2)}, u32[]{:S(2)}) %collective-permute-start.3) | collective-permute-done | bytes 65568 | tf_op jit(solution)/shard_map/ppermute | solution.py:411
  139.9 0.0 collective-permute-done.4.two_ref
  139.9 0.6 collective-permute-done.5.three_ref
  140.5 0.0 copy-done.1
  140.5 1.7 shard_map.196
  142.2 0.0 all-to-all-done.3
  142.2 11.4 %all-to-all-start = ((bf16[16,128,128]{2,1,0:T(8,128)(2,1)}), bf16[16,128,128]{2,1,0:T(8,128)(2,1)S(1)}, u32[]{:S(2)}, u32[]{:S(2)}) async-start(bf16[16,128,128]{2,1,0:T(8,128)(2,1)} %bitcast.7), calls=%async_computation | async-start | bytes 1048576 | tf_op jit(solution)/shard_map/all_to_all | solution.py:477
  153.7 0.7 reduce_sum.32
  154.3 5.7 %all-gather.5.cloned.1.call-done.w_ref = bf16[2048,2048]{1,0:T(8,128)(2,1)} async-done(((bf16[128,2048]{1,0:T(8,128)(2,1)}), bf16[2048,2048]{1,0:T(8,128)(2,1)}) %all-gather.5.cloned.1.call-update) | async-done | bytes 8388624 | tf_op jit(solution)/shard_map/all_gather | solution.py:478
  160.0 11.0 %all-to-all-done.x_ref = bf16[16,128,128]{2,1,0:T(8,128)(2,1)S(1)} async-done(((bf16[16,128,128]{2,1,0:T(8,128)(2,1)}), bf16[16,128,128]{2,1,0:T(8,128)(2,1)S(1)}, u32[]{:S(2)}, u32[]{:S(2)}) %all-to-all-start) | async-done | bytes 524320 | tf_op jit(solution)/shard_map/all_to_all | solution.py:477
  171.0 7.8 %shard_map.197 = bf16[128,2048]{1,0:T(8,128)(2,1)} custom-call(bf16[16,128,128]{2,1,0:T(8,128)(2,1)S(1)} %all-to-all-done.x_ref, bf16[2048,2048]{1,0:T(8,128)(2,1)} %all-gather.5.cloned.1.call-done.w_ref), custom_call_target="tpu_custom_call" | custom-call | flops 1073741824 | bytes 8388608 | tf_op jit(solution)/shard_map/pallas_call | solution.py:267
  (4 shorter events, 0.0 us)
Async XLA Ops:
  7.2 101.6 %all-gather.3.cloned.1.call-start = ((), (), s32[]{:S(2)}) async-start(), calls=%async_computation.4 | async-start | bytes 8912896 | tf_op jit(solution)/shard_map/all_gather | solution.py:451
  39.2 120.8 %all-gather.5.cloned.1.call-start = ((), (), s32[]{:S(2)}) async-start(), calls=%async_computation.5 | async-start | bytes 8912896 | tf_op jit(solution)/shard_map/all_gather | solution.py:478
  61.2 10.4 %collective-permute-start.6 = (bf16[256,2048]{1,0:T(8,128)(2,1)S(1)}, bf16[256,2048]{1,0:T(8,128)(2,1)S(1)}, u32[]{:S(2)}, u32[]{:S(2)}) collective-permute-start(bf16[256,2048]{1,0:T(8,128)(2,1)S(1)} %bitcast.20), channel_id=1, source_target_pairs={{0,1},{1,0},{2,3},{3,2},{4,5},{5,4},{6,7},{7,6},{8,9},{9,8},{10,11... | collective-permute-start | bytes 3145736 | tf_op jit(solution)/shard_map/ppermute | solution.py:438
  77.3 3.1 %collective-permute-start.7 = (bf16[256,2048]{1,0:T(8,128)(2,1)S(1)}, bf16[256,2048]{1,0:T(8,128)(2,1)S(1)}, u32[]{:S(2)}, u32[]{:S(2)}) collective-permute-start(bf16[256,2048]{1,0:T(8,128)(2,1)S(1)} %get-tuple-element.19), channel_id=1, source_target_pairs={{0,1},{1,0},{2,3},{3,2},{4,5},{5,4},{6,7},{7,6},{8,9},{9,8},{10,11... | collective-permute-start | bytes 3145736 | tf_op jit(solution)/shard_map/ppermute | solution.py:438
  80.4 22.7 %copy-start = (bf16[64,2176]{1,0:T(8,128)(2,1)S(1)}, bf16[64,2176]{1,0:T(8,128)(2,1)}, u32[]{:S(2)}) copy-start(bf16[64,2176]{1,0:T(8,128)(2,1)} %all_gather.9.tok_ref.side_ref) | copy-start | bytes 835588
  81.8 27.0 %copy-start.2 = (bf16[2048,16]{0,1:T(8,128)(2,1)S(1)}, bf16[2048,16]{0,1:T(8,128)(2,1)}, u32[]{:S(2)}) copy-start(bf16[2048,16]{0,1:T(8,128)(2,1)} %param.24) | copy-start | bytes 196612
  81.8 27.0 %copy-start.3 = (bf16[2048,16]{0,1:T(8,128)(2,1)S(1)}, bf16[2048,16]{0,1:T(8,128)(2,1)}, u32[]{:S(2)}) copy-start(bf16[2048,16]{0,1:T(8,128)(2,1)} %param.25) | copy-start | bytes 196612
  81.8 27.0 %copy-start.4 = (f32[2048,1]{0,1:T(1,128)S(1)}, f32[2048,1]{0,1:T(1,128)}, u32[]{:S(2)}) copy-start(f32[2048,1]{0,1:T(1,128)} %param.28) | copy-start | bytes 24580
  81.8 21.4 %all-to-all-start.2 = ((bf16[16,16,2048]{2,1,0:T(8,128)(2,1)}), bf16[16,16,2048]{2,1,0:T(8,128)(2,1)S(1)}, u32[]{:S(2)}, u32[]{:S(2)}) async-start(bf16[16,16,2048]{2,1,0:T(8,128)(2,1)} %bitcast.15), calls=%async_computation.2 | async-start | bytes 2097152 | tf_op jit(solution)/shard_map/all_to_all | solution.py:457
  104.5 37.7 %all-to-all-start.3 = ((bf16[8,8,2048]{2,1,0:T(8,128)(2,1)}), bf16[8,8,2048]{2,1,0:T(8,128)(2,1)S(1)}, u32[]{:S(2)}, u32[]{:S(2)}) async-start(bf16[8,8,2048]{2,1,0:T(8,128)(2,1)} %shard_map.200), calls=%async_computation.3 | async-start | bytes 524288 | tf_op jit(solution)/shard_map/all_to_all | solution.py:481
  108.8 31.7 %copy-start.1 = (f32[128]{0:T(128)S(1)}, f32[128]{0:T(128)}, u32[]{:S(2)}) copy-start(f32[128]{0:T(128)} %param.29) | copy-start | bytes 1540
  127.8 5.1 %collective-permute-start = (bf16[128,256]{1,0:T(8,128)(2,1)S(1)}, bf16[128,256]{1,0:T(8,128)(2,1)S(1)}, u32[]{:S(2)}, u32[]{:S(2)}) collective-permute-start(bf16[128,256]{1,0:T(8,128)(2,1)S(1)} %get-tuple-element.12.own_ref), channel_id=1, source_target_pairs={{0,16},{16,32},{32,48},{48,0},{1,17},{17,33},{33,49},{49,1},{2,18}... | collective-permute-start | bytes 196616 | tf_op jit(solution)/shard_map/ppermute | solution.py:411
  127.9 5.4 %collective-permute-start.1 = (bf16[128,256]{1,0:T(8,128)(2,1)S(1)}, bf16[128,256]{1,0:T(8,128)(2,1)S(1)}, u32[]{:S(2)}, u32[]{:S(2)}) collective-permute-start(bf16[128,256]{1,0:T(8,128)(2,1)S(1)} %get-tuple-element.12.own_ref), channel_id=1, source_target_pairs={{0,32},{16,48},{32,0},{48,16},{1,33},{17,49},{33,1},{49,17},{2,34}... | collective-permute-start | bytes 196616 | tf_op jit(solution)/shard_map/ppermute | solution.py:411
  128.9 5.0 %collective-permute-start.2 = (bf16[128,256]{1,0:T(8,128)(2,1)S(1)}, bf16[128,256]{1,0:T(8,128)(2,1)S(1)}, u32[]{:S(2)}, u32[]{:S(2)}) collective-permute-start(bf16[128,256]{1,0:T(8,128)(2,1)S(1)} %get-tuple-element.12.own_ref), channel_id=1, source_target_pairs={{0,48},{16,0},{32,16},{48,32},{1,49},{17,1},{33,17},{49,33},{2,50}... | collective-permute-start | bytes 196616 | tf_op jit(solution)/shard_map/ppermute | solution.py:411
  134.4 5.5 %collective-permute-start.3 = (bf16[128,256]{1,0:T(8,128)(2,1)S(1)}, bf16[128,256]{1,0:T(8,128)(2,1)S(1)}, u32[]{:S(2)}, u32[]{:S(2)}) collective-permute-start(bf16[128,256]{1,0:T(8,128)(2,1)S(1)} %get-tuple-element.13), channel_id=1, source_target_pairs={{0,64},{64,128},{128,192},{192,0},{1,65},{65,129},{129,193},{193,1... | collective-permute-start | bytes 196616 | tf_op jit(solution)/shard_map/ppermute | solution.py:411
  134.5 5.4 %collective-permute-start.4 = (bf16[128,256]{1,0:T(8,128)(2,1)S(1)}, bf16[128,256]{1,0:T(8,128)(2,1)S(1)}, u32[]{:S(2)}, u32[]{:S(2)}) collective-permute-start(bf16[128,256]{1,0:T(8,128)(2,1)S(1)} %get-tuple-element.13), channel_id=1, source_target_pairs={{0,128},{64,192},{128,0},{192,64},{1,129},{65,193},{129,1},{193,65... | collective-permute-start | bytes 196616 | tf_op jit(solution)/shard_map/ppermute | solution.py:411
  136.1 4.4 %collective-permute-start.5 = (bf16[128,256]{1,0:T(8,128)(2,1)S(1)}, bf16[128,256]{1,0:T(8,128)(2,1)S(1)}, u32[]{:S(2)}, u32[]{:S(2)}) collective-permute-start(bf16[128,256]{1,0:T(8,128)(2,1)S(1)} %get-tuple-element.13), channel_id=1, source_target_pairs={{0,192},{64,0},{128,64},{192,128},{1,193},{65,1},{129,65},{193,129... | collective-permute-start | bytes 196616 | tf_op jit(solution)/shard_map/ppermute | solution.py:411
  142.2 28.8 %all-to-all-start = ((bf16[16,128,128]{2,1,0:T(8,128)(2,1)}), bf16[16,128,128]{2,1,0:T(8,128)(2,1)S(1)}, u32[]{:S(2)}, u32[]{:S(2)}) async-start(bf16[16,128,128]{2,1,0:T(8,128)(2,1)} %bitcast.7), calls=%async_computation | async-start | bytes 1048576 | tf_op jit(solution)/shard_map/all_to_all | solution.py:477
Sparse Core Ops, SparseCore 0:
  39.3 61.6 all-gather.2
  102.8 57.1 all-gather.4

commit v3 on v2

--- a/solution.py
+++ b/solution.py
@@ -250,27 +250,61 @@
     )(here, one, two, three, before, g, h, gain.reshape(1, HEAD))
 
 
-def output_kernel(x_ref, w_ref, out_ref, rows):
-    @pl.when(pl.program_id(0) == 0)
-    def _():
-        for h in range(x_ref.shape[0]):
-            rows[:, h * HEAD : (h + 1) * HEAD] = x_ref[h]
-
-    out_ref[...] = mm(rows[...], w_ref[...]).astype(BF16)
+def sum_kernel(*refs):
+    total = refs[0][...].astype(F32)
+    for ref in refs[1:-1]:
+        total = total + ref[...].astype(F32)
+    refs[-1][...] = total.astype(BF16)
+
+
+def sum_parts(parts):
+    vmem = pl.BlockSpec(memory_space=pltpu.VMEM)
+    return pl.pallas_call(
+        sum_kernel,
+        out_shape=jax.ShapeDtypeStruct(parts[0].shape, BF16),
+        in_specs=[vmem] * len(parts),
+        out_specs=vmem,
+        compiler_params=pltpu.CompilerParams(vmem_limit_bytes=4 * 1024 * 1024),
+        cost_estimate=pl.CostEstimate(flops=10**6, bytes_accessed=2 * 9 * parts[0].size, transcendentals=0),
+    )(*parts)
+
+
+def output_kernel(chunks, x_ref, w_ref, out_ref, weights, total, sems):
+    tall = w_ref.shape[0] // chunks
+    copies = [
+        pltpu.make_async_copy(w_ref.at[pl.ds(i * tall, tall)], weights.at[pl.ds(i * tall, tall)], sems.at[i])
+        for i in range(chunks)
+    ]
+    for copy in copies:
+        copy.start()
+    heads = tall // HEAD
+    for i, copy in enumerate(copies):
+        rows = jnp.concatenate([x_ref[i * heads + h] for h in range(heads)], axis=1)
+        copy.wait()
+        part = mm(rows, weights[i * tall : (i + 1) * tall, :])
+        if i == 0:
+            total[...] = part
+        elif i < chunks - 1:
+            total[...] += part
+        else:
+            out_ref[...] = (total[...] + part).astype(BF16)
 
 
 def output_product(by_head, weights):
     depth, width = weights.shape
     count = by_head.shape[1]
-    step = width // 8
-    column = lambda i: (0, i)
-    return pl.pallas_call(
-        output_kernel,
-        grid=(8,),
+    chunks = 4
+    vmem = pl.BlockSpec(memory_space=pltpu.VMEM)
+    return pl.pallas_call(
+        functools.partial(output_kernel, chunks),
         out_shape=jax.ShapeDtypeStruct((count, width), BF16),
-        in_specs=[pl.BlockSpec(by_head.shape, lambda i: (0, 0, 0)), pl.BlockSpec((depth, step), column)],
-        out_specs=pl.BlockSpec((count, step), column),
-        scratch_shapes=[pltpu.VMEM((count, depth), BF16)],
+        in_specs=[vmem, pl.BlockSpec(memory_space=pltpu.HBM)],
+        out_specs=vmem,
+        scratch_shapes=[
+            pltpu.VMEM((depth, width), BF16),
+            pltpu.VMEM((count, width), F32),
+            pltpu.SemaphoreType.DMA((chunks,)),
+        ],
         cost_estimate=pl.CostEstimate(
             flops=2 * count * depth * width, bytes_accessed=2 * depth * width, transcendentals=0
         ),
@@ -322,7 +356,8 @@
     )(tokens)
 
 
-def combine_kernel(experts, side_ref, back_ref, out_ref):
+def combine_kernel(experts, devices, here_ref, side_ref, back_ref, *refs):
+    out_refs, total = refs[:devices], refs[devices]
     side = side_ref[...].astype(F32).T
     first, named, slots = route_columns(side, experts)
     share = [side[2 + k : 3 + k] + side[4 + k : 5 + k] + side[6 + k : 7 + k] for k in range(2)]
@@ -334,28 +369,32 @@
     high = pick.astype(BF16)
     low = (pick - high.astype(F32)).astype(BF16)
     back = back_ref[...]
-    out = mm(high, back, TN) + mm(low, back, TN)
-    out_ref[...] = out.reshape(out_ref.shape).astype(BF16)
-
-
-def combine_tokens(tokens, back, experts):
+    total[...] = (mm(high, back, TN) + mm(low, back, TN)).reshape(total.shape)
+    for k, out_ref in enumerate(out_refs):
+        out_ref[...] = total[(here_ref[0] + k) % len(out_refs)].astype(BF16)
+
+
+def combine_tokens(here, tokens, back, experts):
     count, _ = tokens.shape
     width = back.shape[1]
-    shape = (count // TOKENS, TOKENS, width)
-    return pl.pallas_call(
-        functools.partial(combine_kernel, experts),
+    devices = count // TOKENS
+    piece = (TOKENS, width)
+    return pl.pallas_call(
+        functools.partial(combine_kernel, experts, devices),
         grid=(1,),
-        out_shape=jax.ShapeDtypeStruct(shape, BF16),
+        out_shape=[jax.ShapeDtypeStruct(piece, BF16)] * devices,
         in_specs=[
+            pl.BlockSpec(memory_space=pltpu.SMEM),
             pl.BlockSpec((count, HEAD), lambda i: (0, width // HEAD)),
             pl.BlockSpec(back.shape, lambda i: (0, 0)),
         ],
-        out_specs=pl.BlockSpec(shape, lambda i: (0, 0, 0)),
+        out_specs=[pl.BlockSpec(piece, lambda i: (0, 0))] * devices,
+        scratch_shapes=[pltpu.VMEM((devices, *piece), F32)],
         compiler_params=pltpu.CompilerParams(vmem_limit_bytes=24 * 1024 * 1024),
         cost_estimate=pl.CostEstimate(
             flops=4 * count * back.size, bytes_accessed=2 * back.size + 2 * count * width, transcendentals=0
         ),
-    )(tokens, back)
+    )(here, tokens, back)
 
 
 def expert_kernel(own_ref, other_ref, gate_ref, up_ref, down_ref, mine_ref, theirs_ref, rows, gate, up, down, sems):
@@ -438,6 +477,8 @@
     cross = lambda x: lax.ppermute(x, "tp_1", [(0, 1), (1, 0)])
 
     mix_normed = rms_scale(mixer_input_rows, mixer_norm_gain)
+    mix_rows = lax.all_gather(mix_normed, TP, axis=0, tiled=True)
+
     exp_normed = rms_scale(expert_input_rows, expert_norm_gain)
     parts, rest = [], expert_route_weight
     for _ in range(3):
@@ -446,16 +487,16 @@
         rest = rest - part
     side = jnp.concatenate([routes.astype(BF16)] + parts, axis=1)
     side = jnp.pad(side, ((0, 0), (0, HEAD - side.shape[1])))
-    tokens = lax.all_gather(jnp.concatenate([exp_normed, side], axis=1), "tp_0", axis=0, tiled=True)
-    tokens, mix_normed = lax.optimization_barrier((tokens, mix_normed))
-    mix_rows = lax.all_gather(mix_normed, TP, axis=0, tiled=True)
+    own = jnp.concatenate([exp_normed, side], axis=1)
+    copies = jnp.broadcast_to(own, (lax.axis_size("tp_0"), *own.shape))
+    tokens = lax.all_to_all(copies, "tp_0", split_axis=0, concat_axis=0, tiled=True).reshape(-1, own.shape[1])
     packed = pack_tokens(tokens, experts)
     exp_rows = lax.all_to_all(packed, EP, split_axis=0, concat_axis=0, tiled=True)
     other_rows = cross(exp_rows)
     mine, theirs = expert_sums(exp_rows, other_rows, gate_weight[0].T, up_weight[0].T, down_weight[0])
     pair = (mine.astype(F32) + cross(theirs).astype(F32)).astype(BF16)
     back = lax.all_to_all(pair, EP, split_axis=0, concat_axis=0, tiled=True)
-    combined = combine_tokens(tokens, back, experts)
+    parts = combine_tokens(lax.axis_index("tp_0")[None], tokens, back, experts)
 
     scal = jnp.concatenate([head_decay_speed, largest_write_strength])
     extra = extra_log_decay.reshape(-1, BLOCK)
@@ -478,8 +519,11 @@
     w_whole = lax.all_gather(mixer_output_weight, TP, axis=0, tiled=True)
     mix_out = output_product(by_head, w_whole)
 
-    pieces = lax.all_to_all(combined, "tp_0", split_axis=0, concat_axis=0, tiled=True)
-    exp_out = jnp.sum(pieces.astype(F32), axis=0).astype(BF16)
+    ring = lax.axis_size("tp_0")
+    arrived = [parts[0]]
+    for k in range(1, ring):
+        arrived.append(lax.ppermute(parts[k], "tp_0", [(i, (i + k) % ring) for i in range(ring)]))
+    exp_out = sum_parts(arrived)
     return (mix_out, exp_out)
 
 

time: 187 us -> 158 us (0.84)
  waiting for transfers between devices: 45 us -> 20 us
  starting transfers between devices: 33.8 us -> 39.2 us
  blocking collectives: 44 us -> 40 us
  Pallas kernels: 38.6 us -> 35.6 us
    all_gather x1 -> x0, blocking collectives: 25.3 us -> none  [mixed_step(): lax.all_gather(jnp.concatenate([exp_normed, side], axis=1), 'tp_0', axis=...]
    all_to_all x0 -> x1, blocking collectives: none -> 19.6 us  [mixed_step(): lax.all_to_all(copies, 'tp_0', split_axis=0, concat_axis=0, tiled=True)]
    all_to_all x1, waiting for transfers between devices: 16.2 us -> 0.01 us  [mixed_step(): back = lax.all_to_all(pair, EP, split_axis=0, concat_axis=0, tiled=True)]
    ppermute x0 -> x7, starting transfers between devices: none -> 13.7 us  [mixed_step(): lax.ppermute(parts[k], 'tp_0', [(i, (i + k) % ring) for i in range(ring)])]
    all_to_all x1, waiting for transfers between devices: 11 us -> 0.01 us  [mixed_step(): lax.all_to_all(mixed.reshape(-1, BLOCK, HEAD), TP, split_axis=0, concat_a...]
    ppermute x0 -> x7, waiting for transfers between devices: none -> 10.4 us  [mixed_step(): lax.ppermute(parts[k], 'tp_0', [(i, (i + k) % ring) for i in range(ring)])]
    all_gather x1, waiting for transfers between devices: 5.69 us -> 0.01 us  [mixed_step(): w_whole = lax.all_gather(mixer_output_weight, TP, axis=0, tiled=True)]
    all_to_all x1, starting transfers between devices: 11.4 us -> 6.86 us  [mixed_step(): lax.all_to_all(mixed.reshape(-1, BLOCK, HEAD), TP, split_axis=0, concat_a...]
  transfers between devices with their start and end apart: 13 -> 19, of which waited for: 10 -> 9; matrix products, arithmetic and copies ran while one was open for 1% -> 2% of each run, Pallas kernels for 17% -> 20%
where the time goes in v3:
time: 158 us; the launch traced here: 157 us
  blocking collectives  40 us (25%)
  starting transfers between devices  39.2 us (25%)
  Pallas kernels  35.6 us (23%)
  waiting for transfers between devices  20 us (13%)
  between operations  15.6 us (10%)
  other arithmetic  6.21 us (4%)
    all_to_all x1, blocking collectives, mixed_step(): lax.all_to_all(packed, EP, split_axis=0, concat_axis=0, tiled=True)  20.4 us
    all_to_all x1, blocking collectives, mixed_step(): lax.all_to_all(copies, 'tp_0', split_axis=0, concat_axis=0, tiled=True)  19.6 us
    pallas_call x1, Pallas kernels, span_terms(): pl.pallas_call(functools.partial(span_kernel, chunks), out_shape=(jax.Sha...  19 us
    ppermute x7, starting transfers between devices, mixed_step(): lax.ppermute(parts[k], 'tp_0', [(i, (i + k) % ring) for i in range(ring)])  13.7 us
    ppermute x7, waiting for transfers between devices, mixed_step(): lax.ppermute(parts[k], 'tp_0', [(i, (i + k) % ring) for i in range(ring)])  10.4 us
    ppermute x6, starting transfers between devices, around(): lax.ppermute(x, axis, [(i, (i + k) % size) for i in range(size)])  9.76 us
    all_to_all x1, starting transfers between devices, mixed_step(): lax.all_to_all(mixed.reshape(-1, BLOCK, HEAD), TP, split_axis=0, concat_a...  6.86 us
    pallas_call x1, Pallas kernels, expert_sums(): pl.pallas_call(expert_kernel, out_shape=(out, out), in_specs=[pl.BlockSpe...  5.71 us
  transfers between devices with their start and end apart: 19, of which 9 were waited for; matrix products, arithmetic and copies ran while one was open for 2% of the time, Pallas kernels for 20%

profile of v3, /device:TPU:1, one launch (start us, length us, event | category | flops | bytes accessed | tf_op | source)
XLA Modules:
  0.0 156.7 jit_solution(7417884950038946018)
XLA Ops:
  7.2 0.0 copy-start.8
  7.2 0.0 copy-start.7
  7.2 0.0 copy-start.5
  7.2 0.0 copy-start.6
  7.2 0.0 all-gather.3.cloned.1.call-start
  7.3 1.2 fusion
  8.5 2.0 %fusion.2 = bf16[128,2048]{1,0:T(8,128)(2,1)} fusion(bf16[128,2048]{1,0:T(8,128)(2,1)} %param.19, f32[2048]{0:T(1024)} %param.20, f32[128]{0:T(128)S(1)} %add_rsqrt_fusion.1), kind=kLoop, calls=%fused_computation.5 | loop fusion | flops 1048576 | bytes 1057280 | tf_op jit(solution)/shard_map/convert_element_type | solution.py:41
  10.5 0.0 all-gather.3.cloned.1.call-update
  10.5 0.0 all-gather.5.cloned.1.call-start
  10.6 0.7 all-gather.5.cloned.1.call-update
  11.3 0.0 copy-done.8
  11.4 0.1 copy.22
  11.4 0.0 copy-done.5
  11.4 0.1 fusion.4
  11.6 0.1 fusion.6
  11.7 19.6 %all_to_all.32 = bf16[8,8,2176]{2,1,0:T(8,128)(2,1)} all-to-all(bf16[8,8,2176]{2,1,0:T(8,128)(2,1)S(1)} %broadcast_in_dim.23), channel_id=1, replica_groups=mesh['ep_0'=4,'ep_1'=4,'tp_0'=8,'tp_1'=2] {'tp_0'}, dimensions={0} | all-to-all | bytes 557056 | tf_op jit(solution)/shard_map/all_to_all | solution.py:492
  31.4 2.5 %shard_map.198 = bf16[256,2048]{1,0:T(8,128)(2,1)} custom-call(bf16[64,2176]{1,0:T(8,128)(2,1)} %bitcast.22), custom_call_target="tpu_custom_call" | custom-call | flops 71303168 | bytes 1114112 | tf_op jit(solution)/shard_map/pallas_call | solution.py:350
  33.9 20.4 %all_to_all.33 = bf16[16,16,2048]{2,1,0:T(8,128)(2,1)S(1)} all-to-all(bf16[16,16,2048]{2,1,0:T(8,128)(2,1)} %bitcast.30), channel_id=1, replica_groups=mesh['ep_0'=4,'ep_1'=4,'tp_0'=8,'tp_1'=2] {'ep_0','ep_1'}, dimensions={0} | all-to-all | bytes 2097152 | tf_op jit(solution)/shard_map/all_to_all | solution.py:494
  54.3 4.6 %collective-permute-start.6 = (bf16[256,2048]{1,0:T(8,128)(2,1)S(1)}, bf16[256,2048]{1,0:T(8,128)(2,1)S(1)}, u32[]{:S(2)}, u32[]{:S(2)}) collective-permute-start(bf16[256,2048]{1,0:T(8,128)(2,1)S(1)} %bitcast.24), channel_id=1, source_target_pairs={{0,1},{1,0},{2,3},{3,2},{4,5},{5,4},{6,7},{7,6},{8,9},{9,8},{10,11... | collective-permute-start | bytes 3145736 | tf_op jit(solution)/shard_map/ppermute | solution.py:477
  58.8 2.7 %collective-permute-done.6.other_ref = bf16[256,2048]{1,0:T(8,128)(2,1)S(1)} collective-permute-done((bf16[256,2048]{1,0:T(8,128)(2,1)S(1)}, bf16[256,2048]{1,0:T(8,128)(2,1)S(1)}, u32[]{:S(2)}, u32[]{:S(2)}) %collective-permute-start.6) | collective-permute-done | bytes 1048608 | tf_op jit(solution)/shard_map/ppermute | solution.py:477
  61.5 5.7 %shard_map.199 = (bf16[256,2048]{1,0:T(8,128)(2,1)S(1)}, bf16[256,2048]{1,0:T(8,128)(2,1)S(1)}) custom-call(bf16[256,2048]{1,0:T(8,128)(2,1)S(1)} %bitcast.25, bf16[256,2048]{1,0:T(8,128)(2,1)S(1)} %collective-permute-done.6.other_ref, bf16[448,2048]{1,0:T(8,128)(2,1)} %bitcast.31, bf16[448,2048]{1,0:T(8,128)(2,1)} %bitcast.32, bf16[448,2048]{1,0:T(8,128)(2,1)} %bitcast.33), custom_call_target="tpu_custom_call" | custom-call | flops 2818572288 | bytes 9699328 | tf_op jit(solution)/shard_map/pallas_call | solution.py:427
  67.2 0.4 collective-permute-start.7
  68.9 0.1 pad_maximum_fusion.1.scal_ref
  69.0 1.3 collective-permute-done.7
  70.3 2.6 %add_convert_fusion = bf16[256,2048]{1,0:T(8,128)(2,1)} fusion(bf16[256,2048]{1,0:T(8,128)(2,1)} %collective-permute-done.7, bf16[256,2048]{1,0:T(8,128)(2,1)S(1)} %get-tuple-element.22), kind=kLoop, calls=%fused_computation | loop fusion | flops 2097152 | bytes 3145728 | tf_op jit(solution)/shard_map/convert_element_type | solution.py:497
  72.9 3.8 %all-to-all-start.3 = ((bf16[16,16,2048]{2,1,0:T(8,128)(2,1)}), bf16[16,16,2048]{2,1,0:T(8,128)(2,1)S(1)}, u32[]{:S(2)}, u32[]{:S(2)}) async-start(bf16[16,16,2048]{2,1,0:T(8,128)(2,1)} %bitcast.17), calls=%async_computation.3 | async-start | bytes 2097152 | tf_op jit(solution)/shard_map/all_to_all | solution.py:498
  76.7 0.0 all-gather.3.cloned.1.call-done.rows_ref
  76.8 0.0 copy-start.1
  76.8 19.0 %shard_map.194 = (bf16[2048,128]{1,0:T(8,128)(2,1)S(1)}, f32[2048,128]{1,0:T(8,128)S(1)}, bf16[128,256]{1,0:T(8,128)(2,1)S(1)}) custom-call(f32[2]{0:T(128)S(1)} %pad_maximum_fusion.1.scal_ref, s32[1]{0:T(128)} %bitcast.2.head_ref, bf16[2048,2048]{1,0:T(8,128)(2,1)} %all-gather.3.cloned.1.call-done.rows_ref, bf16[2048,128]{1,0:T(8,128)(2,1)} %q_ref.1, ...), custom_call_target="tpu_custom_call" | custom-call | flops 15032385536 | bytes 12058624 | tf_op jit(solution)/shard_map/pallas_call | solution.py:163
  95.9 1.1 collective-permute-start
  97.0 2.4 %collective-permute-start.1 = (bf16[128,256]{1,0:T(8,128)(2,1)S(1)}, bf16[128,256]{1,0:T(8,128)(2,1)S(1)}, u32[]{:S(2)}, u32[]{:S(2)}) collective-permute-start(bf16[128,256]{1,0:T(8,128)(2,1)S(1)} %get-tuple-element.17.own_ref), channel_id=1, source_target_pairs={{0,32},{16,48},{32,0},{48,16},{1,33},{17,49},{33,1},{49,17},{2,34}... | collective-permute-start | bytes 196616 | tf_op jit(solution)/shard_map/ppermute | solution.py:450
  99.4 1.2 collective-permute-start.2
  100.6 0.1 collective-permute-done.one_ref
  100.7 1.5 collective-permute-done.1.two_ref
  102.2 0.8 collective-permute-done.2.three_ref
  103.0 0.5 shard_map.195
  103.5 1.4 collective-permute-start.3
  104.9 2.4 %collective-permute-start.4 = (bf16[128,256]{1,0:T(8,128)(2,1)S(1)}, bf16[128,256]{1,0:T(8,128)(2,1)S(1)}, u32[]{:S(2)}, u32[]{:S(2)}) collective-permute-start(bf16[128,256]{1,0:T(8,128)(2,1)S(1)} %get-tuple-element.18), channel_id=1, source_target_pairs={{0,128},{64,192},{128,0},{192,64},{1,129},{65,193},{129,1},{193,65... | collective-permute-start | bytes 196616 | tf_op jit(solution)/shard_map/ppermute | solution.py:450
  107.4 1.2 collective-permute-start.5
  108.5 0.0 collective-permute-done.3.one_ref
  108.5 1.3 collective-permute-done.4.two_ref
  109.8 1.2 collective-permute-done.5.three_ref
  111.0 1.7 %shard_map.196 = bf16[2048,128]{1,0:T(8,128)(2,1)} custom-call(s32[1]{0:T(128)} %bitcast.here_ref, bf16[128,256]{1,0:T(8,128)(2,1)S(1)} %collective-permute-done.3.one_ref, bf16[128,256]{1,0:T(8,128)(2,1)S(1)} %collective-permute-done.4.two_ref, bf16[128,256]{1,0:T(8,128)(2,1)S(1)} %collective-permute-done.5.three_ref, ...), custom_call_target="tpu_custom_call" | custom-call | flops 67108864 | bytes 2097152 | tf_op jit(solution)/shard_map/pallas_call | solution.py:242
  112.7 0.0 all-to-all-done.3
  112.7 6.9 %all-to-all-start = ((bf16[16,128,128]{2,1,0:T(8,128)(2,1)}), bf16[16,128,128]{2,1,0:T(8,128)(2,1)S(1)}, u32[]{:S(2)}, u32[]{:S(2)}) async-start(bf16[16,128,128]{2,1,0:T(8,128)(2,1)} %bitcast.7), calls=%async_computation | async-start | bytes 1048576 | tf_op jit(solution)/shard_map/all_to_all | solution.py:518
  119.6 0.0 copy-done
  119.6 0.7 shard_map.200
  120.3 1.7 %collective-permute-start.8 = (bf16[8,2048]{1,0:T(8,128)(2,1)S(1)}, bf16[8,2048]{1,0:T(8,128)(2,1)S(1)}, u32[]{:S(2)}, u32[]{:S(2)}) collective-permute-start(bf16[8,2048]{1,0:T(8,128)(2,1)S(1)} %get-tuple-element.25), channel_id=1, source_target_pairs={{0,2},{2,4},{4,6},{6,8},{8,10},{10,12},{12,14},{14,0},{1,3},{3,5},... | collective-permute-start | bytes 98312 | tf_op jit(solution)/shard_map/ppermute | solution.py:525
  122.0 2.1 %collective-permute-start.9 = (bf16[8,2048]{1,0:T(8,128)(2,1)S(1)}, bf16[8,2048]{1,0:T(8,128)(2,1)S(1)}, u32[]{:S(2)}, u32[]{:S(2)}) collective-permute-start(bf16[8,2048]{1,0:T(8,128)(2,1)S(1)} %get-tuple-element.26), channel_id=1, source_target_pairs={{0,4},{2,6},{4,8},{6,10},{8,12},{10,14},{12,0},{14,2},{1,5},{3,7},... | collective-permute-start | bytes 98312 | tf_op jit(solution)/shard_map/ppermute | solution.py:525
  124.1 2.4 %collective-permute-start.10 = (bf16[8,2048]{1,0:T(8,128)(2,1)S(1)}, bf16[8,2048]{1,0:T(8,128)(2,1)S(1)}, u32[]{:S(2)}, u32[]{:S(2)}) collective-permute-start(bf16[8,2048]{1,0:T(8,128)(2,1)S(1)} %get-tuple-element.27), channel_id=1, source_target_pairs={{0,6},{2,8},{4,10},{6,12},{8,14},{10,0},{12,2},{14,4},{1,7},{3,9},... | collective-permute-start | bytes 98312 | tf_op jit(solution)/shard_map/ppermute | solution.py:525
  126.5 2.1 %collective-permute-start.11 = (bf16[8,2048]{1,0:T(8,128)(2,1)S(1)}, bf16[8,2048]{1,0:T(8,128)(2,1)S(1)}, u32[]{:S(2)}, u32[]{:S(2)}) collective-permute-start(bf16[8,2048]{1,0:T(8,128)(2,1)S(1)} %get-tuple-element.28), channel_id=1, source_target_pairs={{0,8},{2,10},{4,12},{6,14},{8,0},{10,2},{12,4},{14,6},{1,9},{3,11}... | collective-permute-start | bytes 98312 | tf_op jit(solution)/shard_map/ppermute | solution.py:525
  128.6 2.4 %collective-permute-start.12 = (bf16[8,2048]{1,0:T(8,128)(2,1)S(1)}, bf16[8,2048]{1,0:T(8,128)(2,1)S(1)}, u32[]{:S(2)}, u32[]{:S(2)}) collective-permute-start(bf16[8,2048]{1,0:T(8,128)(2,1)S(1)} %get-tuple-element.29), channel_id=1, source_target_pairs={{0,10},{2,12},{4,14},{6,0},{8,2},{10,4},{12,6},{14,8},{1,11},{3,13... | collective-permute-start | bytes 98312 | tf_op jit(solution)/shard_map/ppermute | solution.py:525
  131.0 7.5 %collective-permute-done.8.refs_1_ = bf16[8,2048]{1,0:T(8,128)(2,1)S(1)} collective-permute-done((bf16[8,2048]{1,0:T(8,128)(2,1)S(1)}, bf16[8,2048]{1,0:T(8,128)(2,1)S(1)}, u32[]{:S(2)}, u32[]{:S(2)}) %collective-permute-start.8) | collective-permute-done | bytes 32800 | tf_op jit(solution)/shard_map/ppermute | solution.py:525
  138.4 1.9 %collective-permute-start.13 = (bf16[8,2048]{1,0:T(8,128)(2,1)S(1)}, bf16[8,2048]{1,0:T(8,128)(2,1)S(1)}, u32[]{:S(2)}, u32[]{:S(2)}) collective-permute-start(bf16[8,2048]{1,0:T(8,128)(2,1)S(1)} %get-tuple-element.30), channel_id=1, source_target_pairs={{0,12},{2,14},{4,0},{6,2},{8,4},{10,6},{12,8},{14,10},{1,13},{3,15... | collective-permute-start | bytes 98312 | tf_op jit(solution)/shard_map/ppermute | solution.py:525
  140.4 0.0 collective-permute-done.9.refs_2_
  140.4 1.2 collective-permute-start.14
  141.6 0.0 collective-permute-done.10.refs_3_
  141.6 2.9 %collective-permute-done.11.refs_4_ = bf16[8,2048]{1,0:T(8,128)(2,1)S(1)} collective-permute-done((bf16[8,2048]{1,0:T(8,128)(2,1)S(1)}, bf16[8,2048]{1,0:T(8,128)(2,1)S(1)}, u32[]{:S(2)}, u32[]{:S(2)}) %collective-permute-start.11) | collective-permute-done | bytes 32800 | tf_op jit(solution)/shard_map/ppermute | solution.py:525
  144.5 0.0 collective-permute-done.12.refs_5_
  144.5 0.0 collective-permute-done.13.refs_6_
  144.5 0.0 collective-permute-done.14.refs_7_
  144.5 0.7 shard_map.201
  145.1 0.0 all-to-all-done.x_ref
  145.1 4.7 %shard_map.197 = bf16[128,2048]{1,0:T(8,128)(2,1)} custom-call(bf16[16,128,128]{2,1,0:T(8,128)(2,1)S(1)} %all-to-all-done.x_ref, bf16[2048,2048]{1,0:T(8,128)(2,1)} %all-gather.5.cloned.1.call-done.w_ref), custom_call_target="tpu_custom_call" | custom-call | flops 1073741824 | bytes 8388608 | tf_op jit(solution)/shard_map/pallas_call | solution.py:298
  (18 shorter events, 0.1 us)
Async XLA Ops:
  7.2 4.1 %copy-start.8 = (s32[8,2]{0,1:T(2,128)S(1)}, s32[8,2]{0,1:T(2,128)}, u32[]{:S(2)}) copy-start(s32[8,2]{0,1:T(2,128)} %param.33) | copy-start | bytes 196
  7.2 4.1 %copy-start.7 = (f32[8,2]{0,1:T(2,128)S(1)}, f32[8,2]{0,1:T(2,128)}, u32[]{:S(2)}) copy-start(f32[8,2]{0,1:T(2,128)} %param.34) | copy-start | bytes 196
  7.2 4.3 %copy-start.5 = (bf16[8,2048]{1,0:T(8,128)(2,1)S(1)}, bf16[8,2048]{1,0:T(8,128)(2,1)}, u32[]{:S(2)}) copy-start(bf16[8,2048]{1,0:T(8,128)(2,1)} %param.31) | copy-start | bytes 98308
  7.2 4.4 %copy-start.6 = (f32[2048]{0:T(1024)S(1)}, f32[2048]{0:T(1024)}, u32[]{:S(2)}) copy-start(f32[2048]{0:T(1024)} %param.32) | copy-start | bytes 24580
  7.2 69.6 %all-gather.3.cloned.1.call-start = ((), (), s32[]{:S(2)}) async-start(), calls=%async_computation.4 | async-start | bytes 8912896 | tf_op jit(solution)/shard_map/all_gather | solution.py:480
  10.5 134.6 %all-gather.5.cloned.1.call-start = ((), (), s32[]{:S(2)}) async-start(), calls=%async_computation.5 | async-start | bytes 8912896 | tf_op jit(solution)/shard_map/all_gather | solution.py:519
  54.3 7.2 %collective-permute-start.6 = (bf16[256,2048]{1,0:T(8,128)(2,1)S(1)}, bf16[256,2048]{1,0:T(8,128)(2,1)S(1)}, u32[]{:S(2)}, u32[]{:S(2)}) collective-permute-start(bf16[256,2048]{1,0:T(8,128)(2,1)S(1)} %bitcast.24), channel_id=1, source_target_pairs={{0,1},{1,0},{2,3},{3,2},{4,5},{5,4},{6,7},{7,6},{8,9},{9,8},{10,11... | collective-permute-start | bytes 3145736 | tf_op jit(solution)/shard_map/ppermute | solution.py:477
  67.2 3.1 %collective-permute-start.7 = (bf16[256,2048]{1,0:T(8,128)(2,1)S(1)}, bf16[256,2048]{1,0:T(8,128)(2,1)}, u32[]{:S(2)}, u32[]{:S(2)}) collective-permute-start(bf16[256,2048]{1,0:T(8,128)(2,1)S(1)} %get-tuple-element.23), channel_id=1, source_target_pairs={{0,1},{1,0},{2,3},{3,2},{4,5},{5,4},{6,7},{7,6},{8,9},{9,8},{10,11... | collective-permute-start | bytes 3145736 | tf_op jit(solution)/shard_map/ppermute | solution.py:477
  70.3 6.5 %copy-start.2 = (bf16[2048,16]{0,1:T(8,128)(2,1)S(1)}, bf16[2048,16]{0,1:T(8,128)(2,1)}, u32[]{:S(2)}) copy-start(bf16[2048,16]{0,1:T(8,128)(2,1)} %param.24) | copy-start | bytes 196612
  70.3 6.5 %copy-start.3 = (bf16[2048,16]{0,1:T(8,128)(2,1)S(1)}, bf16[2048,16]{0,1:T(8,128)(2,1)}, u32[]{:S(2)}) copy-start(bf16[2048,16]{0,1:T(8,128)(2,1)} %param.25) | copy-start | bytes 196612
  70.3 6.5 %copy-start.4 = (f32[2048,1]{0,1:T(1,128)S(1)}, f32[2048,1]{0,1:T(1,128)}, u32[]{:S(2)}) copy-start(f32[2048,1]{0,1:T(1,128)} %param.28) | copy-start | bytes 24580
  72.9 39.8 %all-to-all-start.3 = ((bf16[16,16,2048]{2,1,0:T(8,128)(2,1)}), bf16[16,16,2048]{2,1,0:T(8,128)(2,1)S(1)}, u32[]{:S(2)}, u32[]{:S(2)}) async-start(bf16[16,16,2048]{2,1,0:T(8,128)(2,1)} %bitcast.17), calls=%async_computation.3 | async-start | bytes 2097152 | tf_op jit(solution)/shard_map/all_to_all | solution.py:498
  76.8 34.2 %copy-start.1 = (f32[128]{0:T(128)S(1)}, f32[128]{0:T(128)}, u32[]{:S(2)}) copy-start(f32[128]{0:T(128)} %param.29) | copy-start | bytes 1540
  95.9 23.7 %copy-start = (bf16[8,8,2176]{2,1,0:T(8,128)(2,1)S(1)}, bf16[8,8,2176]{2,1,0:T(8,128)(2,1)}, u32[]{:S(2)}) copy-start(bf16[8,8,2176]{2,1,0:T(8,128)(2,1)} %all_to_all.32) | copy-start | bytes 835588
  95.9 4.8 %collective-permute-start = (bf16[128,256]{1,0:T(8,128)(2,1)S(1)}, bf16[128,256]{1,0:T(8,128)(2,1)S(1)}, u32[]{:S(2)}, u32[]{:S(2)}) collective-permute-start(bf16[128,256]{1,0:T(8,128)(2,1)S(1)} %get-tuple-element.17.own_ref), channel_id=1, source_target_pairs={{0,16},{16,32},{32,48},{48,0},{1,17},{17,33},{33,49},{49,1},{2,18}... | collective-permute-start | bytes 196616 | tf_op jit(solution)/shard_map/ppermute | solution.py:450
  97.0 5.2 %collective-permute-start.1 = (bf16[128,256]{1,0:T(8,128)(2,1)S(1)}, bf16[128,256]{1,0:T(8,128)(2,1)S(1)}, u32[]{:S(2)}, u32[]{:S(2)}) collective-permute-start(bf16[128,256]{1,0:T(8,128)(2,1)S(1)} %get-tuple-element.17.own_ref), channel_id=1, source_target_pairs={{0,32},{16,48},{32,0},{48,16},{1,33},{17,49},{33,1},{49,17},{2,34}... | collective-permute-start | bytes 196616 | tf_op jit(solution)/shard_map/ppermute | solution.py:450
  99.4 3.6 %collective-permute-start.2 = (bf16[128,256]{1,0:T(8,128)(2,1)S(1)}, bf16[128,256]{1,0:T(8,128)(2,1)S(1)}, u32[]{:S(2)}, u32[]{:S(2)}) collective-permute-start(bf16[128,256]{1,0:T(8,128)(2,1)S(1)} %get-tuple-element.17.own_ref), channel_id=1, source_target_pairs={{0,48},{16,0},{32,16},{48,32},{1,49},{17,1},{33,17},{49,33},{2,50}... | collective-permute-start | bytes 196616 | tf_op jit(solution)/shard_map/ppermute | solution.py:450
  103.5 5.0 %collective-permute-start.3 = (bf16[128,256]{1,0:T(8,128)(2,1)S(1)}, bf16[128,256]{1,0:T(8,128)(2,1)S(1)}, u32[]{:S(2)}, u32[]{:S(2)}) collective-permute-start(bf16[128,256]{1,0:T(8,128)(2,1)S(1)} %get-tuple-element.18), channel_id=1, source_target_pairs={{0,64},{64,128},{128,192},{192,0},{1,65},{65,129},{129,193},{193,1... | collective-permute-start | bytes 196616 | tf_op jit(solution)/shard_map/ppermute | solution.py:450
  104.9 4.9 %collective-permute-start.4 = (bf16[128,256]{1,0:T(8,128)(2,1)S(1)}, bf16[128,256]{1,0:T(8,128)(2,1)S(1)}, u32[]{:S(2)}, u32[]{:S(2)}) collective-permute-start(bf16[128,256]{1,0:T(8,128)(2,1)S(1)} %get-tuple-element.18), channel_id=1, source_target_pairs={{0,128},{64,192},{128,0},{192,64},{1,129},{65,193},{129,1},{193,65... | collective-permute-start | bytes 196616 | tf_op jit(solution)/shard_map/ppermute | solution.py:450
  107.4 3.7 %collective-permute-start.5 = (bf16[128,256]{1,0:T(8,128)(2,1)S(1)}, bf16[128,256]{1,0:T(8,128)(2,1)S(1)}, u32[]{:S(2)}, u32[]{:S(2)}) collective-permute-start(bf16[128,256]{1,0:T(8,128)(2,1)S(1)} %get-tuple-element.18), channel_id=1, source_target_pairs={{0,192},{64,0},{128,64},{192,128},{1,193},{65,1},{129,65},{193,129... | collective-permute-start | bytes 196616 | tf_op jit(solution)/shard_map/ppermute | solution.py:450
  112.7 32.4 %all-to-all-start = ((bf16[16,128,128]{2,1,0:T(8,128)(2,1)}), bf16[16,128,128]{2,1,0:T(8,128)(2,1)S(1)}, u32[]{:S(2)}, u32[]{:S(2)}) async-start(bf16[16,128,128]{2,1,0:T(8,128)(2,1)} %bitcast.7), calls=%async_computation | async-start | bytes 1048576 | tf_op jit(solution)/shard_map/all_to_all | solution.py:518
  120.3 18.1 %collective-permute-start.8 = (bf16[8,2048]{1,0:T(8,128)(2,1)S(1)}, bf16[8,2048]{1,0:T(8,128)(2,1)S(1)}, u32[]{:S(2)}, u32[]{:S(2)}) collective-permute-start(bf16[8,2048]{1,0:T(8,128)(2,1)S(1)} %get-tuple-element.25), channel_id=1, source_target_pairs={{0,2},{2,4},{4,6},{6,8},{8,10},{10,12},{12,14},{14,0},{1,3},{3,5},... | collective-permute-start | bytes 98312 | tf_op jit(solution)/shard_map/ppermute | solution.py:525
  122.0 18.4 %collective-permute-start.9 = (bf16[8,2048]{1,0:T(8,128)(2,1)S(1)}, bf16[8,2048]{1,0:T(8,128)(2,1)S(1)}, u32[]{:S(2)}, u32[]{:S(2)}) collective-permute-start(bf16[8,2048]{1,0:T(8,128)(2,1)S(1)} %get-tuple-element.26), channel_id=1, source_target_pairs={{0,4},{2,6},{4,8},{6,10},{8,12},{10,14},{12,0},{14,2},{1,5},{3,7},... | collective-permute-start | bytes 98312 | tf_op jit(solution)/shard_map/ppermute | solution.py:525
  124.1 17.5 %collective-permute-start.10 = (bf16[8,2048]{1,0:T(8,128)(2,1)S(1)}, bf16[8,2048]{1,0:T(8,128)(2,1)S(1)}, u32[]{:S(2)}, u32[]{:S(2)}) collective-permute-start(bf16[8,2048]{1,0:T(8,128)(2,1)S(1)} %get-tuple-element.27), channel_id=1, source_target_pairs={{0,6},{2,8},{4,10},{6,12},{8,14},{10,0},{12,2},{14,4},{1,7},{3,9},... | collective-permute-start | bytes 98312 | tf_op jit(solution)/shard_map/ppermute | solution.py:525
  126.5 18.0 %collective-permute-start.11 = (bf16[8,2048]{1,0:T(8,128)(2,1)S(1)}, bf16[8,2048]{1,0:T(8,128)(2,1)S(1)}, u32[]{:S(2)}, u32[]{:S(2)}) collective-permute-start(bf16[8,2048]{1,0:T(8,128)(2,1)S(1)} %get-tuple-element.28), channel_id=1, source_target_pairs={{0,8},{2,10},{4,12},{6,14},{8,0},{10,2},{12,4},{14,6},{1,9},{3,11}... | collective-permute-start | bytes 98312 | tf_op jit(solution)/shard_map/ppermute | solution.py:525
  128.6 15.9 %collective-permute-start.12 = (bf16[8,2048]{1,0:T(8,128)(2,1)S(1)}, bf16[8,2048]{1,0:T(8,128)(2,1)S(1)}, u32[]{:S(2)}, u32[]{:S(2)}) collective-permute-start(bf16[8,2048]{1,0:T(8,128)(2,1)S(1)} %get-tuple-element.29), channel_id=1, source_target_pairs={{0,10},{2,12},{4,14},{6,0},{8,2},{10,4},{12,6},{14,8},{1,11},{3,13... | collective-permute-start | bytes 98312 | tf_op jit(solution)/shard_map/ppermute | solution.py:525
  138.4 6.0 %collective-permute-start.13 = (bf16[8,2048]{1,0:T(8,128)(2,1)S(1)}, bf16[8,2048]{1,0:T(8,128)(2,1)S(1)}, u32[]{:S(2)}, u32[]{:S(2)}) collective-permute-start(bf16[8,2048]{1,0:T(8,128)(2,1)S(1)} %get-tuple-element.30), channel_id=1, source_target_pairs={{0,12},{2,14},{4,0},{6,2},{8,4},{10,6},{12,8},{14,10},{1,13},{3,15... | collective-permute-start | bytes 98312 | tf_op jit(solution)/shard_map/ppermute | solution.py:525
  140.4 4.1 %collective-permute-start.14 = (bf16[8,2048]{1,0:T(8,128)(2,1)S(1)}, bf16[8,2048]{1,0:T(8,128)(2,1)S(1)}, u32[]{:S(2)}, u32[]{:S(2)}) collective-permute-start(bf16[8,2048]{1,0:T(8,128)(2,1)S(1)} %get-tuple-element.31), channel_id=1, source_target_pairs={{0,14},{2,0},{4,2},{6,4},{8,6},{10,8},{12,10},{14,12},{1,15},{3,1}... | collective-permute-start | bytes 98312 | tf_op jit(solution)/shard_map/ppermute | solution.py:525
Sparse Core Ops, SparseCore 0:
  10.7 61.2 all-gather.2
  73.8 61.7 all-gather.4

commit v4 on v3

--- a/solution.py
+++ b/solution.py
@@ -269,7 +269,7 @@
     )(*parts)
 
 
-def output_kernel(chunks, x_ref, w_ref, out_ref, weights, total, sems):
+def output_kernel(chunks, core_ref, x_ref, w_ref, mine_ref, theirs_ref, weights, total, sems):
     tall = w_ref.shape[0] // chunks
     copies = [
         pltpu.make_async_copy(w_ref.at[pl.ds(i * tall, tall)], weights.at[pl.ds(i * tall, tall)], sems.at[i])
@@ -278,8 +278,12 @@
     for copy in copies:
         copy.start()
     heads = tall // HEAD
+    core = core_ref[0]
+    owners = [pl.ds(pl.multiple_of(owner * BLOCK, BLOCK), BLOCK) for owner in (core, 1 - core)]
     for i, copy in enumerate(copies):
-        rows = jnp.concatenate([x_ref[i * heads + h] for h in range(heads)], axis=1)
+        rows = jnp.concatenate(
+            [jnp.concatenate([x_ref[i * heads + h, at, :] for h in range(heads)], axis=1) for at in owners], axis=0
+        )
         copy.wait()
         part = mm(rows, weights[i * tall : (i + 1) * tall, :])
         if i == 0:
@@ -287,19 +291,21 @@
         elif i < chunks - 1:
             total[...] += part
         else:
-            out_ref[...] = (total[...] + part).astype(BF16)
-
-
-def output_product(by_head, weights):
+            whole = total[...] + part
+            mine_ref[...] = whole[:BLOCK]
+            theirs_ref[...] = whole[BLOCK:].astype(BF16)
+
+
+def output_product(core, by_head, weights):
     depth, width = weights.shape
     count = by_head.shape[1]
     chunks = 4
     vmem = pl.BlockSpec(memory_space=pltpu.VMEM)
     return pl.pallas_call(
         functools.partial(output_kernel, chunks),
-        out_shape=jax.ShapeDtypeStruct((count, width), BF16),
-        in_specs=[vmem, pl.BlockSpec(memory_space=pltpu.HBM)],
-        out_specs=vmem,
+        out_shape=(jax.ShapeDtypeStruct((BLOCK, width), F32), jax.ShapeDtypeStruct((BLOCK, width), BF16)),
+        in_specs=[pl.BlockSpec(memory_space=pltpu.SMEM), vmem, pl.BlockSpec(memory_space=pltpu.HBM)],
+        out_specs=(vmem, vmem),
         scratch_shapes=[
             pltpu.VMEM((depth, width), BF16),
             pltpu.VMEM((count, width), F32),
@@ -309,7 +315,23 @@
             flops=2 * count * depth * width, bytes_accessed=2 * depth * width, transcendentals=0
         ),
         compiler_params=pltpu.CompilerParams(vmem_limit_bytes=32 * 1024 * 1024),
-    )(by_head, pltpu.with_memory_space_constraint(weights, pltpu.HBM))
+    )(core, by_head, pltpu.with_memory_space_constraint(weights, pltpu.HBM))
+
+
+def join_kernel(mine_ref, theirs_ref, out_ref):
+    out_ref[...] = (mine_ref[...].astype(F32) + theirs_ref[...].astype(F32)).astype(BF16)
+
+
+def join_halves(mine, theirs):
+    vmem = pl.BlockSpec(memory_space=pltpu.VMEM)
+    return pl.pallas_call(
+        join_kernel,
+        out_shape=jax.ShapeDtypeStruct(mine.shape, BF16),
+        in_specs=[vmem, vmem],
+        out_specs=vmem,
+        compiler_params=pltpu.CompilerParams(vmem_limit_bytes=8 * 1024 * 1024),
+        cost_estimate=pl.CostEstimate(flops=10**6, bytes_accessed=8 * mine.size, transcendentals=0),
+    )(mine, theirs)
 
 
 def route_columns(side, experts):
@@ -473,6 +495,7 @@
     down_weight,
 ):
     head = lax.axis_index(TP)
+    core = lax.axis_index("tp_1")
     experts = gate_weight.shape[0] * lax.axis_size(EP)
     cross = lambda x: lax.ppermute(x, "tp_1", [(0, 1), (1, 0)])
 
@@ -494,7 +517,7 @@
     exp_rows = lax.all_to_all(packed, EP, split_axis=0, concat_axis=0, tiled=True)
     other_rows = cross(exp_rows)
     mine, theirs = expert_sums(exp_rows, other_rows, gate_weight[0].T, up_weight[0].T, down_weight[0])
-    pair = (mine.astype(F32) + cross(theirs).astype(F32)).astype(BF16)
+    pair = join_halves(mine, cross(theirs))
     back = lax.all_to_all(pair, EP, split_axis=0, concat_axis=0, tiled=True)
     parts = combine_tokens(lax.axis_index("tp_0")[None], tokens, back, experts)
 
@@ -515,11 +538,15 @@
     before, total = compose_row(lax.axis_index("ep_1")[None], span, *row_pieces)
     mixed = apply_memory(lax.axis_index("ep_0")[None], *around(total, "ep_0"), before, gains, local, head_norm_gain)
 
-    by_head = lax.all_to_all(mixed.reshape(-1, BLOCK, HEAD), TP, split_axis=0, concat_axis=0, tiled=True)
-    w_whole = lax.all_gather(mixer_output_weight, TP, axis=0, tiled=True)
-    mix_out = output_product(by_head, w_whole)
-
     ring = lax.axis_size("tp_0")
+    by_head = lax.all_to_all(
+        mixed.reshape(ring, 2 * BLOCK, HEAD), "tp_0", split_axis=0, concat_axis=0, tiled=True
+    )
+    w_own = lax.all_gather(mixer_output_weight, "tp_0", axis=0, tiled=True)
+    mix_mine, mix_theirs = output_product(core[None], by_head, w_own)
+    mix_crossed = cross(mix_theirs)
+    mix_out = join_halves(mix_mine, mix_crossed)
+
     arrived = [parts[0]]
     for k in range(1, ring):
         arrived.append(lax.ppermute(parts[k], "tp_0", [(i, (i + k) % ring) for i in range(ring)]))

time: 158 us -> 188 us (1.19); the launches traced: 157 us -> 185 us
  waiting for transfers between devices: 20 us -> 58 us
  blocking collectives: 40 us -> 19.6 us
  starting transfers between devices: 39.2 us -> 46.8 us
  local copies, waits for them, and re-layouts: 0.14 us -> 4.24 us
  other arithmetic: 6.21 us -> 3.59 us
    all_to_all x1 -> x2, waiting for transfers between devices: 0.01 us -> 28 us  [the longest x1 15.6 us: mixed_step(): lax.all_to_all(mixed.reshape(ring, 2 * BLOCK, HEAD), 'tp_0', split_axis=0...]
    all_to_all x1 -> x0, blocking collectives: 20.4 us -> none  [mixed_step(): lax.all_to_all(packed, EP, split_axis=0, concat_axis=0, tiled=True)]
    all_gather x1, waiting for transfers between devices: 0.02 us -> 12.7 us  [mixed_step(): mix_rows = lax.all_gather(mix_normed, TP, axis=0, tiled=True)]
    all_to_all x1, waiting for transfers between devices: 0.01 us -> 10.2 us  [mixed_step(): back = lax.all_to_all(pair, EP, split_axis=0, concat_axis=0, tiled=True)]
    ppermute x7, waiting for transfers between devices: 10.4 us -> 3.91 us  [mixed_step(): lax.ppermute(parts[k], 'tp_0', [(i, (i + k) % ring) for i in range(ring)])]
    all_to_all x1 -> x2, starting transfers between devices: 6.86 us -> 11.1 us  [the longest x1 6.78 us: mixed_step(): lax.all_to_all(packed, EP, split_axis=0, concat_axis=0, tiled=True)]
    unnamed x19 -> x27, local copies, waits for them, and re-layouts: 0.12 us -> 4.22 us
    ppermute x2 -> x3, waiting for transfers between devices: 3.96 us -> 0.01 us  [mixed_step(): cross = lambda x: lax.ppermute(x, 'tp_1', [(0, 1), (1, 0)])]
  transfers between devices with their start and end apart: 19 -> 21, of which waited for: 9 -> 9; matrix products, arithmetic and copies ran while one was open for 2% -> 0% of each run, Pallas kernels for 20% -> 20%
where the time goes in v4:
time: 188 us; the launch traced here: 185 us
  waiting for transfers between devices  58 us (31%)
  starting transfers between devices  46.8 us (25%)
  Pallas kernels  37 us (20%)
  blocking collectives  19.6 us (10%)
  between operations  15.6 us (8%)
  local copies, waits for them, and re-layouts  4.24 us (2%)
  other arithmetic  3.59 us (2%)
    all_to_all x1, blocking collectives, mixed_step(): lax.all_to_all(copies, 'tp_0', split_axis=0, concat_axis=0, tiled=True)  19.6 us
    pallas_call x1, Pallas kernels, span_terms(): pl.pallas_call(functools.partial(span_kernel, chunks), out_shape=(jax.Sha...  19 us
    all_to_all x1, waiting for transfers between devices, mixed_step(): lax.all_to_all(mixed.reshape(ring, 2 * BLOCK, HEAD), 'tp_0', split_axis=0...  15.6 us
    all_gather x1, waiting for transfers between devices, mixed_step(): mix_rows = lax.all_gather(mix_normed, TP, axis=0, tiled=True)  12.7 us
    all_to_all x1, waiting for transfers between devices, mixed_step(): lax.all_to_all(packed, EP, split_axis=0, concat_axis=0, tiled=True)  12.3 us
    ppermute x7, starting transfers between devices, mixed_step(): lax.ppermute(parts[k], 'tp_0', [(i, (i + k) % ring) for i in range(ring)])  11.2 us
    all_to_all x1, waiting for transfers between devices, mixed_step(): back = lax.all_to_all(pair, EP, split_axis=0, concat_axis=0, tiled=True)  10.2 us
    ppermute x6, starting transfers between devices, around(): lax.ppermute(x, axis, [(i, (i + k) % size) for i in range(size)])  9.75 us
  transfers between devices with their start and end apart: 21, of which 9 were waited for; matrix products, arithmetic and copies ran while one was open for 0% of the time, Pallas kernels for 20%

profile of v4, /device:TPU:1, one launch (start us, length us, event | category | flops | bytes accessed | tf_op | source)
XLA Modules:
  0.0 184.8 jit_solution(15096338711951434273)
XLA Ops:
  7.2 0.0 all-gather.3.cloned.1.call-start
  7.3 1.2 fusion
  8.5 2.0 %fusion.2 = bf16[128,2048]{1,0:T(8,128)(2,1)} fusion(bf16[128,2048]{1,0:T(8,128)(2,1)} %param.19, f32[2048]{0:T(1024)} %param.20, f32[128]{0:T(128)S(1)} %add_rsqrt_fusion.1), kind=kLoop, calls=%fused_computation.4 | loop fusion | flops 1048576 | bytes 1057280 | tf_op jit(solution)/shard_map/convert_element_type | solution.py:41
  10.5 0.0 all-gather.3.cloned.1.call-update
  10.5 0.0 all-gather.5.cloned.1.call-start
  10.6 0.7 all-gather.5.cloned.1.call-update
  11.4 0.1 copy.22
  11.4 0.1 fusion.4
  11.6 0.1 fusion.6
  11.7 19.6 %all_to_all.32 = bf16[8,8,2176]{2,1,0:T(8,128)(2,1)} all-to-all(bf16[8,8,2176]{2,1,0:T(8,128)(2,1)S(1)} %broadcast_in_dim.27), channel_id=1, replica_groups=mesh['ep_0'=4,'ep_1'=4,'tp_0'=8,'tp_1'=2] {'tp_0'}, dimensions={0} | all-to-all | bytes 557056 | tf_op jit(solution)/shard_map/all_to_all | solution.py:515
  31.4 2.6 %shard_map.199 = bf16[256,2048]{1,0:T(8,128)(2,1)} custom-call(bf16[64,2176]{1,0:T(8,128)(2,1)} %bitcast.23), custom_call_target="tpu_custom_call" | custom-call | flops 71303168 | bytes 1114112 | tf_op jit(solution)/shard_map/pallas_call | solution.py:372
  33.9 6.8 %all-to-all-start.2 = ((bf16[16,16,2048]{2,1,0:T(8,128)(2,1)}), bf16[16,16,2048]{2,1,0:T(8,128)(2,1)S(1)}, u32[]{:S(2)}, u32[]{:S(2)}) async-start(bf16[16,16,2048]{2,1,0:T(8,128)(2,1)} %bitcast.31), calls=%async_computation.2 | async-start | bytes 2097152 | tf_op jit(solution)/shard_map/all_to_all | solution.py:517
  42.0 0.1 pad_maximum_fusion.1.scal_ref
  42.1 12.3 %all-to-all-done.2 = bf16[16,16,2048]{2,1,0:T(8,128)(2,1)S(1)} async-done(((bf16[16,16,2048]{2,1,0:T(8,128)(2,1)}), bf16[16,16,2048]{2,1,0:T(8,128)(2,1)S(1)}, u32[]{:S(2)}, u32[]{:S(2)}) %all-to-all-start.2) | async-done | bytes 1048608 | tf_op jit(solution)/shard_map/all_to_all | solution.py:517
  54.4 4.8 %collective-permute-start.7 = (bf16[256,2048]{1,0:T(8,128)(2,1)S(1)}, bf16[256,2048]{1,0:T(8,128)(2,1)S(1)}, u32[]{:S(2)}, u32[]{:S(2)}) collective-permute-start(bf16[256,2048]{1,0:T(8,128)(2,1)S(1)} %bitcast.25), channel_id=1, source_target_pairs={{0,1},{1,0},{2,3},{3,2},{4,5},{5,4},{6,7},{7,6},{8,9},{9,8},{10,11... | collective-permute-start | bytes 3145736 | tf_op jit(solution)/shard_map/ppermute | solution.py:500
  59.3 12.7 %all-gather.3.cloned.1.call-done.rows_ref = bf16[2048,2048]{1,0:T(8,128)(2,1)} async-done(((bf16[128,2048]{1,0:T(8,128)(2,1)}), bf16[2048,2048]{1,0:T(8,128)(2,1)}) %all-gather.3.cloned.1.call-update) | async-done | bytes 8388624 | tf_op jit(solution)/shard_map/all_gather | solution.py:503
  72.0 19.0 %shard_map.194 = (bf16[2048,128]{1,0:T(8,128)(2,1)S(1)}, f32[2048,128]{1,0:T(8,128)S(1)}, bf16[128,256]{1,0:T(8,128)(2,1)S(1)}) custom-call(f32[2]{0:T(128)S(1)} %pad_maximum_fusion.1.scal_ref, s32[1]{0:T(128)} %bitcast.3.head_ref, bf16[2048,2048]{1,0:T(8,128)(2,1)} %all-gather.3.cloned.1.call-done.rows_ref, bf16[2048,128]{1,0:T(8,128)(2,1)} %q_ref.1, ...), custom_call_target="tpu_custom_call" | custom-call | flops 15032385536 | bytes 12058624 | tf_op jit(solution)/shard_map/pallas_call | solution.py:163
  91.0 1.3 collective-permute-start
  92.3 2.4 %collective-permute-start.1 = (bf16[128,256]{1,0:T(8,128)(2,1)S(1)}, bf16[128,256]{1,0:T(8,128)(2,1)}, u32[]{:S(2)}, u32[]{:S(2)}) collective-permute-start(bf16[128,256]{1,0:T(8,128)(2,1)S(1)} %get-tuple-element.19.own_ref), channel_id=1, source_target_pairs={{0,32},{16,48},{32,0},{48,16},{1,33},{17,49},{33,1},{49,17},{2,34}... | collective-permute-start | bytes 196616 | tf_op jit(solution)/shard_map/ppermute | solution.py:472
  94.7 1.2 collective-permute-start.2
  95.9 0.0 collective-permute-done.7.other_ref
  95.9 1.0 copy-done.4
  96.9 1.2 copy-done.5
  98.1 6.1 %shard_map.200 = (bf16[256,2048]{1,0:T(8,128)(2,1)S(1)}, bf16[256,2048]{1,0:T(8,128)(2,1)}) custom-call(bf16[256,2048]{1,0:T(8,128)(2,1)S(1)} %bitcast.26, bf16[256,2048]{1,0:T(8,128)(2,1)S(1)} %copy-done.5, bf16[448,2048]{1,0:T(8,128)(2,1)} %bitcast.32, bf16[448,2048]{1,0:T(8,128)(2,1)} %bitcast.33, bf16[448,2048]{1,0:T(8,128)(2,1)} %bitcast.34), custom_call_target="tpu_custom_call" | custom-call | flops 2818572288 | bytes 9699328 | tf_op jit(solution)/shard_map/pallas_call | solution.py:449
  104.2 1.2 collective-permute-start.8
  105.4 0.0 collective-permute-done.one_ref
  105.4 0.0 collective-permute-done.1.two_ref
  105.4 0.0 collective-permute-done.2.three_ref
  105.4 1.4 shard_map.195
  106.7 1.3 collective-permute-start.3
  108.0 2.5 %collective-permute-start.4 = (bf16[128,256]{1,0:T(8,128)(2,1)S(1)}, bf16[128,256]{1,0:T(8,128)(2,1)S(1)}, u32[]{:S(2)}, u32[]{:S(2)}) collective-permute-start(bf16[128,256]{1,0:T(8,128)(2,1)S(1)} %get-tuple-element.20), channel_id=1, source_target_pairs={{0,128},{64,192},{128,0},{192,64},{1,129},{65,193},{129,1},{193,65... | collective-permute-start | bytes 196616 | tf_op jit(solution)/shard_map/ppermute | solution.py:472
  110.5 1.1 collective-permute-start.5
  111.6 0.1 collective-permute-done.3.one_ref
  111.7 2.3 %collective-permute-done.4.two_ref = bf16[128,256]{1,0:T(8,128)(2,1)S(1)} collective-permute-done((bf16[128,256]{1,0:T(8,128)(2,1)S(1)}, bf16[128,256]{1,0:T(8,128)(2,1)S(1)}, u32[]{:S(2)}, u32[]{:S(2)}) %collective-permute-start.4) | collective-permute-done | bytes 65568 | tf_op jit(solution)/shard_map/ppermute | solution.py:472
  114.1 0.0 collective-permute-done.5.three_ref
  114.1 1.2 copy-done.2
  115.3 0.7 copy-done.3
  116.0 1.7 shard_map.196
  117.7 4.3 %all-to-all-start = ((bf16[8,256,128]{2,1,0:T(8,128)(2,1)}), bf16[8,256,128]{2,1,0:T(8,128)(2,1)S(1)}, u32[]{:S(2)}, u32[]{:S(2)}) async-start(bf16[8,256,128]{2,1,0:T(8,128)(2,1)} %bitcast.8), calls=%async_computation | async-start | bytes 1048576 | tf_op jit(solution)/shard_map/all_to_all | solution.py:542
  122.0 0.0 collective-permute-done.8.theirs_ref
  122.0 1.2 shard_map.201
  123.3 15.6 %all-to-all-done.x_ref = bf16[8,256,128]{2,1,0:T(8,128)(2,1)S(1)} async-done(((bf16[8,256,128]{2,1,0:T(8,128)(2,1)}), bf16[8,256,128]{2,1,0:T(8,128)(2,1)S(1)}, u32[]{:S(2)}, u32[]{:S(2)}) %all-to-all-start) | async-done | bytes 524320 | tf_op jit(solution)/shard_map/all_to_all | solution.py:542
  138.9 6.6 %all-to-all-start.3 = ((bf16[16,16,2048]{2,1,0:T(8,128)(2,1)}), bf16[16,16,2048]{2,1,0:T(8,128)(2,1)S(1)}, u32[]{:S(2)}, u32[]{:S(2)}) async-start(bf16[16,16,2048]{2,1,0:T(8,128)(2,1)} %bitcast.18), calls=%async_computation.3 | async-start | bytes 2097152 | tf_op jit(solution)/shard_map/all_to_all | solution.py:521
  145.5 0.0 all-gather.5.cloned.1.call-done.w_ref
  145.5 2.7 %shard_map.197 = (f32[128,2048]{1,0:T(8,128)S(1)}, bf16[128,2048]{1,0:T(8,128)(2,1)S(1)}) custom-call(s32[1]{0:T(128)} %bitcast.core_ref, bf16[8,256,128]{2,1,0:T(8,128)(2,1)S(1)} %all-to-all-done.x_ref, bf16[1024,2048]{1,0:T(8,128)(2,1)} %all-gather.5.cloned.1.call-done.w_ref), custom_call_target="tpu_custom_call" | custom-call | flops 1073741824 | bytes 4194304 | tf_op jit(solution)/shard_map/pallas_call | solution.py:304
  148.3 2.1 %collective-permute-start.6 = (bf16[128,2048]{1,0:T(8,128)(2,1)S(1)}, bf16[128,2048]{1,0:T(8,128)(2,1)S(1)}, u32[]{:S(2)}, u32[]{:S(2)}) collective-permute-start(bf16[128,2048]{1,0:T(8,128)(2,1)S(1)} %get-tuple-element.25), channel_id=1, source_target_pairs={{0,1},{1,0},{2,3},{3,2},{4,5},{5,4},{6,7},{7,6},{8,9},{9,8},{10,11... | collective-permute-start | bytes 1572872 | tf_op jit(solution)/shard_map/ppermute | solution.py:500
  150.4 10.2 %all-to-all-done.3 = bf16[16,16,2048]{2,1,0:T(8,128)(2,1)S(1)} async-done(((bf16[16,16,2048]{2,1,0:T(8,128)(2,1)}), bf16[16,16,2048]{2,1,0:T(8,128)(2,1)S(1)}, u32[]{:S(2)}, u32[]{:S(2)}) %all-to-all-start.3) | async-done | bytes 1048608 | tf_op jit(solution)/shard_map/all_to_all | solution.py:521
  160.6 0.7 shard_map.202
  161.3 1.9 %collective-permute-start.9 = (bf16[8,2048]{1,0:T(8,128)(2,1)S(1)}, bf16[8,2048]{1,0:T(8,128)(2,1)S(1)}, u32[]{:S(2)}, u32[]{:S(2)}) collective-permute-start(bf16[8,2048]{1,0:T(8,128)(2,1)S(1)} %get-tuple-element.29), channel_id=1, source_target_pairs={{0,2},{2,4},{4,6},{6,8},{8,10},{10,12},{12,14},{14,0},{1,3},{3,5},... | collective-permute-start | bytes 98312 | tf_op jit(solution)/shard_map/ppermute | solution.py:552
  163.2 0.0 collective-permute-start.10
  163.2 2.7 %collective-permute-start.11 = (bf16[8,2048]{1,0:T(8,128)(2,1)S(1)}, bf16[8,2048]{1,0:T(8,128)(2,1)S(1)}, u32[]{:S(2)}, u32[]{:S(2)}) collective-permute-start(bf16[8,2048]{1,0:T(8,128)(2,1)S(1)} %get-tuple-element.31), channel_id=1, source_target_pairs={{0,6},{2,8},{4,10},{6,12},{8,14},{10,0},{12,2},{14,4},{1,7},{3,9},... | collective-permute-start | bytes 98312 | tf_op jit(solution)/shard_map/ppermute | solution.py:552
  165.9 2.8 %collective-permute-start.12 = (bf16[8,2048]{1,0:T(8,128)(2,1)S(1)}, bf16[8,2048]{1,0:T(8,128)(2,1)S(1)}, u32[]{:S(2)}, u32[]{:S(2)}) collective-permute-start(bf16[8,2048]{1,0:T(8,128)(2,1)S(1)} %get-tuple-element.32), channel_id=1, source_target_pairs={{0,8},{2,10},{4,12},{6,14},{8,0},{10,2},{12,4},{14,6},{1,9},{3,11}... | collective-permute-start | bytes 98312 | tf_op jit(solution)/shard_map/ppermute | solution.py:552
  168.7 0.0 collective-permute-done.9.refs_1_
  168.7 1.5 collective-permute-start.13
  170.2 0.0 collective-permute-done.10.refs_2_
  170.2 1.9 %collective-permute-start.14 = (bf16[8,2048]{1,0:T(8,128)(2,1)S(1)}, bf16[8,2048]{1,0:T(8,128)(2,1)S(1)}, u32[]{:S(2)}, u32[]{:S(2)}) collective-permute-start(bf16[8,2048]{1,0:T(8,128)(2,1)S(1)} %get-tuple-element.34), channel_id=1, source_target_pairs={{0,12},{2,14},{4,0},{6,2},{8,4},{10,6},{12,8},{14,10},{1,13},{3,15... | collective-permute-start | bytes 98312 | tf_op jit(solution)/shard_map/ppermute | solution.py:552
  172.1 0.0 collective-permute-done.11.refs_3_
  172.1 0.4 collective-permute-start.15
  172.5 0.5 collective-permute-done.12.refs_4_
  173.0 0.6 collective-permute-done.13.refs_5_
  173.6 2.8 %collective-permute-done.14.refs_6_ = bf16[8,2048]{1,0:T(8,128)(2,1)S(1)} collective-permute-done((bf16[8,2048]{1,0:T(8,128)(2,1)S(1)}, bf16[8,2048]{1,0:T(8,128)(2,1)S(1)}, u32[]{:S(2)}, u32[]{:S(2)}) %collective-permute-start.14) | collective-permute-done | bytes 32800 | tf_op jit(solution)/shard_map/ppermute | solution.py:552
  176.4 0.0 collective-permute-done.15.refs_7_
  176.4 0.7 shard_map.203
  177.0 0.9 shard_map.198
  (30 shorter events, 0.1 us)
Async XLA Ops:
  7.2 4.1 %copy-start.12 = (s32[8,2]{0,1:T(2,128)S(1)}, s32[8,2]{0,1:T(2,128)}, u32[]{:S(2)}) copy-start(s32[8,2]{0,1:T(2,128)} %param.33) | copy-start | bytes 196
  7.2 4.1 %copy-start.11 = (f32[8,2]{0,1:T(2,128)S(1)}, f32[8,2]{0,1:T(2,128)}, u32[]{:S(2)}) copy-start(f32[8,2]{0,1:T(2,128)} %param.34) | copy-start | bytes 196
  7.2 4.3 %copy-start.9 = (bf16[8,2048]{1,0:T(8,128)(2,1)S(1)}, bf16[8,2048]{1,0:T(8,128)(2,1)}, u32[]{:S(2)}) copy-start(bf16[8,2048]{1,0:T(8,128)(2,1)} %param.31) | copy-start | bytes 98308
  7.2 4.4 %copy-start.10 = (f32[2048]{0:T(1024)S(1)}, f32[2048]{0:T(1024)}, u32[]{:S(2)}) copy-start(f32[2048]{0:T(1024)} %param.32) | copy-start | bytes 24580
  7.2 64.8 %all-gather.3.cloned.1.call-start = ((), (), s32[]{:S(2)}) async-start(), calls=%async_computation.4 | async-start | bytes 8912896 | tf_op jit(solution)/shard_map/all_gather | solution.py:503
  10.5 134.9 %all-gather.5.cloned.1.call-start = ((), (), s32[]{:S(2)}) async-start(), calls=%async_computation.5 | async-start | bytes 4718592 | tf_op jit(solution)/shard_map/all_gather | solution.py:545
  31.4 40.6 %copy-start.6 = (bf16[2048,16]{0,1:T(8,128)(2,1)S(1)}, bf16[2048,16]{0,1:T(8,128)(2,1)}, u32[]{:S(2)}) copy-start(bf16[2048,16]{0,1:T(8,128)(2,1)} %param.24) | copy-start | bytes 196612
  31.4 40.6 %copy-start.7 = (bf16[2048,16]{0,1:T(8,128)(2,1)S(1)}, bf16[2048,16]{0,1:T(8,128)(2,1)}, u32[]{:S(2)}) copy-start(bf16[2048,16]{0,1:T(8,128)(2,1)} %param.25) | copy-start | bytes 196612
  31.4 40.6 %copy-start.8 = (f32[2048,1]{0,1:T(1,128)S(1)}, f32[2048,1]{0,1:T(1,128)}, u32[]{:S(2)}) copy-start(f32[2048,1]{0,1:T(1,128)} %param.28) | copy-start | bytes 24580
  33.9 20.5 %all-to-all-start.2 = ((bf16[16,16,2048]{2,1,0:T(8,128)(2,1)}), bf16[16,16,2048]{2,1,0:T(8,128)(2,1)S(1)}, u32[]{:S(2)}, u32[]{:S(2)}) async-start(bf16[16,16,2048]{2,1,0:T(8,128)(2,1)} %bitcast.31), calls=%async_computation.2 | async-start | bytes 2097152 | tf_op jit(solution)/shard_map/all_to_all | solution.py:517
  54.4 41.4 %collective-permute-start.7 = (bf16[256,2048]{1,0:T(8,128)(2,1)S(1)}, bf16[256,2048]{1,0:T(8,128)(2,1)S(1)}, u32[]{:S(2)}, u32[]{:S(2)}) collective-permute-start(bf16[256,2048]{1,0:T(8,128)(2,1)S(1)} %bitcast.25), channel_id=1, source_target_pairs={{0,1},{1,0},{2,3},{3,2},{4,5},{5,4},{6,7},{7,6},{8,9},{9,8},{10,11... | collective-permute-start | bytes 3145736 | tf_op jit(solution)/shard_map/ppermute | solution.py:500
  91.0 13.1 %copy-start.1 = (f32[2048,128]{1,0:T(8,128)}, f32[2048,128]{1,0:T(8,128)S(1)}, u32[]{:S(2)}) copy-start(f32[2048,128]{1,0:T(8,128)S(1)} %get-tuple-element.23.h_ref) | copy-start | bytes 3145732
  91.0 14.3 %collective-permute-start = (bf16[128,256]{1,0:T(8,128)(2,1)S(1)}, bf16[128,256]{1,0:T(8,128)(2,1)S(1)}, u32[]{:S(2)}, u32[]{:S(2)}) collective-permute-start(bf16[128,256]{1,0:T(8,128)(2,1)S(1)} %get-tuple-element.19.own_ref), channel_id=1, source_target_pairs={{0,16},{16,32},{32,48},{48,0},{1,17},{17,33},{33,49},{49,1},{2,18}... | collective-permute-start | bytes 196616 | tf_op jit(solution)/shard_map/ppermute | solution.py:472
  92.3 13.1 %collective-permute-start.1 = (bf16[128,256]{1,0:T(8,128)(2,1)S(1)}, bf16[128,256]{1,0:T(8,128)(2,1)}, u32[]{:S(2)}, u32[]{:S(2)}) collective-permute-start(bf16[128,256]{1,0:T(8,128)(2,1)S(1)} %get-tuple-element.19.own_ref), channel_id=1, source_target_pairs={{0,32},{16,48},{32,0},{48,16},{1,33},{17,49},{33,1},{49,17},{2,34}... | collective-permute-start | bytes 196616 | tf_op jit(solution)/shard_map/ppermute | solution.py:472
  94.7 10.6 %collective-permute-start.2 = (bf16[128,256]{1,0:T(8,128)(2,1)S(1)}, bf16[128,256]{1,0:T(8,128)(2,1)}, u32[]{:S(2)}, u32[]{:S(2)}) collective-permute-start(bf16[128,256]{1,0:T(8,128)(2,1)S(1)} %get-tuple-element.19.own_ref), channel_id=1, source_target_pairs={{0,48},{16,0},{32,16},{48,32},{1,49},{17,1},{33,17},{49,33},{2,50}... | collective-permute-start | bytes 196616 | tf_op jit(solution)/shard_map/ppermute | solution.py:472
  95.9 1.0 copy-start.4
  96.9 1.2 copy-start.5
  104.2 17.9 %collective-permute-start.8 = (bf16[256,2048]{1,0:T(8,128)(2,1)}, bf16[256,2048]{1,0:T(8,128)(2,1)S(1)}, u32[]{:S(2)}, u32[]{:S(2)}) collective-permute-start(bf16[256,2048]{1,0:T(8,128)(2,1)} %get-tuple-element.27), channel_id=1, source_target_pairs={{0,1},{1,0},{2,3},{3,2},{4,5},{5,4},{6,7},{7,6},{8,9},{9,8},{10,11... | collective-permute-start | bytes 3145736 | tf_op jit(solution)/shard_map/ppermute | solution.py:500
  106.7 5.0 %collective-permute-start.3 = (bf16[128,256]{1,0:T(8,128)(2,1)S(1)}, bf16[128,256]{1,0:T(8,128)(2,1)S(1)}, u32[]{:S(2)}, u32[]{:S(2)}) collective-permute-start(bf16[128,256]{1,0:T(8,128)(2,1)S(1)} %get-tuple-element.20), channel_id=1, source_target_pairs={{0,64},{64,128},{128,192},{192,0},{1,65},{65,129},{129,193},{193,1... | collective-permute-start | bytes 196616 | tf_op jit(solution)/shard_map/ppermute | solution.py:472
  108.0 6.0 %collective-permute-start.4 = (bf16[128,256]{1,0:T(8,128)(2,1)S(1)}, bf16[128,256]{1,0:T(8,128)(2,1)S(1)}, u32[]{:S(2)}, u32[]{:S(2)}) collective-permute-start(bf16[128,256]{1,0:T(8,128)(2,1)S(1)} %get-tuple-element.20), channel_id=1, source_target_pairs={{0,128},{64,192},{128,0},{192,64},{1,129},{65,193},{129,1},{193,65... | collective-permute-start | bytes 196616 | tf_op jit(solution)/shard_map/ppermute | solution.py:472
  110.5 3.5 %collective-permute-start.5 = (bf16[128,256]{1,0:T(8,128)(2,1)S(1)}, bf16[128,256]{1,0:T(8,128)(2,1)S(1)}, u32[]{:S(2)}, u32[]{:S(2)}) collective-permute-start(bf16[128,256]{1,0:T(8,128)(2,1)S(1)} %get-tuple-element.20), channel_id=1, source_target_pairs={{0,192},{64,0},{128,64},{192,128},{1,193},{65,1},{129,65},{193,129... | collective-permute-start | bytes 196616 | tf_op jit(solution)/shard_map/ppermute | solution.py:472
  114.1 1.2 copy-start.2
  115.3 0.7 copy-start.3
  117.7 21.2 %all-to-all-start = ((bf16[8,256,128]{2,1,0:T(8,128)(2,1)}), bf16[8,256,128]{2,1,0:T(8,128)(2,1)S(1)}, u32[]{:S(2)}, u32[]{:S(2)}) async-start(bf16[8,256,128]{2,1,0:T(8,128)(2,1)} %bitcast.8), calls=%async_computation | async-start | bytes 1048576 | tf_op jit(solution)/shard_map/all_to_all | solution.py:542
  138.9 21.7 %all-to-all-start.3 = ((bf16[16,16,2048]{2,1,0:T(8,128)(2,1)}), bf16[16,16,2048]{2,1,0:T(8,128)(2,1)S(1)}, u32[]{:S(2)}, u32[]{:S(2)}) async-start(bf16[16,16,2048]{2,1,0:T(8,128)(2,1)} %bitcast.18), calls=%async_computation.3 | async-start | bytes 2097152 | tf_op jit(solution)/shard_map/all_to_all | solution.py:521
  145.5 15.1 %copy-start = (bf16[8,8,2176]{2,1,0:T(8,128)(2,1)S(1)}, bf16[8,8,2176]{2,1,0:T(8,128)(2,1)}, u32[]{:S(2)}) copy-start(bf16[8,8,2176]{2,1,0:T(8,128)(2,1)} %all_to_all.32) | copy-start | bytes 835588
  148.3 28.8 %collective-permute-start.6 = (bf16[128,2048]{1,0:T(8,128)(2,1)S(1)}, bf16[128,2048]{1,0:T(8,128)(2,1)S(1)}, u32[]{:S(2)}, u32[]{:S(2)}) collective-permute-start(bf16[128,2048]{1,0:T(8,128)(2,1)S(1)} %get-tuple-element.25), channel_id=1, source_target_pairs={{0,1},{1,0},{2,3},{3,2},{4,5},{5,4},{6,7},{7,6},{8,9},{9,8},{10,11... | collective-permute-start | bytes 1572872 | tf_op jit(solution)/shard_map/ppermute | solution.py:500
  161.3 7.4 %collective-permute-start.9 = (bf16[8,2048]{1,0:T(8,128)(2,1)S(1)}, bf16[8,2048]{1,0:T(8,128)(2,1)S(1)}, u32[]{:S(2)}, u32[]{:S(2)}) collective-permute-start(bf16[8,2048]{1,0:T(8,128)(2,1)S(1)} %get-tuple-element.29), channel_id=1, source_target_pairs={{0,2},{2,4},{4,6},{6,8},{8,10},{10,12},{12,14},{14,0},{1,3},{3,5},... | collective-permute-start | bytes 98312 | tf_op jit(solution)/shard_map/ppermute | solution.py:552
  163.2 6.9 %collective-permute-start.10 = (bf16[8,2048]{1,0:T(8,128)(2,1)S(1)}, bf16[8,2048]{1,0:T(8,128)(2,1)S(1)}, u32[]{:S(2)}, u32[]{:S(2)}) collective-permute-start(bf16[8,2048]{1,0:T(8,128)(2,1)S(1)} %get-tuple-element.30), channel_id=1, source_target_pairs={{0,4},{2,6},{4,8},{6,10},{8,12},{10,14},{12,0},{14,2},{1,5},{3,7},... | collective-permute-start | bytes 98312 | tf_op jit(solution)/shard_map/ppermute | solution.py:552
  163.2 8.9 %collective-permute-start.11 = (bf16[8,2048]{1,0:T(8,128)(2,1)S(1)}, bf16[8,2048]{1,0:T(8,128)(2,1)S(1)}, u32[]{:S(2)}, u32[]{:S(2)}) collective-permute-start(bf16[8,2048]{1,0:T(8,128)(2,1)S(1)} %get-tuple-element.31), channel_id=1, source_target_pairs={{0,6},{2,8},{4,10},{6,12},{8,14},{10,0},{12,2},{14,4},{1,7},{3,9},... | collective-permute-start | bytes 98312 | tf_op jit(solution)/shard_map/ppermute | solution.py:552
  165.9 7.1 %collective-permute-start.12 = (bf16[8,2048]{1,0:T(8,128)(2,1)S(1)}, bf16[8,2048]{1,0:T(8,128)(2,1)S(1)}, u32[]{:S(2)}, u32[]{:S(2)}) collective-permute-start(bf16[8,2048]{1,0:T(8,128)(2,1)S(1)} %get-tuple-element.32), channel_id=1, source_target_pairs={{0,8},{2,10},{4,12},{6,14},{8,0},{10,2},{12,4},{14,6},{1,9},{3,11}... | collective-permute-start | bytes 98312 | tf_op jit(solution)/shard_map/ppermute | solution.py:552
  168.7 4.9 %collective-permute-start.13 = (bf16[8,2048]{1,0:T(8,128)(2,1)S(1)}, bf16[8,2048]{1,0:T(8,128)(2,1)S(1)}, u32[]{:S(2)}, u32[]{:S(2)}) collective-permute-start(bf16[8,2048]{1,0:T(8,128)(2,1)S(1)} %get-tuple-element.33), channel_id=1, source_target_pairs={{0,10},{2,12},{4,14},{6,0},{8,2},{10,4},{12,6},{14,8},{1,11},{3,13... | collective-permute-start | bytes 98312 | tf_op jit(solution)/shard_map/ppermute | solution.py:552
  170.2 6.2 %collective-permute-start.14 = (bf16[8,2048]{1,0:T(8,128)(2,1)S(1)}, bf16[8,2048]{1,0:T(8,128)(2,1)S(1)}, u32[]{:S(2)}, u32[]{:S(2)}) collective-permute-start(bf16[8,2048]{1,0:T(8,128)(2,1)S(1)} %get-tuple-element.34), channel_id=1, source_target_pairs={{0,12},{2,14},{4,0},{6,2},{8,4},{10,6},{12,8},{14,10},{1,13},{3,15... | collective-permute-start | bytes 98312 | tf_op jit(solution)/shard_map/ppermute | solution.py:552
  172.1 4.3 %collective-permute-start.15 = (bf16[8,2048]{1,0:T(8,128)(2,1)S(1)}, bf16[8,2048]{1,0:T(8,128)(2,1)S(1)}, u32[]{:S(2)}, u32[]{:S(2)}) collective-permute-start(bf16[8,2048]{1,0:T(8,128)(2,1)S(1)} %get-tuple-element.35), channel_id=1, source_target_pairs={{0,14},{2,0},{4,2},{6,4},{8,6},{10,8},{12,10},{14,12},{1,15},{3,1}... | collective-permute-start | bytes 98312 | tf_op jit(solution)/shard_map/ppermute | solution.py:552
Sparse Core Ops, SparseCore 0:
  10.7 61.2 all-gather.2
  73.8 52.9 all-gather.4
